TPU v7x, 512 devices: a whole 4x8x8 slice. The times are simulated.
512 devices in a mesh: sp: 64 (over z, y), tp: 8 (over x, core).
Axes of the slice: x: 4, y: 8, z: 8, core: 2. Of those that a mesh axis runs over, the one named last changes fastest.
Arguments:
- skip_path_inputs: bfloat16 [8192, 2048], P('sp'), may hold values from -62 to 62
- probe_vectors: bfloat16 [8192, 1024], P('sp', 'tp'), may hold values from -6 to 6
- lookup_vectors: bfloat16 [8192, 1024], P('sp', 'tp'), may hold values from -6 to 6
- payload_vectors: bfloat16 [8192, 1024], P('sp', 'tp'), may hold values from -6 to 6
- learning_strength_preacts: float32 [2, 8192, 8], P(None, 'sp', 'tp'), may hold values from -6 to 6
- forget_preacts: float32 [2, 8192, 8], P(None, 'sp', 'tp'), may hold values from -5 to 5
- forgetting_speed_exponent: float32 [2, 8], P(None, 'tp'), may hold values from -12 to -2
- extra_forgetting_spikes: float32 [2, 8192, 8], P(None, 'sp', 'tp'), may hold values from -0.7 to 0
- sample_membership: int32 [8192], P('sp'), may hold values from 0 to 15, never falling along the last dimension, each value on 1 to 1024 neighbouring positions
- channel_group_scaling: float32 [128], replicated, may hold values from 0.1 to 1.9
- blend_exit_weights: bfloat16 [1024, 2048], P('tp'), may hold values from -0.1875 to 0.1875
- dense_block_scaling: float32 [2048], replicated, may hold values from 0.1 to 1.9
- widen_projection_weights: bfloat16 [2048, 8192], P('sp', 'tp'), may hold values from -0.125 to 0.125
- shrink_projection_weights: bfloat16 [8192, 2048], P('tp', 'sp'), may hold values from -0.0625 to 0.0625
Outputs:
- result: bfloat16 [8192, 2048], P('sp', 'tp')
Inputs may be any that keep to these rules, and one draw needn't show every extreme that they name: `sample_membership`: document numbers never fall along the positions; each document holds 1 to 1024 positions.
All inputs are finite; a program needn't handle non-finite values.
Results may differ from a plain program's by a relative error of at most 0.015.
Values may be sent and summed in bfloat16 or wider, within the bound.
No kernel may reach another device: no remote copies, remote signals or barrier semaphores. Data moves between devices by JAX's collectives and lax.ppermute only.
A program may use at most 64 MiB of HBM per device.

v0:
```python
import jax
import jax.numpy as jnp
from jax import lax
from jax.sharding import Mesh
from jax.sharding import PartitionSpec as P

BLOCK = 64
SP = ("sp_0", "sp_1")


EPSILON = 1e-06


def rows_first(arrays, axis, dims):
    turned = [jnp.moveaxis(a, dim, 0) for a, dim in zip(arrays, dims)]
    both = jnp.concatenate([t.reshape(len(t), -1) for t in turned], axis=1)
    out, at, gathered = (lax.all_gather(both, axis, axis=0, tiled=True), 0, [])
    for t, dim in zip(turned, dims):
        section = out[:, at : at + t[0].size].reshape(-1, *t.shape[1:])
        gathered.append(jnp.moveaxis(section, 0, dim))
        at += t[0].size
    return tuple(gathered)


def neutral_like(array, identity):
    return jax.tree.map(
        lambda a, e: jnp.broadcast_to(jnp.asarray(e, a.dtype), a.shape), array, identity
    )


def all_in_one(array, axis):
    leaves = jax.tree.leaves(array)
    turns = sorted(range(len(leaves)), key=lambda k: -leaves[k].size)
    width = (1, *leaves[turns[0]].shape)[-1]
    lines = [
        jnp.pad(leaves[k].reshape(-1), (0, -leaves[k].size % width)).reshape(-1, width)
        for k in turns
    ]
    both, at, found = (lax.all_gather(jnp.concatenate(lines), axis), 0, {})
    for k, line in zip(turns, lines):
        section = both[:, at : at + len(line)].reshape(len(both), -1)
        found[k] = section[:, : leaves[k].size].reshape(-1, *leaves[k].shape)
        at += len(line)
    numbers = iter(range(len(leaves)))
    return jax.tree.map(lambda _: found[next(numbers)], array)


def carried_in(array, axes, combine, identity, reverse):
    before = start = neutral_like(array, identity)
    running = array
    for axis in reversed(axes):
        length, here = (lax.axis_size(axis), lax.axis_index(axis))
        pieces = all_in_one(
            jax.tree.map(
                lambda part, kind: part.astype(kind),
                running,
                jax.tree.map(lambda a: jnp.bfloat16 if a.dtype == jnp.float32 else a.dtype, array),
            ),
            axis,
        )
        inside, running = (start, start)
        for k in reversed(range(length)) if reverse else range(length):
            passed = k > here if reverse else k < here
            running = combine(
                running, jax.tree.map(lambda part, own: part[k].astype(own.dtype), pieces, array)
            )
            inside = jax.tree.map(lambda new, old: jnp.where(passed, new, old), running, inside)
        before = combine(inside, before)
    return before


def split_up(array, dim, length):
    before, after = (array.shape[:dim], array.shape[dim + 1 :])
    return jnp.moveaxis(array.reshape(*before, length, -1, *after), dim, 0)


def sent_and_summed(array, axis, dim):
    length = lax.axis_size(axis)
    parts = lax.all_to_all(split_up(array, dim, length), axis, 0, 0, tiled=True)
    return jnp.sum(parts.astype(jnp.float32), axis=0)


def sent_to_all(array, axis):
    length = lax.axis_size(axis)
    return lax.all_to_all(
        jnp.broadcast_to(array[None], (length, *array.shape)), axis, 0, 0, tiled=True
    )


def of_everyone(array, axis):
    everything = sent_to_all(array, axis)
    return jnp.sum(everything, axis=0)


def joined_along(parts, dim):
    parts = jnp.moveaxis(parts, 0, dim)
    dims = parts.shape
    return parts.reshape(*dims[:dim], dims[dim] * dims[dim + 1], *dims[dim + 2 :])


def gathered_copies(array, axis, dim):
    return joined_along(sent_to_all(array, axis), dim)


def block_pass(
    memory,
    probe_vectors,
    lookup_vectors,
    payload_vectors,
    strengths,
    forget_multipliers,
    doc_ids,
    prior_doc,
    wanted,
):
    value_width = payload_vectors.shape[-1]
    block_len = probe_vectors.shape[1]
    running = jnp.cumsum(forget_multipliers, axis=-1)
    row_ids = lax.broadcasted_iota(jnp.int32, (block_len, block_len), 0)
    col_ids = lax.broadcasted_iota(jnp.int32, (block_len, block_len), 1)
    shared = doc_ids[:, None] == doc_ids[None, :]
    within = (row_ids >= col_ids) & shared
    before = (row_ids > col_ids) & shared
    spread = jnp.exp(jnp.where(within, running[:, :, None] - running[:, None, :], -jnp.inf))
    linked = (doc_ids == prior_doc).astype(jnp.float32)
    ending = (doc_ids == doc_ids[-1]).astype(jnp.float32)
    weighted = lookup_vectors * strengths[..., None]
    system = jnp.eye(block_len, dtype=jnp.float32) + jnp.where(
        before, jnp.einsum("hik,hjk->hij", weighted, lookup_vectors) * spread, 0.0
    )
    right_side = jnp.concatenate(
        [payload_vectors * strengths[..., None], weighted * (jnp.exp(running) * linked)[..., None]],
        axis=-1,
    )
    solved = jax.scipy.linalg.solve_triangular(system, right_side, lower=True, unit_diagonal=True)
    update = solved[..., :value_width] - jnp.einsum(
        "hck,hkw->hcw", solved[..., value_width:], memory
    )
    faded_keys = lookup_vectors * (jnp.exp(running[:, -1:] - running) * ending)[..., None]
    kept_share = jnp.exp(running[:, -1]) * linked[-1]
    renewed = memory * kept_share[:, None, None] + jnp.einsum("hck,hcw->hkw", faded_keys, update)
    if not wanted:
        return (renewed, None)
    scores = jnp.where(
        within, jnp.einsum("hik,hjk->hij", probe_vectors, lookup_vectors) * spread, 0.0
    )
    reading = jnp.einsum(
        "hck,hkw->hcw", probe_vectors * (jnp.exp(running) * linked)[..., None], memory
    )
    return (renewed, reading + jnp.einsum("hij,hjw->hiw", scores, update))


def run_blocks(
    memory,
    prior_doc,
    probe_vectors,
    lookup_vectors,
    payload_vectors,
    strengths,
    forget_multipliers,
    doc_ids,
    wanted,
):
    head_count, length, key_width = probe_vectors.shape
    block_count = length // BLOCK

    def split_blocks(tensor):
        return jnp.moveaxis(
            tensor.reshape((head_count, block_count, BLOCK) + tensor.shape[2:]), 1, 0
        )

    def advance(carried, inputs):
        held, earlier_doc = carried
        query_block, key_block, value_block, gate_block, decay_block, doc_block = inputs
        held, produced = block_pass(
            held,
            query_block,
            key_block,
            value_block,
            gate_block,
            decay_block,
            doc_block,
            earlier_doc,
            wanted,
        )
        return ((held, doc_block[-1]), produced)

    (final, _), produced = lax.scan(
        advance,
        (memory, prior_doc),
        (
            split_blocks(probe_vectors),
            split_blocks(lookup_vectors),
            split_blocks(payload_vectors),
            split_blocks(strengths),
            split_blocks(forget_multipliers),
            doc_ids.reshape(block_count, BLOCK),
        ),
    )
    if wanted:
        produced = jnp.moveaxis(produced, 0, 1).reshape(head_count, length, -1)
    return (final, produced)


def unit_rows(tensor):
    return tensor * lax.rsqrt(jnp.sum(tensor * tensor, axis=-1, keepdims=True) + EPSILON)


def heads_first(tensor, head_width):
    row_count = tensor.shape[0]
    return jnp.transpose(tensor.astype(jnp.float32).reshape(row_count, -1, head_width), (1, 0, 2))


def summarize(
    probe_vectors, lookup_vectors, payload_vectors, strengths, forget_multipliers, doc_ids
):
    head_count, length, key_width = probe_vectors.shape
    start_map = jnp.concatenate(
        [
            jnp.broadcast_to(
                jnp.eye(key_width, dtype=jnp.float32), (head_count, key_width, key_width)
            ),
            jnp.zeros((head_count, key_width, payload_vectors.shape[-1]), jnp.float32),
        ],
        axis=-1,
    )
    padded = jnp.concatenate(
        [jnp.zeros((head_count, length, key_width), jnp.float32), payload_vectors], axis=-1
    )
    final, _ = run_blocks(
        start_map,
        doc_ids[0],
        probe_vectors,
        lookup_vectors,
        padded,
        strengths,
        forget_multipliers,
        doc_ids,
        False,
    )
    as_float = doc_ids.astype(jnp.float32)
    return (final[..., :key_width], final[..., key_width:], as_float[0], as_float[-1])


def compose(earlier, later):
    early_map, early_shift, early_first, early_last = earlier
    late_map, late_shift, late_first, late_last = later
    joined = ((late_first == early_last) | (early_last < 0) | (late_first < 0)).astype(jnp.float32)
    new_map = jnp.einsum("hij,hjk->hik", late_map, early_map) * joined
    new_shift = jnp.einsum("hij,hjk->hik", late_map, early_shift) * joined + late_shift
    return (
        new_map,
        new_shift,
        jnp.where(early_first < 0, late_first, early_first),
        jnp.where(late_last < 0, early_last, late_last),
    )


def neutral(head_count, key_width, value_width):
    return (
        jnp.broadcast_to(jnp.eye(key_width, dtype=jnp.float32), (head_count, key_width, key_width)),
        jnp.zeros((head_count, key_width, value_width), jnp.float32),
        jnp.full((), -1.0, jnp.float32),
        jnp.full((), -1.0, jnp.float32),
    )


def shards(
    skip_path_inputs,
    probe_vectors,
    lookup_vectors,
    payload_vectors,
    learning_strength_preacts,
    forget_preacts,
    forgetting_speed_exponent,
    extra_forgetting_spikes,
    sample_membership,
    channel_group_scaling,
    blend_exit_weights,
    dense_block_scaling,
    widen_projection_weights,
    shrink_projection_weights,
):
    up_whole, down_whole = rows_first(
        (widen_projection_weights, shrink_projection_weights), SP, (0, 1)
    )
    length = probe_vectors.shape[0]
    key_width = channel_group_scaling.shape[0]
    query_heads = unit_rows(heads_first(probe_vectors, key_width)) * key_width ** (-0.5)
    key_heads = unit_rows(heads_first(lookup_vectors, key_width))
    value_heads = heads_first(payload_vectors, key_width)
    head_count = query_heads.shape[0]
    strengths = jnp.transpose(jax.nn.sigmoid(learning_strength_preacts), (0, 2, 1))
    forget_multipliers = jnp.transpose(
        -jnp.exp(forgetting_speed_exponent)[:, None, :] * jax.nn.softplus(forget_preacts)
        + extra_forgetting_spikes,
        (0, 2, 1),
    )
    forward_parts = summarize(
        query_heads, key_heads, value_heads, strengths[0], forget_multipliers[0], sample_membership
    )
    forward_prefix = carried_in(
        forward_parts, SP, compose, neutral(head_count, key_width, key_width), False
    )
    _, forward_out = run_blocks(
        forward_prefix[1],
        forward_prefix[3].astype(jnp.int32),
        query_heads,
        key_heads,
        value_heads,
        strengths[0],
        forget_multipliers[0],
        sample_membership,
        True,
    )
    flipped_queries = jnp.flip(query_heads, 1)
    flipped_keys = jnp.flip(key_heads, 1)
    flipped_values = jnp.flip(value_heads, 1)
    flipped_gates = jnp.flip(strengths[1], 1)
    flipped_decays = jnp.flip(forget_multipliers[1], 1)
    flipped_docs = jnp.flip(sample_membership, 0)
    backward_parts = summarize(
        flipped_queries, flipped_keys, flipped_values, flipped_gates, flipped_decays, flipped_docs
    )
    backward_prefix = carried_in(
        backward_parts, SP, compose, neutral(head_count, key_width, key_width), True
    )
    _, backward_out = run_blocks(
        backward_prefix[1],
        backward_prefix[3].astype(jnp.int32),
        flipped_queries,
        flipped_keys,
        flipped_values,
        flipped_gates,
        flipped_decays,
        flipped_docs,
        True,
    )
    attn = forward_out + jnp.flip(backward_out, 1)
    scaled = (
        attn
        * lax.rsqrt(jnp.mean(attn * attn, axis=-1, keepdims=True) + EPSILON)
        * channel_group_scaling
    )
    mixed = (
        jnp.transpose(scaled, (1, 0, 2))
        .reshape(length, head_count * key_width)
        .astype(jnp.bfloat16)
    )
    head_terms = lax.optimization_barrier(
        jnp.dot(mixed, blend_exit_weights, preferred_element_type=jnp.float32).astype(jnp.bfloat16)
    ).astype(jnp.float32)
    model_width = skip_path_inputs.shape[1]
    col_count = model_width // lax.axis_size("tp")
    col_start = lax.axis_index("tp") * col_count
    summed = sent_and_summed(head_terms.astype(jnp.bfloat16), "tp", 1)
    own_residual = (
        lax.dynamic_slice_in_dim(skip_path_inputs, col_start, col_count, 1).astype(jnp.float32)
        + summed
    )
    squares = of_everyone(jnp.sum(own_residual * own_residual, axis=1), "tp")
    own_gain = lax.dynamic_slice_in_dim(dense_block_scaling, col_start, col_count, 0)
    own_normed = (
        own_residual * lax.rsqrt(squares / model_width + EPSILON)[:, None] * own_gain
    ).astype(jnp.bfloat16)
    normed = gathered_copies(own_normed, "tp", 1)
    raised = jnp.dot(normed, up_whole, preferred_element_type=jnp.float32)
    active = jnp.square(jax.nn.relu(raised)).astype(jnp.bfloat16)
    lowered = jnp.dot(active, down_whole, preferred_element_type=jnp.float32)
    rounded = lax.optimization_barrier(lowered.astype(jnp.bfloat16)).astype(jnp.float32)
    mixer_cols = sent_and_summed(rounded.astype(jnp.bfloat16), "tp", 1)
    return (own_residual + mixer_cols).astype(jnp.bfloat16)


def solution(mesh):
    torus = Mesh(mesh.devices.reshape(8, 8, mesh.shape["tp"]), ("sp_0", "sp_1", "tp"))
    placed = (
        P(SP, None),
        P(SP, "tp"),
        P(SP, "tp"),
        P(SP, "tp"),
        P(None, SP, "tp"),
        P(None, SP, "tp"),
        P(None, "tp"),
        P(None, SP, "tp"),
        P(SP),
        P(),
        P("tp", None),
        P(),
        P(SP, "tp"),
        P("tp", SP),
    )
    return jax.shard_map(
        shards, mesh=torus, in_specs=placed, out_specs=P(SP, "tp"), check_vma=False
    )
```

profile of v0, /device:TPU:1, one launch (start us, length us, event | category | flops | bytes accessed | tf_op | source)
XLA Modules:
  0.0 393.1 jit_solution(14457314746386228299)
XLA Ops:
  6.6 1.6 pad_maximum_fusion
  8.2 0.7 rev.22
  9.0 1.3 fusion.353
  10.3 0.7 convert_convert_fusion.1
  11.0 0.7 negate_bitcast_fusion
  11.7 0.7 add_divide_fusion
  12.4 0.8 fusion.328
  15.1 0.9 fusion.231
  16.0 0.8 convert_multiply_fusion.2
  16.9 0.8 reverse.12
  17.7 22.2 %while.54 = (s32[]{:T(128)}, f32[1,128,256]{2,1,0:T(8,128)S(1)}, s32[]{:T(128)}, s32[2,64]{1,0:T(2,128)S(1)}, f32[2,1,64]{2,1,0:T(1,128)S(1)}, /*index=5*/f32[2,...) while((s32[]{:T(128)}, f32[1,128,256]{2,1,0:T(8,128)S(1)}, ...), condition=%wide.region_10.13_spmd, body=%wide.region_8.12_spmd.sunk | while | flops 28541312 | bytes 1286924 | solution.py:188
  19.8 1.3 fusion.516
  21.4 4.9 %custom-call.18 = f32[1,64,64]{1,2,0:T(8,128)S(1)} custom-call(f32[1,64,64]{2,1,0:T(8,128)S(1)} %fusion.519), custom_call_target="InvertDiagBlocksLowerTriangular" | custom-call | tf_op jit(solution)/shard_map/while/body/eval_jaxpr/jit(_solve_triangular)/triangular_solve | solution.py:135
  31.0 1.3 fusion.516
  32.6 4.9 %custom-call.18 = f32[1,64,64]{1,2,0:T(8,128)S(1)} custom-call(f32[1,64,64]{2,1,0:T(8,128)S(1)} %fusion.519), custom_call_target="InvertDiagBlocksLowerTriangular" | custom-call | tf_op jit(solution)/shard_map/while/body/eval_jaxpr/jit(_solve_triangular)/triangular_solve | solution.py:135
  41.7 0.7 select_bitcast_fusion
  42.4 23.5 %all-gather.6 = bf16[8,258,128]{2,1,0:T(8,128)(2,1)S(1)} all-gather(bf16[1,258,128]{2,1,0:T(8,128)(2,1)S(1)} %maximum_bitcast_fusion.10), channel_id=4, replica_groups=mesh['sp_0'=8,'sp_1'=8,'tp'=8] {'sp_1'}, dimensions={0}, use_global_device_ids=true | all-gather | bytes 594432 | tf_op jit(solution)/shard_map/all_gather | solution.py:39
  66.2 0.6 fusion.348
  69.5 0.6 fusion.347
  95.0 28.1 %all-gather.7 = bf16[8,258,128]{2,1,0:T(8,128)(2,1)S(1)} all-gather(bf16[1,258,128]{2,1,0:T(8,128)(2,1)S(1)} %maximum_bitcast_fusion.11), channel_id=5, replica_groups=mesh['sp_0'=8,'sp_1'=8,'tp'=8] {'sp_0'}, dimensions={0}, use_global_device_ids=true | all-gather | bytes 594432 | tf_op jit(solution)/shard_map/all_gather | solution.py:39
  123.3 0.6 fusion.345
  134.4 0.6 fusion.346
  145.9 23.4 %while.55 = (s32[]{:T(128)}, f32[1,128,128]{2,1,0:T(8,128)S(1)}, s32[]{:T(128)}, f32[2,1,64,128]{3,2,1,0:T(8,128)S(1)}, s32[2,64]{1,0:T(2,128)S(1)}, /*index=5*/...) while((s32[]{:T(128)}, f32[1,128,128]{2,1,0:T(8,128)S(1)}, ...), condition=%wide.region_13.16_spmd, body=%wide.region_11.15_spmd.sunk | while | flops 22245764 | bytes 946716 | solution.py:188
  146.0 0.6 slice.1381
  146.8 0.6 slice.1380
  147.5 1.3 fusion.534
  149.0 4.9 %custom-call.19 = f32[1,64,64]{1,2,0:T(8,128)S(1)} custom-call(f32[1,64,64]{2,1,0:T(8,128)S(1)} %fusion.535), custom_call_target="InvertDiagBlocksLowerTriangular" | custom-call | tf_op jit(solution)/shard_map/while/body/eval_jaxpr/jit(_solve_triangular)/triangular_solve | solution.py:135
  155.5 0.6 slice.1382
  157.7 0.6 slice.1381
  158.6 0.6 slice.1380
  159.2 1.3 fusion.534
  160.7 4.9 %custom-call.19 = f32[1,64,64]{1,2,0:T(8,128)S(1)} custom-call(f32[1,64,64]{2,1,0:T(8,128)S(1)} %fusion.535), custom_call_target="InvertDiagBlocksLowerTriangular" | custom-call | tf_op jit(solution)/shard_map/while/body/eval_jaxpr/jit(_solve_triangular)/triangular_solve | solution.py:135
  169.6 22.6 %while.52 = (s32[]{:T(128)}, f32[1,128,256]{2,1,0:T(8,128)S(1)}, s32[]{:T(128)}, s32[2,64]{1,0:T(2,128)S(1)}, f32[2,1,64]{2,1,0:T(1,128)S(1)}, /*index=5*/f32[2,...) while((s32[]{:T(128)}, f32[1,128,256]{2,1,0:T(8,128)S(1)}, ...), condition=%wide.region_3.5_spmd, body=%wide.region_1.4_spmd.sunk | while | flops 28541312 | bytes 1286924 | solution.py:188
  171.7 1.3 fusion.486
  173.2 4.9 %custom-call.16 = f32[1,64,64]{1,2,0:T(8,128)S(1)} custom-call(f32[1,64,64]{2,1,0:T(8,128)S(1)} %fusion.489), custom_call_target="InvertDiagBlocksLowerTriangular" | custom-call | tf_op jit(solution)/shard_map/while/body/eval_jaxpr/jit(_solve_triangular)/triangular_solve | solution.py:135
  179.2 0.7 slice.1367
  183.0 1.3 fusion.486
  184.5 4.9 %custom-call.16 = f32[1,64,64]{1,2,0:T(8,128)S(1)} custom-call(f32[1,64,64]{2,1,0:T(8,128)S(1)} %fusion.489), custom_call_target="InvertDiagBlocksLowerTriangular" | custom-call | tf_op jit(solution)/shard_map/while/body/eval_jaxpr/jit(_solve_triangular)/triangular_solve | solution.py:135
  190.5 0.7 slice.1367
  192.2 20.4 %all-gather.4 = bf16[8,258,128]{2,1,0:T(8,128)(2,1)S(1)} all-gather(bf16[1,258,128]{2,1,0:T(8,128)(2,1)S(1)} %maximum_bitcast_fusion.8), channel_id=2, replica_groups=mesh['sp_0'=8,'sp_1'=8,'tp'=8] {'sp_1'}, dimensions={0}, use_global_device_ids=true | all-gather | bytes 594432 | tf_op jit(solution)/shard_map/all_gather | solution.py:39
  212.7 0.6 fusion.352
  241.7 18.9 %all-gather.5 = bf16[8,258,128]{2,1,0:T(8,128)(2,1)S(1)} all-gather(bf16[1,258,128]{2,1,0:T(8,128)(2,1)S(1)} %maximum_bitcast_fusion.9), channel_id=3, replica_groups=mesh['sp_0'=8,'sp_1'=8,'tp'=8] {'sp_0'}, dimensions={0}, use_global_device_ids=true | all-gather | bytes 594432 | tf_op jit(solution)/shard_map/all_gather | solution.py:39
  260.7 0.6 fusion.349
  271.6 0.6 fusion.350
  283.0 23.1 %while.53 = (s32[]{:T(128)}, f32[1,128,128]{2,1,0:T(8,128)S(1)}, s32[]{:T(128)}, f32[2,1,64,128]{3,2,1,0:T(8,128)S(1)}, s32[2,64]{1,0:T(2,128)S(1)}, /*index=5*/...) while((s32[]{:T(128)}, f32[1,128,128]{2,1,0:T(8,128)S(1)}, ...), condition=%wide.region_7.10_spmd, body=%wide.region_5.9_spmd.sunk | while | flops 22245764 | bytes 946716 | solution.py:188
  283.8 0.6 slice.1370
  284.5 1.2 fusion.504
  286.0 4.9 %custom-call.17 = f32[1,64,64]{1,2,0:T(8,128)S(1)} custom-call(f32[1,64,64]{2,1,0:T(8,128)S(1)} %fusion.505), custom_call_target="InvertDiagBlocksLowerTriangular" | custom-call | tf_op jit(solution)/shard_map/while/body/eval_jaxpr/jit(_solve_triangular)/triangular_solve | solution.py:135
  295.4 0.6 slice.1370
  296.0 1.2 fusion.504
  297.6 4.9 %custom-call.17 = f32[1,64,64]{1,2,0:T(8,128)S(1)} custom-call(f32[1,64,64]{2,1,0:T(8,128)S(1)} %fusion.505), custom_call_target="InvertDiagBlocksLowerTriangular" | custom-call | tf_op jit(solution)/shard_map/while/body/eval_jaxpr/jit(_solve_triangular)/triangular_solve | solution.py:135
  306.5 0.9 copy.111
  307.4 25.5 %all-to-all-start = ((bf16[8,128,256]{2,1,0:T(8,128)(2,1)}), bf16[8,128,256]{2,1,0:T(8,128)(2,1)S(1)}, u32[]{:S(2)}, u32[]{:S(2)}) async-start(bf16[8,128,256]{2,1,0:T(8,128)(2,1)} %bitcast.880), calls=%async_computation | async-start | bytes 1048576 | tf_op jit(solution)/shard_map/all_to_all | solution.py:79
  332.9 9.3 %all-to-all-done = bf16[8,128,256]{2,1,0:T(8,128)(2,1)S(1)} async-done(((bf16[8,128,256]{2,1,0:T(8,128)(2,1)}), bf16[8,128,256]{2,1,0:T(8,128)(2,1)S(1)}, u32[]{:S(2)}, u32[]{:S(2)}) %all-to-all-start) | async-done | bytes 524320 | tf_op jit(solution)/shard_map/all_to_all | solution.py:79
  342.4 0.9 multiply_reduce_fusion
  343.3 0.6 broadcast_in_dim.93
  343.9 4.2 %all-to-all-start.1 = ((f32[8,1,128]{2,1,0:T(1,128)}), f32[8,1,128]{2,1,0:T(1,128)S(1)}, u32[]{:S(2)}, u32[]{:S(2)}) async-start(f32[8,1,128]{2,1,0:T(1,128)} %broadcast_in_dim.93), calls=%async_computation.1 | async-start | bytes 8192 | tf_op jit(solution)/shard_map/all_to_all | solution.py:85
  348.1 0.8 dynamic_slice.77
  348.9 3.8 all-to-all-done.1
  352.7 0.9 multiply_convert_fusion
  353.8 12.4 %all_to_all.21 = bf16[8,128,256]{1,2,0:T(8,128)(2,1)S(1)} all-to-all(bf16[8,128,256]{1,2,0:T(8,128)(2,1)S(1)} %broadcast_in_dim.94), channel_id=1, replica_groups=mesh['sp_0'=8,'sp_1'=8,'tp'=8] {'tp'}, dimensions={0} | all-to-all | bytes 1048576 | tf_op jit(solution)/shard_map/all_to_all | solution.py:85
  366.2 5.6 %fusion.180 = bf16[128,2048]{1,0:T(8,128)(2,1)S(1)} fusion(bf16[2048,2048]{1,0:T(8,128)(2,1)} %all-gather.10.cloned.1.call-done, bf16[128,2048]{0,1:T(8,128)(2,1)S(1)} %bitcast.1124), kind=kOutput, calls=%fused_computation.262 | convolution fusion | flops 1074397184 | bytes 9437184 | tf_op jit(solution)/shard_map/dot_general | solution.py:369
  371.9 12.8 %all_to_all.22 = bf16[8,128,256]{2,1,0:T(8,128)(2,1)S(1)} all-to-all(bf16[8,128,256]{2,1,0:T(8,128)(2,1)S(1)} %bitcast.1116), channel_id=1, replica_groups=mesh['sp_0'=8,'sp_1'=8,'tp'=8] {'tp'}, dimensions={0} | all-to-all | bytes 1048576 | tf_op jit(solution)/shard_map/all_to_all | solution.py:79
  384.7 1.5 add_convert_fusion
  (241 shorter events, 34.0 us)
Async XLA Ops:
  6.5 299.6 %copy-start = (bf16[128,2048]{1,0:T(8,128)(2,1)S(1)}, bf16[128,2048]{1,0:T(8,128)(2,1)}, u32[]{:S(2)}) copy-start(bf16[128,2048]{1,0:T(8,128)(2,1)} %param.36) | copy-start | bytes 1572868
  6.5 35.1 %copy-start.5 = (pred[128]{0:T(512)(128)(4,1)S(1)}, pred[128]{0:T(512)(128)(4,1)}, u32[]{:S(2)}) copy-start(pred[128]{0:T(512)(128)(4,1)} %constant.152.clone.1) | copy-start | bytes 388
  6.5 35.2 %copy-start.3 = (s32[128]{0:T(128)S(1)}, s32[128]{0:T(128)}, u32[]{:S(2)}) copy-start(s32[128]{0:T(128)} %param.34) | copy-start | bytes 1540
  6.5 116.7 %copy-start.1 = (bf16[128,128]{1,0:T(8,128)(2,1)S(1)}, bf16[128,128]{1,0:T(8,128)(2,1)}, u32[]{:S(2)}) copy-start(bf16[128,128]{1,0:T(8,128)(2,1)} %param.29) | copy-start | bytes 98308
  6.5 139.1 %copy-start.2 = (bf16[128,128]{1,0:T(8,128)(2,1)S(1)}, bf16[128,128]{1,0:T(8,128)(2,1)}, u32[]{:S(2)}) copy-start(bf16[128,128]{1,0:T(8,128)(2,1)} %param.27) | copy-start | bytes 98308
  6.5 359.7 %all-gather.10.cloned.1.call-start = ((), (), s32[]{:S(2)}) async-start(), calls=%async_computation.4 | async-start | bytes 8519680 | tf_op jit(solution)/shard_map/all_gather | solution.py:17
  169.6 136.6 %copy-start.4 = (f32[128]{0:T(128)S(1)}, f32[128]{0:T(128)}, u32[]{:S(2)}) copy-start(f32[128]{0:T(128)} %param.35) | copy-start | bytes 1540
  307.4 34.9 %all-to-all-start = ((bf16[8,128,256]{2,1,0:T(8,128)(2,1)}), bf16[8,128,256]{2,1,0:T(8,128)(2,1)S(1)}, u32[]{:S(2)}, u32[]{:S(2)}) async-start(bf16[8,128,256]{2,1,0:T(8,128)(2,1)} %bitcast.880), calls=%async_computation | async-start | bytes 1048576 | tf_op jit(solution)/shard_map/all_to_all | solution.py:79
  343.9 8.7 %all-to-all-start.1 = ((f32[8,1,128]{2,1,0:T(1,128)}), f32[8,1,128]{2,1,0:T(1,128)S(1)}, u32[]{:S(2)}, u32[]{:S(2)}) async-start(f32[8,1,128]{2,1,0:T(1,128)} %broadcast_in_dim.93), calls=%async_computation.1 | async-start | bytes 8192 | tf_op jit(solution)/shard_map/all_to_all | solution.py:85
Sparse Core Ops, SparseCore 0:
  10.4 106.8 all-gather.9
where the time goes:
time: 395 us; the launch traced here: 393 us
  blocking collectives  116 us (29%)
  between operations  104 us (26%)
  other arithmetic  64.2 us (16%)
  starting transfers between devices  29.8 us (8%)
  local copies, waits for them, and re-layouts  27.9 us (7%)
  matrix products  22 us (6%)
  loops' own time  15.9 us (4%)
  waiting for transfers between devices  13.2 us (3%)
    all_gather x4, blocking collectives, all_in_one(): both, at, found = (lax.all_gather(jnp.concatenate(lines), axis), 0, {})  91 us
    another operation x16, other arithmetic, block_pass(): jax.scipy.linalg.solve_triangular(system, right_side, lower=True, unit_di...  39.3 us
    all_to_all x1, starting transfers between devices, sent_and_summed(): parts = lax.all_to_all(split_up(array, dim, length), axis, 0, 0, tiled=True)  25.5 us
    another operation x4, loops' own time, run_blocks(): lax.scan(advance, (memory, prior_doc), (split_blocks(probe_vectors), spli...  15.9 us
    all_to_all x1, blocking collectives, sent_and_summed(): parts = lax.all_to_all(split_up(array, dim, length), axis, 0, 0, tiled=True)  12.8 us
    all_to_all x1, blocking collectives, sent_to_all(): lax.all_to_all(jnp.broadcast_to(array[None], (length, *array.shape)), axi...  12.4 us
    mul x8, other arithmetic, block_pass(): jnp.exp(running[:, -1:] - running) * ending  10.1 us
    slice x16, local copies, waits for them, and re-layouts, block_pass(): kept_share = jnp.exp(running[:, -1]) * linked[-1]  9.66 us
  transfers between devices with their start and end apart: 3, of which 2 were waited for; matrix products, arithmetic and copies ran while one was open for 27% of the time, Pallas kernels for 0%

commit v1 on v0

v1 whole, which is shorter than its diff:
```python
import jax
import jax.numpy as jnp
from jax import lax
from jax.experimental import pallas as pl
from jax.experimental.pallas import tpu as pltpu
from jax.sharding import Mesh
from jax.sharding import PartitionSpec as P

SP = ("sp_0", "sp_1")
EPSILON = 1e-06
F32 = jnp.float32
BF16 = jnp.bfloat16
NT = (((1,), (1,)), ((), ()))
NN = (((1,), (0,)), ((), ()))


def mm(a, b, dims=NN):
    return lax.dot_general(a.astype(BF16), b.astype(BF16), dims, preferred_element_type=F32)


def split_in_two(a):
    high = a.astype(BF16)
    return high, (a - high.astype(F32)).astype(BF16)


def mm2(a, b, dims=NN):
    high, low = split_in_two(a)
    return mm(high, b, dims) + mm(low, b, dims)


def mm3(a, b):
    a_high, a_low = split_in_two(a)
    b_high, b_low = split_in_two(b)
    return mm(a_high, b_high) + (mm(a_high, b_low) + mm(a_low, b_high))


def local_kernel(
    q_ref, k_ref, v_ref, gates_ref, speed_ref, docs_ref, fwd_ref, bwd_ref, read_ref, own_ref
):
    n, width = q_ref.shape
    q, k, v = q_ref[...], k_ref[...], v_ref[...]
    rows = lax.broadcasted_iota(jnp.int32, (n, n), 0)
    cols = lax.broadcasted_iota(jnp.int32, (n, n), 1)
    eye = rows == cols

    def to_col(row):
        return jnp.sum(jnp.where(eye, row, 0.0), axis=1, keepdims=True)

    def to_row(col):
        return jnp.sum(jnp.where(eye, col, 0.0), axis=0, keepdims=True)

    gates = gates_ref[...]
    betas = jax.nn.sigmoid(gates[0:2])
    preacts = gates[2:4]
    soft = jnp.maximum(preacts, 0.0) + jnp.log1p(jnp.exp(-jnp.abs(preacts)))
    decays = -jnp.exp(speed_ref[...]) * soft + gates[4:6]
    docs_row = docs_ref[...].astype(F32)
    docs_col = to_col(docs_row)
    shared = docs_col == docs_row
    qf, kf = q.astype(F32), k.astype(F32)
    q_scale = lax.rsqrt(jnp.sum(qf * qf, axis=1, keepdims=True) + EPSILON) * width ** (-0.5)
    k_scale = lax.rsqrt(jnp.sum(kf * kf, axis=1, keepdims=True) + EPSILON)
    k_scale_row = to_row(k_scale)
    similar = mm(k, k, NT) * k_scale * k_scale_row
    scored = mm(q, k, NT) * q_scale * k_scale_row
    k_turned = jnp.transpose(kf)
    near = [((rows ^ cols) >> lg) == 1 for lg in range(7)]
    outputs = 0.0
    for way, message_ref in ((0, fwd_ref), (1, bwd_ref)):
        first, last = (0, n - 1) if way == 0 else (n - 1, 0)
        reach = (rows >= cols) if way == 0 else (rows <= cols)
        decay_row = decays[way : way + 1]
        beta_row = betas[way : way + 1]
        running = jnp.sum(jnp.where(reach, decay_row, 0.0), axis=1, keepdims=True)
        running_row = to_row(running)
        within = reach & shared
        spread = jnp.exp(jnp.where(within, running - running_row, -jnp.inf))
        strict = jnp.where(eye, 0.0, similar * spread * to_col(beta_row))
        inverse = jnp.where(eye, 1.0, 0.0) - jnp.where(near[0], strict, 0.0)
        for lg in range(1, 7):
            inverse = inverse - mm3(inverse, mm3(jnp.where(near[lg], strict, 0.0), inverse))
        linked_row = (docs_row == docs_row[:, first : first + 1]).astype(F32)
        linked = (docs_col == docs_col[first : first + 1]).astype(F32)
        ending_row = (docs_row == docs_row[:, last : last + 1]).astype(F32)
        total = running_row[:, last : last + 1]
        update = mm2(inverse * beta_row, v)
        mask = inverse * (beta_row * jnp.exp(running_row) * linked_row * k_scale_row)
        drop = mm2(mask, k)
        faded = k_turned * (k_scale_row * jnp.exp(total - running_row) * ending_row)
        kept = jnp.exp(total) * linked_row[:, last : last + 1]
        message_ref[:, :width] = jnp.where(eye, kept, 0.0) - mm(faded, drop)
        message_ref[:, width:] = mm(faded, update)
        scores = scored * spread
        queries = qf * (q_scale * jnp.exp(running) * linked)
        read_ref[way] = (queries - mm(scores, drop)).astype(BF16)
        outputs = outputs + mm(scores, update)
    own_ref[...] = outputs


def combine_kernel(fwd_ref, fwd_in_ref, bwd_ref, bwd_in_ref, fwd_out_ref, bwd_out_ref):
    for own_ref, in_ref, out_ref in (
        (fwd_ref, fwd_in_ref, fwd_out_ref),
        (bwd_ref, bwd_in_ref, bwd_out_ref),
    ):
        n = own_ref.shape[0]
        moved = mm(own_ref[:, :n], in_ref[...])
        out_ref[:, :n] = moved[:, :n].astype(BF16)
        out_ref[:, n:] = (moved[:, n:] + own_ref[:, n:].astype(F32)).astype(BF16)


def finish_kernel(
    own_ref, read_ref, fwd_ref, fwd_far_ref, bwd_ref, bwd_far_ref, links_ref, gain_ref, exit_ref, out_ref
):
    n = own_ref.shape[0]
    attn = own_ref[...]
    for way, near_ref, far_ref in ((0, fwd_ref, fwd_far_ref), (1, bwd_ref, bwd_far_ref)):
        state = mm(near_ref[:, :n], far_ref[...]) + near_ref[:, n:].astype(F32)
        attn = attn + mm(read_ref[way], state * links_ref[way : way + 1])
    mean = jnp.mean(attn * attn, axis=1, keepdims=True)
    mixed = (attn * lax.rsqrt(mean + EPSILON) * gain_ref[...]).astype(BF16)
    terms = mm(mixed, exit_ref[...]).astype(BF16)
    step = out_ref.shape[2]
    for m in range(out_ref.shape[0]):
        out_ref[m] = terms[:, m * step : (m + 1) * step]


def vmem(count):
    return [pl.BlockSpec(memory_space=pltpu.VMEM)] * count


def shards(
    skip_path_inputs,
    probe_vectors,
    lookup_vectors,
    payload_vectors,
    learning_strength_preacts,
    forget_preacts,
    forgetting_speed_exponent,
    extra_forgetting_spikes,
    sample_membership,
    channel_group_scaling,
    blend_exit_weights,
    dense_block_scaling,
    widen_projection_weights,
    shrink_projection_weights,
):
    up_width = widen_projection_weights.shape[1]
    weights = lax.all_gather(
        jnp.concatenate([widen_projection_weights, shrink_projection_weights.T], axis=1),
        SP,
        axis=0,
        tiled=True,
    )
    length, width = probe_vectors.shape
    count = lax.axis_size(SP)

    def passed(array, distance):
        pairs = [(i, (i + distance) % count) for i in range(count)]
        return lax.ppermute(array, SP, pairs)

    docs = sample_membership.reshape(1, length)
    prior = passed(docs, 1)
    later = passed(docs, -1)
    gates = jnp.concatenate(
        [
            learning_strength_preacts.reshape(2, length),
            forget_preacts.reshape(2, length),
            extra_forgetting_spikes.reshape(2, length),
        ]
    )
    square = (width, width)
    pair = (width, 2 * width)
    fwd, bwd, read, own = pl.pallas_call(
        local_kernel,
        out_shape=(
            jax.ShapeDtypeStruct(pair, F32),
            jax.ShapeDtypeStruct(pair, F32),
            jax.ShapeDtypeStruct((2, length, width), BF16),
            jax.ShapeDtypeStruct((length, width), F32),
        ),
        in_specs=vmem(6),
        out_specs=tuple(vmem(4)),
        name="local_maps",
    )(
        probe_vectors,
        lookup_vectors,
        payload_vectors,
        gates,
        forgetting_speed_exponent,
        docs,
    )
    fwd_link = (prior[0, length - 1] == docs[0, 0]).astype(F32)
    bwd_link = (later[0, 0] == docs[0, length - 1]).astype(F32)
    is_map = lax.broadcasted_iota(jnp.int32, pair, 1) < width
    fwd = (fwd * jnp.where(is_map, fwd_link, 1.0)).astype(BF16)
    bwd = (bwd * jnp.where(is_map, bwd_link, 1.0)).astype(BF16)
    links = jnp.broadcast_to(jnp.stack([fwd_link, bwd_link])[:, None], (2, width))
    for distance in (1, 2):
        fwd, bwd = pl.pallas_call(
            combine_kernel,
            out_shape=(jax.ShapeDtypeStruct(pair, BF16),) * 2,
            in_specs=vmem(4),
            out_specs=tuple(vmem(2)),
            name="combine_maps",
        )(fwd, passed(fwd, distance), bwd, passed(bwd, -distance))
    head_terms = pl.pallas_call(
        finish_kernel,
        out_shape=jax.ShapeDtypeStruct((8, length, blend_exit_weights.shape[1] // 8), BF16),
        in_specs=vmem(9),
        out_specs=vmem(1)[0],
        name="finish_mixer",
    )(
        own,
        read,
        passed(fwd, 1),
        passed(fwd[:, width:], 5),
        passed(bwd, -1),
        passed(bwd[:, width:], -5),
        links,
        channel_group_scaling.reshape(1, width),
        blend_exit_weights,
    )
    model_width = skip_path_inputs.shape[1]
    col_count = model_width // lax.axis_size("tp")
    col_start = lax.axis_index("tp") * col_count
    parts = lax.all_to_all(head_terms, "tp", 0, 0, tiled=True)
    own_residual = lax.dynamic_slice_in_dim(skip_path_inputs, col_start, col_count, 1).astype(
        F32
    ) + jnp.sum(parts.astype(F32), axis=0)
    residual = lax.all_gather(own_residual.astype(BF16), "tp", axis=1, tiled=True).astype(F32)
    squares = jnp.mean(residual * residual, axis=1, keepdims=True)
    normed = (residual * lax.rsqrt(squares + EPSILON) * dense_block_scaling).astype(BF16)
    raised = jnp.dot(normed, weights[:, :up_width], preferred_element_type=F32)
    active = jnp.square(jax.nn.relu(raised)).astype(BF16)
    lowered = lax.dot_general(active, weights[:, up_width:], NT, preferred_element_type=F32)
    turned = jnp.moveaxis(lowered.astype(BF16).reshape(length, -1, col_count), 1, 0)
    pieces = lax.all_to_all(turned, "tp", 0, 0, tiled=True)
    return (own_residual + jnp.sum(pieces.astype(F32), axis=0)).astype(BF16)


def solution(mesh):
    torus = Mesh(mesh.devices.reshape(8, 8, mesh.shape["tp"]), ("sp_0", "sp_1", "tp"))
    placed = (
        P(SP, None),
        P(SP, "tp"),
        P(SP, "tp"),
        P(SP, "tp"),
        P(None, SP, "tp"),
        P(None, SP, "tp"),
        P(None, "tp"),
        P(None, SP, "tp"),
        P(SP),
        P(),
        P("tp", None),
        P(),
        P(SP, "tp"),
        P("tp", SP),
    )
    return jax.shard_map(
        shards, mesh=torus, in_specs=placed, out_specs=P(SP, "tp"), check_vma=False
    )
```

time: 395 us -> 159 us (0.40)
  the two profiles are of different devices: /device:TPU:1 before, /device:TPU:24 now
where the time goes in v1:
time: 159 us; the launch traced here: 158 us
  starting transfers between devices  59.4 us (37%)
  blocking collectives  26 us (16%)
  waiting for transfers between devices  24.8 us (16%)
  between operations  15.5 us (10%)
  Pallas kernels  12.6 us (8%)
  other arithmetic  7.45 us (5%)
  local copies, waits for them, and re-layouts  6.67 us (4%)
  matrix products  5.62 us (4%)
    ppermute x10, starting transfers between devices, passed(): return lax.ppermute(array, SP, pairs)  55.1 us
    ppermute x10, waiting for transfers between devices, passed(): return lax.ppermute(array, SP, pairs)  14.4 us
    all_gather x1, blocking collectives, shards(): lax.all_gather(own_residual.astype(BF16), 'tp', axis=1, tiled=True)  13.1 us
    all_to_all x1, blocking collectives, shards(): pieces = lax.all_to_all(turned, 'tp', 0, 0, tiled=True)  12.9 us
    all_to_all x1, waiting for transfers between devices, shards(): parts = lax.all_to_all(head_terms, 'tp', 0, 0, tiled=True)  10.3 us
    pallas_call x1, Pallas kernels, shards(): pl.pallas_call(local_kernel, out_shape=(jax.ShapeDtypeStruct(pair, F32),...  6.32 us
    dot_general x1, matrix products, shards(): lax.dot_general(active, weights[:, up_width:], NT, preferred_element_type...  5.62 us
    all_to_all x1, starting transfers between devices, shards(): parts = lax.all_to_all(head_terms, 'tp', 0, 0, tiled=True)  4.29 us
  transfers between devices with their start and end apart: 12, of which 6 were waited for; matrix products, arithmetic and copies ran while one was open for 6% of the time, Pallas kernels for 8%

profile of v1, /device:TPU:24, one launch (start us, length us, event | category | flops | bytes accessed | tf_op | source)
XLA Modules:
  0.0 158.0 jit_solution(16601894456295666487)
XLA Ops:
  6.5 0.0 all-gather.2.cloned.1.call-start
  6.5 1.5 pad_maximum_fusion
  8.1 0.0 all-gather.2.cloned.1.call-update
  8.1 2.4 %collective-permute-start.2 = (s32[1,128]{1,0:T(1,128)}, s32[1,128]{1,0:T(1,128)S(1)}, u32[]{:S(2)}, u32[]{:S(2)}) collective-permute-start(s32[1,128]{1,0:T(1,128)} %bitcast.21), channel_id=1, source_target_pairs={{0,504},{8,0},{16,8},{24,16},{32,24},{40,32},{48,40},{56,48},{64,5... | collective-permute-start | bytes 1544 | tf_op jit(solution)/shard_map/ppermute | solution.py:159
  10.5 4.7 %collective-permute-start = (s32[1,128]{1,0:T(1,128)}, s32[1,128]{1,0:T(1,128)S(1)}, u32[]{:S(2)}, u32[]{:S(2)}) collective-permute-start(s32[1,128]{1,0:T(1,128)} %bitcast.22), channel_id=1, source_target_pairs={{0,8},{8,16},{16,24},{24,32},{32,40},{40,48},{48,56},{56,64},{64,7... | collective-permute-start | bytes 1544 | tf_op jit(solution)/shard_map/ppermute | solution.py:159
  15.2 1.4 fusion.32
  16.5 1.3 pad_maximum_fusion.1.gates_ref
  17.8 1.3 copy.16.speed_ref
  19.1 6.3 %local_maps.1 = (f32[128,256]{1,0:T(8,128)}, f32[128,256]{1,0:T(8,128)}, bf16[2,128,128]{2,1,0:T(8,128)(2,1)}, f32[128,128]{1,0:T(8,128)}) custom-call(bf16[128,128]{1,0:T(8,128)(2,1)} %q_ref.1, bf16[128,128]{1,0:T(8,128)(2,1)} %k_ref.1, bf16[128,128]{1,0:T(8,128)(2,1)} %v_ref.1, f32[6,128]{1,0:T(8,128)} %pad_maximum_fusion.1.gates_ref, ...), custom_call_target="tpu_custom_call" | custom-call | tf_op jit(solution)/shard_map/local_maps/pallas_call | solution.py:173
  25.4 0.0 collective-permute-done.2
  26.2 0.0 collective-permute-done
  26.2 0.6 slice.24
  27.9 0.9 multiply_convert_fusion.bwd_ref
  28.8 0.0 copy-start
  28.8 1.9 %collective-permute-start.3 = (bf16[128,256]{1,0:T(8,128)(2,1)S(1)}, bf16[128,256]{1,0:T(8,128)(2,1)S(1)}, u32[]{:S(2)}, u32[]{:S(2)}) collective-permute-start(bf16[128,256]{1,0:T(8,128)(2,1)S(1)} %multiply_convert_fusion.bwd_ref), channel_id=1, source_target_pairs={{0,504},{8,0},{16,8},{24,16},{32,24},{40,32},{48,40},{56,48},{64,5... | collective-permute-start | bytes 196616 | tf_op jit(solution)/shard_map/ppermute | solution.py:159
  30.8 0.9 multiply_convert_fusion.1.fwd_ref
  31.7 0.0 copy-start.1
  31.7 5.1 %collective-permute-start.1 = (bf16[128,256]{1,0:T(8,128)(2,1)S(1)}, bf16[128,256]{1,0:T(8,128)(2,1)S(1)}, u32[]{:S(2)}, u32[]{:S(2)}) collective-permute-start(bf16[128,256]{1,0:T(8,128)(2,1)S(1)} %multiply_convert_fusion.1.fwd_ref), channel_id=1, source_target_pairs={{0,8},{8,16},{16,24},{24,32},{32,40},{40,48},{48,56},{56,64},{64,7... | collective-permute-start | bytes 196616 | tf_op jit(solution)/shard_map/ppermute | solution.py:159
  36.9 0.0 collective-permute-done.3.bwd_in_ref
  36.9 0.0 copy-start.4
  36.9 2.5 %collective-permute-done.1.fwd_in_ref = bf16[128,256]{1,0:T(8,128)(2,1)S(1)} collective-permute-done((bf16[128,256]{1,0:T(8,128)(2,1)S(1)}, bf16[128,256]{1,0:T(8,128)(2,1)S(1)}, u32[]{:S(2)}, u32[]{:S(2)}) %collective-permute-start.1) | collective-permute-done | bytes 65568 | tf_op jit(solution)/shard_map/ppermute | solution.py:159
  39.3 0.0 copy-done
  39.3 0.0 copy-done.1
  39.3 0.0 copy-done.4
  39.3 0.0 copy-start.6
  39.4 0.6 copy-done.6
  40.0 1.8 %combine_maps.2 = (bf16[128,256]{1,0:T(8,128)(2,1)}, bf16[128,256]{1,0:T(8,128)(2,1)}) custom-call(bf16[128,256]{1,0:T(8,128)(2,1)} %copy-done.1, bf16[128,256]{1,0:T(8,128)(2,1)} %copy-done.6, bf16[128,256]{1,0:T(8,128)(2,1)} %copy-done, bf16[128,256]{1,0:T(8,128)(2,1)} %copy-done.4), custom_call_target="tpu_custom_call" | custom-call | tf_op jit(solution)/shard_map/combine_maps/pallas_call | solution.py:199
  41.7 3.8 %collective-permute-start.4 = (bf16[128,256]{1,0:T(8,128)(2,1)}, bf16[128,256]{1,0:T(8,128)(2,1)S(1)}, u32[]{:S(2)}, u32[]{:S(2)}) collective-permute-start(bf16[128,256]{1,0:T(8,128)(2,1)} %get-tuple-element.17.fwd_ref), channel_id=1, source_target_pairs={{0,16},{8,24},{16,32},{24,40},{32,48},{40,56},{48,64},{56,72},{64,... | collective-permute-start | bytes 196616 | tf_op jit(solution)/shard_map/ppermute | solution.py:159
  45.6 12.2 %collective-permute-start.5 = (bf16[128,256]{1,0:T(8,128)(2,1)}, bf16[128,256]{1,0:T(8,128)(2,1)S(1)}, u32[]{:S(2)}, u32[]{:S(2)}) collective-permute-start(bf16[128,256]{1,0:T(8,128)(2,1)} %get-tuple-element.18.bwd_ref), channel_id=1, source_target_pairs={{0,496},{8,504},{16,0},{24,8},{32,16},{40,24},{48,32},{56,40},{64,... | collective-permute-start | bytes 196616 | tf_op jit(solution)/shard_map/ppermute | solution.py:159
  57.8 0.5 collective-permute-done.4.fwd_in_ref
  58.3 0.0 copy-start.5
  58.3 1.7 %collective-permute-done.5.bwd_in_ref = bf16[128,256]{1,0:T(8,128)(2,1)S(1)} collective-permute-done((bf16[128,256]{1,0:T(8,128)(2,1)}, bf16[128,256]{1,0:T(8,128)(2,1)S(1)}, u32[]{:S(2)}, u32[]{:S(2)}) %collective-permute-start.5) | collective-permute-done | bytes 65568 | tf_op jit(solution)/shard_map/ppermute | solution.py:159
  60.0 0.0 copy-done.5
  60.0 0.6 copy-done.7
  60.6 1.8 %combine_maps.3 = (bf16[128,256]{1,0:T(8,128)(2,1)}, bf16[128,256]{1,0:T(8,128)(2,1)}) custom-call(bf16[128,256]{1,0:T(8,128)(2,1)} %get-tuple-element.17.fwd_ref, bf16[128,256]{1,0:T(8,128)(2,1)} %copy-done.5, bf16[128,256]{1,0:T(8,128)(2,1)} %get-tuple-element.18.bwd_ref, bf16[128,256]{1,0:T(8,128)(2,1)} %copy-done.7), custom_call_target="tpu_custom_call" | custom-call | tf_op jit(solution)/shard_map/combine_maps/pallas_call | solution.py:199
  62.4 0.8 slice.28
  63.2 1.9 %collective-permute-start.6 = (bf16[128,256]{1,0:T(8,128)(2,1)}, bf16[128,256]{1,0:T(8,128)(2,1)S(1)}, u32[]{:S(2)}, u32[]{:S(2)}) collective-permute-start(bf16[128,256]{1,0:T(8,128)(2,1)} %get-tuple-element.19), channel_id=1, source_target_pairs={{0,8},{8,16},{16,24},{24,32},{32,40},{40,48},{48,56},{56,64},{64,7... | collective-permute-start | bytes 196616 | tf_op jit(solution)/shard_map/ppermute | solution.py:159
  65.1 0.8 slice.29
  65.8 6.5 %collective-permute-start.8 = (bf16[128,256]{1,0:T(8,128)(2,1)}, bf16[128,256]{1,0:T(8,128)(2,1)S(1)}, u32[]{:S(2)}, u32[]{:S(2)}) collective-permute-start(bf16[128,256]{1,0:T(8,128)(2,1)} %get-tuple-element.20), channel_id=1, source_target_pairs={{0,504},{8,0},{16,8},{24,16},{32,24},{40,32},{48,40},{56,48},{64,5... | collective-permute-start | bytes 196616 | tf_op jit(solution)/shard_map/ppermute | solution.py:159
  72.4 14.6 %collective-permute-start.9 = (bf16[128,128]{1,0:T(8,128)(2,1)S(1)}, bf16[128,128]{1,0:T(8,128)(2,1)S(1)}, u32[]{:S(2)}, u32[]{:S(2)}) collective-permute-start(bf16[128,128]{1,0:T(8,128)(2,1)S(1)} %slice.29), channel_id=1, source_target_pairs={{0,472},{8,480},{16,488},{24,496},{32,504},{40,0},{48,8},{56,16},{... | collective-permute-start | bytes 98312 | tf_op jit(solution)/shard_map/ppermute | solution.py:159
  87.0 1.9 %collective-permute-start.7 = (bf16[128,128]{1,0:T(8,128)(2,1)S(1)}, bf16[128,128]{1,0:T(8,128)(2,1)S(1)}, u32[]{:S(2)}, u32[]{:S(2)}) collective-permute-start(bf16[128,128]{1,0:T(8,128)(2,1)S(1)} %slice.28), channel_id=1, source_target_pairs={{0,40},{8,48},{16,56},{24,64},{32,72},{40,80},{48,88},{56,96},{64,... | collective-permute-start | bytes 98312 | tf_op jit(solution)/shard_map/ppermute | solution.py:159
  88.9 0.1 pad_maximum_fusion.2
  89.0 0.1 collective-permute-done.9.bwd_far_ref
  89.1 9.6 %collective-permute-done.7.fwd_far_ref = bf16[128,128]{1,0:T(8,128)(2,1)S(1)} collective-permute-done((bf16[128,128]{1,0:T(8,128)(2,1)S(1)}, bf16[128,128]{1,0:T(8,128)(2,1)S(1)}, u32[]{:S(2)}, u32[]{:S(2)}) %collective-permute-start.7) | collective-permute-done | bytes 32800 | tf_op jit(solution)/shard_map/ppermute | solution.py:159
  98.7 0.0 collective-permute-done.6.fwd_ref
  98.7 0.0 collective-permute-done.8.bwd_ref
  98.7 0.0 copy-start.3
  98.8 0.6 broadcast_in_dim.23.links_ref
  99.4 0.0 copy-done.8
  99.4 0.0 copy-done.9
  99.4 0.0 copy-done.2
  99.4 0.0 copy-done.3
  99.4 2.7 %finish_mixer.1 = bf16[8,128,256]{2,1,0:T(8,128)(2,1)} custom-call(f32[128,128]{1,0:T(8,128)} %get-tuple-element.13.own_ref, bf16[2,128,128]{2,1,0:T(8,128)(2,1)} %get-tuple-element.14.read_ref, bf16[128,256]{1,0:T(8,128)(2,1)} %copy-done.2, bf16[128,128]{1,0:T(8,128)(2,1)} %copy-done.9, bf16[128,256]{1,0:T(8,128)(2,1)} %copy-done.3, ...), custom_call_target="tpu_custom_call" | custom-call | tf_op jit(solution)/shard_map/finish_mixer/pallas_call | solution.py:206
  102.2 4.3 %all-to-all-start = ((bf16[8,128,256]{2,1,0:T(8,128)(2,1)}), bf16[8,128,256]{2,1,0:T(8,128)(2,1)S(1)}, u32[]{:S(2)}, u32[]{:S(2)}) async-start(bf16[8,128,256]{2,1,0:T(8,128)(2,1)} %finish_mixer.1), calls=%async_computation | async-start | bytes 1048576 | tf_op jit(solution)/shard_map/all_to_all | solution.py:226
  106.5 10.3 %all-to-all-done = bf16[8,128,256]{2,1,0:T(8,128)(2,1)S(1)} async-done(((bf16[8,128,256]{2,1,0:T(8,128)(2,1)}), bf16[8,128,256]{2,1,0:T(8,128)(2,1)S(1)}, u32[]{:S(2)}, u32[]{:S(2)}) %all-to-all-start) | async-done | bytes 524320 | tf_op jit(solution)/shard_map/all_to_all | solution.py:226
  116.8 0.1 convert_reduce_fusion.1
  116.8 0.9 fusion.28
  117.7 13.1 %all_gather.6 = bf16[128,2048]{1,0:T(8,128)(2,1)S(1)} all-gather(bf16[128,256]{1,0:T(8,128)(2,1)S(1)} %fusion.28), channel_id=1, replica_groups=mesh['sp_0'=8,'sp_1'=8,'tp'=8] {'tp'}, dimensions={1}, use_global_device_ids=true | all-gather | bytes 589824 | tf_op jit(solution)/shard_map/all_gather | solution.py:230
  130.8 0.2 fusion.18
  131.0 0.0 all-gather.2.cloned.1.call-done
  131.0 5.6 %fusion.4 = bf16[128,2048]{1,0:T(8,128)(2,1)S(1)} fusion(bf16[2048,2048]{1,0:T(8,128)(2,1)} %all-gather.2.cloned.1.call-done, bf16[128,2048]{1,0:T(8,128)(2,1)S(1)} %all_gather.6, f32[2048]{0:T(1024)} %param.25, f32[128]{0:T(128)S(1)} %add_rsqrt_fusion), kind=kOutput, calls=%fused_computation.4 | convolution fusion | flops 1075445760 | bytes 9445888 | tf_op jit(solution)/shard_map/dot_general | solution.py:235
  136.7 12.9 %all_to_all.10 = bf16[8,128,256]{2,1,0:T(8,128)(2,1)S(1)} all-to-all(bf16[8,128,256]{2,1,0:T(8,128)(2,1)S(1)} %bitcast.18), channel_id=1, replica_groups=mesh['sp_0'=8,'sp_1'=8,'tp'=8] {'tp'}, dimensions={0} | all-to-all | bytes 1048576 | tf_op jit(solution)/shard_map/all_to_all | solution.py:237
  149.6 0.1 convert_reduce_fusion
  149.7 1.5 add_convert_fusion
  (8 shorter events, 0.1 us)
Async XLA Ops:
  6.5 124.5 %all-gather.2.cloned.1.call-start = ((), (), s32[]{:S(2)}) async-start(), calls=%async_computation.2 | async-start | bytes 8519680 | tf_op jit(solution)/shard_map/all_gather | solution.py:148
  8.1 17.3 %collective-permute-start.2 = (s32[1,128]{1,0:T(1,128)}, s32[1,128]{1,0:T(1,128)S(1)}, u32[]{:S(2)}, u32[]{:S(2)}) collective-permute-start(s32[1,128]{1,0:T(1,128)} %bitcast.21), channel_id=1, source_target_pairs={{0,504},{8,0},{16,8},{24,16},{32,24},{40,32},{48,40},{56,48},{64,5... | collective-permute-start | bytes 1544 | tf_op jit(solution)/shard_map/ppermute | solution.py:159
  10.5 15.7 %collective-permute-start = (s32[1,128]{1,0:T(1,128)}, s32[1,128]{1,0:T(1,128)S(1)}, u32[]{:S(2)}, u32[]{:S(2)}) collective-permute-start(s32[1,128]{1,0:T(1,128)} %bitcast.22), channel_id=1, source_target_pairs={{0,8},{8,16},{16,24},{24,32},{32,40},{40,48},{48,56},{56,64},{64,7... | collective-permute-start | bytes 1544 | tf_op jit(solution)/shard_map/ppermute | solution.py:159
  28.8 10.5 %copy-start = (bf16[128,256]{1,0:T(8,128)(2,1)}, bf16[128,256]{1,0:T(8,128)(2,1)S(1)}, u32[]{:S(2)}) copy-start(bf16[128,256]{1,0:T(8,128)(2,1)S(1)} %multiply_convert_fusion.bwd_ref) | copy-start | bytes 196612
  28.8 8.0 %collective-permute-start.3 = (bf16[128,256]{1,0:T(8,128)(2,1)S(1)}, bf16[128,256]{1,0:T(8,128)(2,1)S(1)}, u32[]{:S(2)}, u32[]{:S(2)}) collective-permute-start(bf16[128,256]{1,0:T(8,128)(2,1)S(1)} %multiply_convert_fusion.bwd_ref), channel_id=1, source_target_pairs={{0,504},{8,0},{16,8},{24,16},{32,24},{40,32},{48,40},{56,48},{64,5... | collective-permute-start | bytes 196616 | tf_op jit(solution)/shard_map/ppermute | solution.py:159
  31.7 7.6 %copy-start.1 = (bf16[128,256]{1,0:T(8,128)(2,1)}, bf16[128,256]{1,0:T(8,128)(2,1)S(1)}, u32[]{:S(2)}) copy-start(bf16[128,256]{1,0:T(8,128)(2,1)S(1)} %multiply_convert_fusion.1.fwd_ref) | copy-start | bytes 196612
  31.7 7.6 %collective-permute-start.1 = (bf16[128,256]{1,0:T(8,128)(2,1)S(1)}, bf16[128,256]{1,0:T(8,128)(2,1)S(1)}, u32[]{:S(2)}, u32[]{:S(2)}) collective-permute-start(bf16[128,256]{1,0:T(8,128)(2,1)S(1)} %multiply_convert_fusion.1.fwd_ref), channel_id=1, source_target_pairs={{0,8},{8,16},{16,24},{24,32},{32,40},{40,48},{48,56},{56,64},{64,7... | collective-permute-start | bytes 196616 | tf_op jit(solution)/shard_map/ppermute | solution.py:159
  36.9 2.5 %copy-start.4 = (bf16[128,256]{1,0:T(8,128)(2,1)}, bf16[128,256]{1,0:T(8,128)(2,1)S(1)}, u32[]{:S(2)}) copy-start(bf16[128,256]{1,0:T(8,128)(2,1)S(1)} %collective-permute-done.3.bwd_in_ref) | copy-start | bytes 196612
  39.3 0.6 copy-start.6
  41.7 16.6 %collective-permute-start.4 = (bf16[128,256]{1,0:T(8,128)(2,1)}, bf16[128,256]{1,0:T(8,128)(2,1)S(1)}, u32[]{:S(2)}, u32[]{:S(2)}) collective-permute-start(bf16[128,256]{1,0:T(8,128)(2,1)} %get-tuple-element.17.fwd_ref), channel_id=1, source_target_pairs={{0,16},{8,24},{16,32},{24,40},{32,48},{40,56},{48,64},{56,72},{64,... | collective-permute-start | bytes 196616 | tf_op jit(solution)/shard_map/ppermute | solution.py:159
  45.6 14.5 %collective-permute-start.5 = (bf16[128,256]{1,0:T(8,128)(2,1)}, bf16[128,256]{1,0:T(8,128)(2,1)S(1)}, u32[]{:S(2)}, u32[]{:S(2)}) collective-permute-start(bf16[128,256]{1,0:T(8,128)(2,1)} %get-tuple-element.18.bwd_ref), channel_id=1, source_target_pairs={{0,496},{8,504},{16,0},{24,8},{32,16},{40,24},{48,32},{56,40},{64,... | collective-permute-start | bytes 196616 | tf_op jit(solution)/shard_map/ppermute | solution.py:159
  58.3 1.7 %copy-start.5 = (bf16[128,256]{1,0:T(8,128)(2,1)}, bf16[128,256]{1,0:T(8,128)(2,1)S(1)}, u32[]{:S(2)}) copy-start(bf16[128,256]{1,0:T(8,128)(2,1)S(1)} %collective-permute-done.4.fwd_in_ref) | copy-start | bytes 196612
  60.0 0.6 copy-start.7
  63.2 35.6 %collective-permute-start.6 = (bf16[128,256]{1,0:T(8,128)(2,1)}, bf16[128,256]{1,0:T(8,128)(2,1)S(1)}, u32[]{:S(2)}, u32[]{:S(2)}) collective-permute-start(bf16[128,256]{1,0:T(8,128)(2,1)} %get-tuple-element.19), channel_id=1, source_target_pairs={{0,8},{8,16},{16,24},{24,32},{32,40},{40,48},{48,56},{56,64},{64,7... | collective-permute-start | bytes 196616 | tf_op jit(solution)/shard_map/ppermute | solution.py:159
  65.8 32.9 %collective-permute-start.8 = (bf16[128,256]{1,0:T(8,128)(2,1)}, bf16[128,256]{1,0:T(8,128)(2,1)S(1)}, u32[]{:S(2)}, u32[]{:S(2)}) collective-permute-start(bf16[128,256]{1,0:T(8,128)(2,1)} %get-tuple-element.20), channel_id=1, source_target_pairs={{0,504},{8,0},{16,8},{24,16},{32,24},{40,32},{48,40},{56,48},{64,5... | collective-permute-start | bytes 196616 | tf_op jit(solution)/shard_map/ppermute | solution.py:159
  72.4 16.7 %collective-permute-start.9 = (bf16[128,128]{1,0:T(8,128)(2,1)S(1)}, bf16[128,128]{1,0:T(8,128)(2,1)S(1)}, u32[]{:S(2)}, u32[]{:S(2)}) collective-permute-start(bf16[128,128]{1,0:T(8,128)(2,1)S(1)} %slice.29), channel_id=1, source_target_pairs={{0,472},{8,480},{16,488},{24,496},{32,504},{40,0},{48,8},{56,16},{... | collective-permute-start | bytes 98312 | tf_op jit(solution)/shard_map/ppermute | solution.py:159
  87.0 11.8 %collective-permute-start.7 = (bf16[128,128]{1,0:T(8,128)(2,1)S(1)}, bf16[128,128]{1,0:T(8,128)(2,1)S(1)}, u32[]{:S(2)}, u32[]{:S(2)}) collective-permute-start(bf16[128,128]{1,0:T(8,128)(2,1)S(1)} %slice.28), channel_id=1, source_target_pairs={{0,40},{8,48},{16,56},{24,64},{32,72},{40,80},{48,88},{56,96},{64,... | collective-permute-start | bytes 98312 | tf_op jit(solution)/shard_map/ppermute | solution.py:159
  89.1 10.3 %copy-start.8 = (bf16[128,128]{1,0:T(8,128)(2,1)}, bf16[128,128]{1,0:T(8,128)(2,1)S(1)}, u32[]{:S(2)}) copy-start(bf16[128,128]{1,0:T(8,128)(2,1)S(1)} %collective-permute-done.9.bwd_far_ref) | copy-start | bytes 98308
  98.7 0.7 copy-start.9
  98.7 0.7 copy-start.2
  98.7 0.7 copy-start.3
  102.2 14.6 %all-to-all-start = ((bf16[8,128,256]{2,1,0:T(8,128)(2,1)}), bf16[8,128,256]{2,1,0:T(8,128)(2,1)S(1)}, u32[]{:S(2)}, u32[]{:S(2)}) async-start(bf16[8,128,256]{2,1,0:T(8,128)(2,1)} %finish_mixer.1), calls=%async_computation | async-start | bytes 1048576 | tf_op jit(solution)/shard_map/all_to_all | solution.py:226
Sparse Core Ops, SparseCore 0:
  10.4 106.5 all-gather.1

commit v2 on v1

v2 whole, which is shorter than its diff:
```python
import jax
import jax.numpy as jnp
from jax import lax
from jax.experimental import pallas as pl
from jax.experimental.pallas import tpu as pltpu
from jax.sharding import Mesh
from jax.sharding import PartitionSpec as P

SP = ("sp_0", "sp_1")
EPSILON = 1e-06
F32 = jnp.float32
BF16 = jnp.bfloat16
NT = (((1,), (1,)), ((), ()))
NN = (((1,), (0,)), ((), ()))


def mm(a, b, dims=NN):
    return lax.dot_general(a.astype(BF16), b.astype(BF16), dims, preferred_element_type=F32)


def split_in_two(a):
    high = a.astype(BF16)
    return high, (a - high.astype(F32)).astype(BF16)


def mm2(a, b, dims=NN):
    high, low = split_in_two(a)
    return mm(high, b, dims) + mm(low, b, dims)


def mm3(a, b):
    a_high, a_low = split_in_two(a)
    b_high, b_low = split_in_two(b)
    return mm(a_high, b_high) + (mm(a_high, b_low) + mm(a_low, b_high))


def local_kernel(own_ref, own_rows_ref, pal_ref, pal_rows_ref, message_ref, read_ref, base_ref):
    n = own_ref.shape[0]
    width = own_ref.shape[1] // 3
    back = lax.axis_index("sp_1") % 2
    sign = 1 - 2 * back
    forward = back == 0
    rows = lax.broadcasted_iota(jnp.int32, (n, n), 0)
    cols = lax.broadcasted_iota(jnp.int32, (n, n), 1)
    eye = rows == cols
    reach = (rows - cols) * sign >= 0
    near = [((rows ^ cols) >> lg) == 1 for lg in range(7)]

    def to_col(row):
        return jnp.sum(jnp.where(eye, row, 0.0), axis=1, keepdims=True)

    def to_row(col):
        return jnp.sum(jnp.where(eye, col, 0.0), axis=0, keepdims=True)

    def chosen(pair):
        return jnp.where(forward, pair[0:1], pair[1:2])

    def block(data_ref, rows_ref):
        q, k, v = (data_ref[:, m * width : (m + 1) * width] for m in range(3))
        gates = rows_ref[...]
        beta_row = jax.nn.sigmoid(chosen(gates[0:2]))
        preacts = chosen(gates[2:4])
        soft = jnp.maximum(preacts, 0.0) + jnp.log1p(jnp.exp(-jnp.abs(preacts)))
        speed = jnp.where(forward, gates[7:8, 0:1], gates[7:8, n - 1 : n])
        decay_row = -jnp.exp(speed) * soft + chosen(gates[4:6])
        docs_row = gates[6:7]
        docs_first = jnp.where(forward, docs_row[:, 0:1], docs_row[:, n - 1 : n])
        docs_last = jnp.where(forward, docs_row[:, n - 1 : n], docs_row[:, 0:1])
        docs_col = to_col(docs_row)
        qf, kf = q.astype(F32), k.astype(F32)
        q_scale = lax.rsqrt(jnp.sum(qf * qf, axis=1, keepdims=True) + EPSILON) * width ** (-0.5)
        k_scale = lax.rsqrt(jnp.sum(kf * kf, axis=1, keepdims=True) + EPSILON)
        k_scale_row = to_row(k_scale)
        similar = mm(k, k, NT) * k_scale * k_scale_row
        scored = mm(q, k, NT) * q_scale * k_scale_row
        running = jnp.sum(jnp.where(reach, decay_row, 0.0), axis=1, keepdims=True)
        running_row = to_row(running)
        total = jnp.sum(decay_row, axis=1, keepdims=True)
        within = reach & (docs_col == docs_row)
        spread = jnp.exp(jnp.where(within, running - running_row, -jnp.inf))
        strict = jnp.where(eye, 0.0, similar * spread * to_col(beta_row))
        inverse = jnp.where(eye, 1.0, 0.0) - jnp.where(near[0], strict, 0.0)
        for lg in range(1, 7):
            inverse = inverse - mm3(inverse, mm3(jnp.where(near[lg], strict, 0.0), inverse))
        linked_row = (docs_row == docs_first).astype(F32)
        linked = (docs_col == docs_first).astype(F32)
        ending_row = (docs_row == docs_last).astype(F32)
        update = mm2(inverse * beta_row, v)
        drop = mm2(inverse * (beta_row * jnp.exp(running_row) * linked_row * k_scale_row), k)
        tail = jnp.exp(jnp.minimum(total - running_row, 0.0))
        faded = jnp.transpose(kf) * (k_scale_row * tail * ending_row)
        kept = jnp.exp(total) * (docs_first == docs_last).astype(F32)
        step = jnp.where(eye, kept, 0.0) - mm(faded, drop)
        shift = mm(faded, update)
        scores = scored * spread
        read = qf * (q_scale * jnp.exp(running) * linked) - mm(scores, drop)
        return step, shift, read, mm(scores, update), docs_first, docs_last

    step, shift, read, base, docs_first, docs_mid = block(own_ref, own_rows_ref)
    pal_step, pal_shift, pal_read, pal_base, docs_next, docs_last = block(pal_ref, pal_rows_ref)
    link = (docs_mid == docs_next).astype(F32)
    step, shift = step * link, shift * link
    message_ref[:n, :width] = mm(pal_step, step).astype(BF16)
    message_ref[:n, width:] = (mm(pal_step, shift) + pal_shift).astype(BF16)
    mark_docs(message_ref, n, docs_first, docs_last)
    read_ref[0] = read.astype(BF16)
    read_ref[1] = mm(pal_read, step).astype(BF16)
    base_ref[0] = base
    base_ref[1] = pal_base + mm(pal_read, shift)


def mark_docs(ref, n, docs_first, docs_last):
    ref[n : n + 8] = jnp.broadcast_to(docs_first, (8, ref.shape[1])).astype(BF16)
    ref[n + 8 :] = jnp.broadcast_to(docs_last, (8, ref.shape[1])).astype(BF16)


def combine_kernel(own_ref, in_ref, out_ref, far_ref):
    n = own_ref.shape[0] - 16
    docs_first = own_ref[n : n + 8, 0:1][0:1].astype(F32)
    in_last = in_ref[n + 8 :, 0:1][0:1].astype(F32)
    link = (docs_first == in_last).astype(F32)
    moved = mm(own_ref[:n, :n], in_ref[:n, :]) * link
    shift = (moved[:, n:] + own_ref[:n, n:].astype(F32)).astype(BF16)
    out_ref[:n, :n] = moved[:, :n].astype(BF16)
    out_ref[:n, n:] = shift
    out_ref[n : n + 8] = in_ref[n : n + 8]
    out_ref[n + 8 :] = own_ref[n + 8 :]
    far_ref[:n] = shift
    far_ref[n : n + 8] = in_ref[n : n + 8, :n]
    far_ref[n + 8 :] = own_ref[n + 8 :, :n]


def apply_kernel(own_ref, near_ref, far_ref, read_ref, base_ref, mine_ref, other_ref):
    n = own_ref.shape[0] - 16
    docs_first = own_ref[n : n + 8, 0:1][0:1].astype(F32)
    near_first = near_ref[n : n + 8, 0:1][0:1].astype(F32)
    near_last = near_ref[n + 8 :, 0:1][0:1].astype(F32)
    far_last = far_ref[n + 8 :, 0:1][0:1].astype(F32)
    state = mm(near_ref[:n, :n], far_ref[:n]) * (near_first == far_last).astype(F32)
    state = (state + near_ref[:n, n:].astype(F32)) * (docs_first == near_last).astype(F32)
    other_ref[...] = (base_ref[1] + mm(read_ref[1], state)).astype(BF16)
    mine_ref[...] = base_ref[0] + mm(read_ref[0], state)


def finish_kernel(mine_ref, in_ref, gain_ref, exit_ref, out_ref):
    attn = mine_ref[...] + in_ref[...].astype(F32)
    mean = jnp.mean(attn * attn, axis=1, keepdims=True)
    mixed = (attn * lax.rsqrt(mean + EPSILON) * gain_ref[...]).astype(BF16)
    terms = mm(mixed, exit_ref[...]).astype(BF16)
    step = out_ref.shape[2]
    for m in range(out_ref.shape[0]):
        out_ref[m] = terms[:, m * step : (m + 1) * step]


def vmem(count):
    return [pl.BlockSpec(memory_space=pltpu.VMEM)] * count


def shards(
    skip_path_inputs,
    probe_vectors,
    lookup_vectors,
    payload_vectors,
    learning_strength_preacts,
    forget_preacts,
    forgetting_speed_exponent,
    extra_forgetting_spikes,
    sample_membership,
    channel_group_scaling,
    blend_exit_weights,
    dense_block_scaling,
    widen_projection_weights,
    shrink_projection_weights,
):
    up_width = widen_projection_weights.shape[1]
    weights = lax.all_gather(
        jnp.concatenate([widen_projection_weights, shrink_projection_weights.T], axis=1),
        SP,
        axis=0,
        tiled=True,
    )
    length, width = probe_vectors.shape
    count = lax.axis_size(SP)

    def swapped(array):
        return lax.ppermute(array, SP, [(i, i ^ 1) for i in range(count)])

    def passed(array, distance):
        ways = (2 * distance, -2 * distance)
        return lax.ppermute(array, SP, [(i, (i + ways[i % 2]) % count) for i in range(count)])

    data = jnp.concatenate([probe_vectors, lookup_vectors, payload_vectors], axis=1)
    lanes = lax.broadcasted_iota(jnp.int32, (1, length), 1)
    rows = jnp.concatenate(
        [
            learning_strength_preacts.reshape(2, length),
            forget_preacts.reshape(2, length),
            extra_forgetting_spikes.reshape(2, length),
            sample_membership.astype(F32).reshape(1, length),
            jnp.where(
                lanes < length // 2,
                forgetting_speed_exponent[0:1],
                forgetting_speed_exponent[1:2],
            ),
        ]
    )
    tall = width + 16
    message, read, base = pl.pallas_call(
        local_kernel,
        out_shape=(
            jax.ShapeDtypeStruct((tall, 2 * width), BF16),
            jax.ShapeDtypeStruct((2, length, width), BF16),
            jax.ShapeDtypeStruct((2, length, width), F32),
        ),
        in_specs=vmem(4),
        out_specs=tuple(vmem(3)),
        name="local_maps",
    )(data, rows, swapped(data), swapped(rows))
    joined, far = pl.pallas_call(
        combine_kernel,
        out_shape=(
            jax.ShapeDtypeStruct((tall, 2 * width), BF16),
            jax.ShapeDtypeStruct((tall, width), BF16),
        ),
        in_specs=vmem(2),
        out_specs=tuple(vmem(2)),
        name="combine_maps",
    )(message, passed(message, 1))
    mine, other = pl.pallas_call(
        apply_kernel,
        out_shape=(
            jax.ShapeDtypeStruct((length, width), F32),
            jax.ShapeDtypeStruct((length, width), BF16),
        ),
        in_specs=vmem(5),
        out_specs=tuple(vmem(2)),
        name="apply_state",
    )(message, passed(joined, 1), passed(far, 3), read, base)
    head_terms = pl.pallas_call(
        finish_kernel,
        out_shape=jax.ShapeDtypeStruct((8, length, blend_exit_weights.shape[1] // 8), BF16),
        in_specs=vmem(4),
        out_specs=vmem(1)[0],
        name="finish_mixer",
    )(mine, swapped(other), channel_group_scaling.reshape(1, width), blend_exit_weights)
    model_width = skip_path_inputs.shape[1]
    col_count = model_width // lax.axis_size("tp")
    col_start = lax.axis_index("tp") * col_count
    parts = lax.all_to_all(head_terms, "tp", 0, 0, tiled=True)
    own_residual = lax.dynamic_slice_in_dim(skip_path_inputs, col_start, col_count, 1).astype(
        F32
    ) + jnp.sum(parts.astype(F32), axis=0)
    residual = lax.all_gather(own_residual.astype(BF16), "tp", axis=1, tiled=True).astype(F32)
    squares = jnp.mean(residual * residual, axis=1, keepdims=True)
    normed = (residual * lax.rsqrt(squares + EPSILON) * dense_block_scaling).astype(BF16)
    raised = jnp.dot(normed, weights[:, :up_width], preferred_element_type=F32)
    active = jnp.square(jax.nn.relu(raised)).astype(BF16)
    lowered = lax.dot_general(active, weights[:, up_width:], NT, preferred_element_type=F32)
    turned = jnp.moveaxis(lowered.astype(BF16).reshape(length, -1, col_count), 1, 0)
    pieces = lax.all_to_all(turned, "tp", 0, 0, tiled=True)
    return (own_residual + jnp.sum(pieces.astype(F32), axis=0)).astype(BF16)


def solution(mesh):
    torus = Mesh(mesh.devices.reshape(8, 8, mesh.shape["tp"]), ("sp_0", "sp_1", "tp"))
    placed = (
        P(SP, None),
        P(SP, "tp"),
        P(SP, "tp"),
        P(SP, "tp"),
        P(None, SP, "tp"),
        P(None, SP, "tp"),
        P(None, "tp"),
        P(None, SP, "tp"),
        P(SP),
        P(),
        P("tp", None),
        P(),
        P(SP, "tp"),
        P("tp", SP),
    )
    return jax.shard_map(
        shards, mesh=torus, in_specs=placed, out_specs=P(SP, "tp"), check_vma=False
    )
```

time: 159 us -> 145 us (0.912)
  the two profiles are of different devices: /device:TPU:24 before, /device:TPU:1 now
where the time goes in v2:
time: 145 us; the launch traced here: 144 us
  waiting for transfers between devices  39.2 us (27%)
  starting transfers between devices  30.8 us (21%)
  blocking collectives  28.2 us (19%)
  between operations  13.5 us (9%)
  Pallas kernels  13.1 us (9%)
  local copies, waits for them, and re-layouts  7.49 us (5%)
  other arithmetic  6.11 us (4%)
  matrix products  5.61 us (4%)
    ppermute x3, waiting for transfers between devices, passed(): lax.ppermute(array, SP, [(i, (i + ways[i % 2]) % count) for i in range(co...  18.5 us
    all_to_all x1, blocking collectives, shards(): pieces = lax.all_to_all(turned, 'tp', 0, 0, tiled=True)  14.3 us
    all_gather x1, blocking collectives, shards(): lax.all_gather(own_residual.astype(BF16), 'tp', axis=1, tiled=True)  13.9 us
    ppermute x3, starting transfers between devices, swapped(): return lax.ppermute(array, SP, [(i, i ^ 1) for i in range(count)])  12.5 us
    all_to_all x1, starting transfers between devices, shards(): parts = lax.all_to_all(head_terms, 'tp', 0, 0, tiled=True)  10.7 us
    all_to_all x1, waiting for transfers between devices, shards(): parts = lax.all_to_all(head_terms, 'tp', 0, 0, tiled=True)  9.35 us
    ppermute x3, starting transfers between devices, passed(): lax.ppermute(array, SP, [(i, (i + ways[i % 2]) % count) for i in range(co...  7.7 us
    all_gather x1, waiting for transfers between devices, shards(): lax.all_gather(jnp.concatenate([widen_projection_weights, shrink_projecti...  7.1 us
  transfers between devices with their start and end apart: 8, of which 6 were waited for; matrix products, arithmetic and copies ran while one was open for 5% of the time, Pallas kernels for 9%

profile of v2, /device:TPU:1, one launch (start us, length us, event | category | flops | bytes accessed | tf_op | source)
XLA Modules:
  0.0 144.1 jit_solution(3581295332342463476)
XLA Ops:
  6.5 0.0 all-gather.2.cloned.1.call-start
  6.5 1.5 %pad_maximum_fusion = bf16[32,2048]{1,0:T(8,128)(2,1)} fusion(bf16[32,1024]{1,0:T(8,128)(2,1)} %bitcast.18, bf16[32,1024]{1,0:T(8,128)(2,1)} %param.26), kind=kLoop, calls=%fused_computation.19 | loop fusion | flops 262144 | bytes 262144 | tf_op jit(solution)/shard_map/concatenate | solution.py:177
  8.1 0.0 all-gather.2.cloned.1.call-update
  8.1 0.8 constant_dynamic-update-slice_fusion.2
  8.9 0.8 constant_dynamic-update-slice_fusion.1
  9.6 0.8 constant_dynamic-update-slice_fusion.own_ref
  10.4 0.0 copy-start
  10.4 4.0 %collective-permute-start = (bf16[128,384]{1,0:T(8,128)(2,1)S(1)}, bf16[128,384]{1,0:T(8,128)(2,1)S(1)}, u32[]{:S(2)}, u32[]{:S(2)}) collective-permute-start(bf16[128,384]{1,0:T(8,128)(2,1)S(1)} %constant_dynamic-update-slice_fusion.own_ref), channel_id=1, source_target_pairs={{0,8},{8,0},{16,24},{24,16},{32,40},{40,32},{48,56},{56,48},{64,72... | collective-permute-start | bytes 294920 | tf_op jit(solution)/shard_map/ppermute | solution.py:186
  14.4 1.3 fusion.30
  15.8 0.7 convert_bitcast_fusion
  16.4 1.2 compare_select_fusion
  17.6 0.7 concatenate.10.own_rows_ref
  18.4 0.0 copy-start.6
  18.4 1.9 %collective-permute-start.1 = (f32[8,128]{1,0:T(8,128)S(1)}, f32[8,128]{1,0:T(8,128)S(1)}, u32[]{:S(2)}, u32[]{:S(2)}) collective-permute-start(f32[8,128]{1,0:T(8,128)S(1)} %concatenate.10.own_rows_ref), channel_id=1, source_target_pairs={{0,8},{8,0},{16,24},{24,16},{32,40},{40,32},{48,56},{56,48},{64,72... | collective-permute-start | bytes 12296 | tf_op jit(solution)/shard_map/ppermute | solution.py:186
  20.3 2.8 %collective-permute-done.1.pal_rows_ref = f32[8,128]{1,0:T(8,128)S(1)} collective-permute-done((f32[8,128]{1,0:T(8,128)S(1)}, f32[8,128]{1,0:T(8,128)S(1)}, u32[]{:S(2)}, u32[]{:S(2)}) %collective-permute-start.1) | collective-permute-done | bytes 4128 | tf_op jit(solution)/shard_map/ppermute | solution.py:186
  23.0 0.0 copy-start.7
  23.0 0.0 collective-permute-done.pal_ref
  23.0 0.0 copy-done
  23.1 0.0 copy-done.6
  23.1 0.6 copy-done.7
  23.6 0.0 copy-start.1
  23.6 0.6 copy-done.1
  24.3 6.9 %local_maps.1 = (bf16[144,256]{1,0:T(8,128)(2,1)}, bf16[2,128,128]{2,1,0:T(8,128)(2,1)}, f32[2,128,128]{2,1,0:T(8,128)}) custom-call(bf16[128,384]{1,0:T(8,128)(2,1)} %copy-done, f32[8,128]{1,0:T(8,128)} %copy-done.6, bf16[128,384]{1,0:T(8,128)(2,1)} %copy-done.1, f32[8,128]{1,0:T(8,128)} %copy-done.7), custom_call_target="tpu_custom_call" | custom-call | tf_op jit(solution)/shard_map/local_maps/pallas_call | solution.py:208
  31.2 3.9 %collective-permute-start.2 = (bf16[144,256]{1,0:T(8,128)(2,1)}, bf16[144,256]{1,0:T(8,128)(2,1)S(1)}, u32[]{:S(2)}, u32[]{:S(2)}) collective-permute-start(bf16[144,256]{1,0:T(8,128)(2,1)} %get-tuple-element.12.own_ref), channel_id=1, source_target_pairs={{0,16},{8,504},{16,32},{24,8},{32,48},{40,24},{48,64},{56,40},{64,... | collective-permute-start | bytes 221192 | tf_op jit(solution)/shard_map/ppermute | solution.py:190
  35.0 11.3 %collective-permute-done.2.in_ref = bf16[144,256]{1,0:T(8,128)(2,1)S(1)} collective-permute-done((bf16[144,256]{1,0:T(8,128)(2,1)}, bf16[144,256]{1,0:T(8,128)(2,1)S(1)}, u32[]{:S(2)}, u32[]{:S(2)}) %collective-permute-start.2) | collective-permute-done | bytes 73760 | tf_op jit(solution)/shard_map/ppermute | solution.py:190
  46.3 0.0 copy-start.2
  46.3 0.6 copy-done.2
  47.0 1.7 %combine_maps.1 = (bf16[144,256]{1,0:T(8,128)(2,1)}, bf16[144,128]{1,0:T(8,128)(2,1)}) custom-call(bf16[144,256]{1,0:T(8,128)(2,1)} %get-tuple-element.12.own_ref, bf16[144,256]{1,0:T(8,128)(2,1)} %copy-done.2), custom_call_target="tpu_custom_call" | custom-call | tf_op jit(solution)/shard_map/combine_maps/pallas_call | solution.py:219
  48.7 1.9 %collective-permute-start.3 = (bf16[144,256]{1,0:T(8,128)(2,1)}, bf16[144,256]{1,0:T(8,128)(2,1)S(1)}, u32[]{:S(2)}, u32[]{:S(2)}) collective-permute-start(bf16[144,256]{1,0:T(8,128)(2,1)} %get-tuple-element.13), channel_id=1, source_target_pairs={{0,16},{8,504},{16,32},{24,8},{32,48},{40,24},{48,64},{56,40},{64,... | collective-permute-start | bytes 221192 | tf_op jit(solution)/shard_map/ppermute | solution.py:190
  50.6 1.9 %collective-permute-start.4 = (bf16[144,128]{1,0:T(8,128)(2,1)}, bf16[144,128]{1,0:T(8,128)(2,1)S(1)}, u32[]{:S(2)}, u32[]{:S(2)}) collective-permute-start(bf16[144,128]{1,0:T(8,128)(2,1)} %get-tuple-element.14), channel_id=1, source_target_pairs={{0,48},{8,472},{16,64},{24,488},{32,80},{40,504},{48,96},{56,8},{6... | collective-permute-start | bytes 110600 | tf_op jit(solution)/shard_map/ppermute | solution.py:190
  52.5 7.2 %collective-permute-done.4.far_ref = bf16[144,128]{1,0:T(8,128)(2,1)S(1)} collective-permute-done((bf16[144,128]{1,0:T(8,128)(2,1)}, bf16[144,128]{1,0:T(8,128)(2,1)S(1)}, u32[]{:S(2)}, u32[]{:S(2)}) %collective-permute-start.4) | collective-permute-done | bytes 36896 | tf_op jit(solution)/shard_map/ppermute | solution.py:190
  59.7 0.0 copy-start.4
  59.7 0.0 collective-permute-done.3.near_ref
  59.7 0.0 copy-start.3
  59.7 0.6 copy-done.4
  60.3 0.0 copy-done.3
  60.4 2.0 %apply_state.1 = (f32[128,128]{1,0:T(8,128)}, bf16[128,128]{1,0:T(8,128)(2,1)}) custom-call(bf16[144,256]{1,0:T(8,128)(2,1)} %get-tuple-element.12.own_ref, bf16[144,256]{1,0:T(8,128)(2,1)} %copy-done.3, bf16[144,128]{1,0:T(8,128)(2,1)} %copy-done.4, bf16[2,128,128]{2,1,0:T(8,128)(2,1)} %get-tuple-element.15.read_ref, f32[2,128,128]{2,1,0:T(8,128)} %get-tuple-element.16.base_ref), custom_call_target="tpu_custom_call" | custom-call | tf_op jit(solution)/shard_map/apply_state/pallas_call | solution.py:229
  62.3 6.5 %collective-permute-start.5 = (bf16[128,128]{1,0:T(8,128)(2,1)}, bf16[128,128]{1,0:T(8,128)(2,1)S(1)}, u32[]{:S(2)}, u32[]{:S(2)}) collective-permute-start(bf16[128,128]{1,0:T(8,128)(2,1)} %get-tuple-element.18), channel_id=1, source_target_pairs={{0,8},{8,0},{16,24},{24,16},{32,40},{40,32},{48,56},{56,48},{64,72... | collective-permute-start | bytes 98312 | tf_op jit(solution)/shard_map/ppermute | solution.py:186
  68.9 1.5 %collective-permute-done.5.in_ref = bf16[128,128]{1,0:T(8,128)(2,1)S(1)} collective-permute-done((bf16[128,128]{1,0:T(8,128)(2,1)}, bf16[128,128]{1,0:T(8,128)(2,1)S(1)}, u32[]{:S(2)}, u32[]{:S(2)}) %collective-permute-start.5) | collective-permute-done | bytes 32800 | tf_op jit(solution)/shard_map/ppermute | solution.py:186
  70.4 0.0 copy-start.5
  70.4 0.6 copy-done.5
  71.0 2.5 %finish_mixer.1 = bf16[8,128,256]{2,1,0:T(8,128)(2,1)} custom-call(f32[128,128]{1,0:T(8,128)} %get-tuple-element.17.mine_ref, bf16[128,128]{1,0:T(8,128)(2,1)} %copy-done.5, f32[1,128]{1,0:T(1,128)} %bitcast.22, bf16[128,2048]{1,0:T(8,128)(2,1)} %exit_ref.1), custom_call_target="tpu_custom_call" | custom-call | tf_op jit(solution)/shard_map/finish_mixer/pallas_call | solution.py:239
  73.5 10.7 %all-to-all-start = ((bf16[8,128,256]{2,1,0:T(8,128)(2,1)}), bf16[8,128,256]{2,1,0:T(8,128)(2,1)S(1)}, u32[]{:S(2)}, u32[]{:S(2)}) async-start(bf16[8,128,256]{2,1,0:T(8,128)(2,1)} %finish_mixer.1), calls=%async_computation | async-start | bytes 1048576 | tf_op jit(solution)/shard_map/all_to_all | solution.py:249
  84.1 9.3 %all-to-all-done = bf16[8,128,256]{2,1,0:T(8,128)(2,1)S(1)} async-done(((bf16[8,128,256]{2,1,0:T(8,128)(2,1)}), bf16[8,128,256]{2,1,0:T(8,128)(2,1)S(1)}, u32[]{:S(2)}, u32[]{:S(2)}) %all-to-all-start) | async-done | bytes 524320 | tf_op jit(solution)/shard_map/all_to_all | solution.py:249
  93.5 0.1 convert_reduce_fusion.1
  93.6 0.9 fusion.28
  94.4 13.9 %all_gather.6 = bf16[128,2048]{1,0:T(8,128)(2,1)S(1)} all-gather(bf16[128,256]{1,0:T(8,128)(2,1)S(1)} %fusion.28), channel_id=1, replica_groups=mesh['sp_0'=8,'sp_1'=8,'tp'=8] {'tp'}, dimensions={1}, use_global_device_ids=true | all-gather | bytes 589824 | tf_op jit(solution)/shard_map/all_gather | solution.py:253
  108.4 0.2 fusion.18
  108.5 7.1 %all-gather.2.cloned.1.call-done = bf16[2048,2048]{1,0:T(8,128)(2,1)} async-done(((bf16[32,2048]{1,0:T(8,128)(2,1)}), bf16[2048,2048]{1,0:T(8,128)(2,1)}) %all-gather.2.cloned.1.call-update) | async-done | bytes 8388624 | tf_op jit(solution)/shard_map/all_gather | solution.py:176
  115.7 5.6 %fusion.4 = bf16[128,2048]{1,0:T(8,128)(2,1)S(1)} fusion(bf16[2048,2048]{1,0:T(8,128)(2,1)} %all-gather.2.cloned.1.call-done, bf16[128,2048]{1,0:T(8,128)(2,1)S(1)} %all_gather.6, f32[2048]{0:T(1024)} %param.25, f32[128]{0:T(128)S(1)} %add_rsqrt_fusion), kind=kOutput, calls=%fused_computation.4 | convolution fusion | flops 1075445760 | bytes 9445888 | tf_op jit(solution)/shard_map/dot_general | solution.py:258
  121.3 14.3 %all_to_all.10 = bf16[8,128,256]{2,1,0:T(8,128)(2,1)S(1)} all-to-all(bf16[8,128,256]{2,1,0:T(8,128)(2,1)S(1)} %bitcast.16), channel_id=1, replica_groups=mesh['sp_0'=8,'sp_1'=8,'tp'=8] {'tp'}, dimensions={0} | all-to-all | bytes 1048576 | tf_op jit(solution)/shard_map/all_to_all | solution.py:260
  135.6 0.1 convert_reduce_fusion
  135.7 1.5 %add_convert_fusion = bf16[128,256]{1,0:T(8,128)(2,1)} fusion(f32[128,256]{1,0:T(8,128)S(1)} %convert_reduce_fusion, f32[128,256]{1,0:T(8,128)S(1)} %convert_reduce_fusion.1, bf16[128,2048]{1,0:T(8,128)(2,1)} %param.14, s32[]{:T(128)S(6)} %select_n.15), kind=kLoop, calls=%fused_computation.20 | loop fusion | flops 131072 | bytes 393220 | tf_op jit(solution)/shard_map/convert_element_type | solution.py:261
  (2 shorter events, 0.0 us)
Async XLA Ops:
  6.5 109.1 %all-gather.2.cloned.1.call-start = ((), (), s32[]{:S(2)}) async-start(), calls=%async_computation.2 | async-start | bytes 8519680 | tf_op jit(solution)/shard_map/all_gather | solution.py:176
  10.4 12.6 %copy-start = (bf16[128,384]{1,0:T(8,128)(2,1)}, bf16[128,384]{1,0:T(8,128)(2,1)S(1)}, u32[]{:S(2)}) copy-start(bf16[128,384]{1,0:T(8,128)(2,1)S(1)} %constant_dynamic-update-slice_fusion.own_ref) | copy-start | bytes 294916
  10.4 12.6 %collective-permute-start = (bf16[128,384]{1,0:T(8,128)(2,1)S(1)}, bf16[128,384]{1,0:T(8,128)(2,1)S(1)}, u32[]{:S(2)}, u32[]{:S(2)}) collective-permute-start(bf16[128,384]{1,0:T(8,128)(2,1)S(1)} %constant_dynamic-update-slice_fusion.own_ref), channel_id=1, source_target_pairs={{0,8},{8,0},{16,24},{24,16},{32,40},{40,32},{48,56},{56,48},{64,72... | collective-permute-start | bytes 294920 | tf_op jit(solution)/shard_map/ppermute | solution.py:186
  18.4 4.7 %copy-start.6 = (f32[8,128]{1,0:T(8,128)}, f32[8,128]{1,0:T(8,128)S(1)}, u32[]{:S(2)}) copy-start(f32[8,128]{1,0:T(8,128)S(1)} %concatenate.10.own_rows_ref) | copy-start | bytes 12292
  18.4 4.7 %collective-permute-start.1 = (f32[8,128]{1,0:T(8,128)S(1)}, f32[8,128]{1,0:T(8,128)S(1)}, u32[]{:S(2)}, u32[]{:S(2)}) collective-permute-start(f32[8,128]{1,0:T(8,128)S(1)} %concatenate.10.own_rows_ref), channel_id=1, source_target_pairs={{0,8},{8,0},{16,24},{24,16},{32,40},{40,32},{48,56},{56,48},{64,72... | collective-permute-start | bytes 12296 | tf_op jit(solution)/shard_map/ppermute | solution.py:186
  23.0 0.6 copy-start.7
  23.6 0.6 copy-start.1
  31.2 15.2 %collective-permute-start.2 = (bf16[144,256]{1,0:T(8,128)(2,1)}, bf16[144,256]{1,0:T(8,128)(2,1)S(1)}, u32[]{:S(2)}, u32[]{:S(2)}) collective-permute-start(bf16[144,256]{1,0:T(8,128)(2,1)} %get-tuple-element.12.own_ref), channel_id=1, source_target_pairs={{0,16},{8,504},{16,32},{24,8},{32,48},{40,24},{48,64},{56,40},{64,... | collective-permute-start | bytes 221192 | tf_op jit(solution)/shard_map/ppermute | solution.py:190
  46.3 0.6 copy-start.2
  48.7 11.0 %collective-permute-start.3 = (bf16[144,256]{1,0:T(8,128)(2,1)}, bf16[144,256]{1,0:T(8,128)(2,1)S(1)}, u32[]{:S(2)}, u32[]{:S(2)}) collective-permute-start(bf16[144,256]{1,0:T(8,128)(2,1)} %get-tuple-element.13), channel_id=1, source_target_pairs={{0,16},{8,504},{16,32},{24,8},{32,48},{40,24},{48,64},{56,40},{64,... | collective-permute-start | bytes 221192 | tf_op jit(solution)/shard_map/ppermute | solution.py:190
  50.6 9.1 %collective-permute-start.4 = (bf16[144,128]{1,0:T(8,128)(2,1)}, bf16[144,128]{1,0:T(8,128)(2,1)S(1)}, u32[]{:S(2)}, u32[]{:S(2)}) collective-permute-start(bf16[144,128]{1,0:T(8,128)(2,1)} %get-tuple-element.14), channel_id=1, source_target_pairs={{0,48},{8,472},{16,64},{24,488},{32,80},{40,504},{48,96},{56,8},{6... | collective-permute-start | bytes 110600 | tf_op jit(solution)/shard_map/ppermute | solution.py:190
  59.7 0.6 copy-start.4
  59.7 0.6 copy-start.3
  62.3 8.0 %collective-permute-start.5 = (bf16[128,128]{1,0:T(8,128)(2,1)}, bf16[128,128]{1,0:T(8,128)(2,1)S(1)}, u32[]{:S(2)}, u32[]{:S(2)}) collective-permute-start(bf16[128,128]{1,0:T(8,128)(2,1)} %get-tuple-element.18), channel_id=1, source_target_pairs={{0,8},{8,0},{16,24},{24,16},{32,40},{40,32},{48,56},{56,48},{64,72... | collective-permute-start | bytes 98312 | tf_op jit(solution)/shard_map/ppermute | solution.py:186
  70.4 0.6 copy-start.5
  73.5 20.0 %all-to-all-start = ((bf16[8,128,256]{2,1,0:T(8,128)(2,1)}), bf16[8,128,256]{2,1,0:T(8,128)(2,1)S(1)}, u32[]{:S(2)}, u32[]{:S(2)}) async-start(bf16[8,128,256]{2,1,0:T(8,128)(2,1)} %finish_mixer.1), calls=%async_computation | async-start | bytes 1048576 | tf_op jit(solution)/shard_map/all_to_all | solution.py:249
Sparse Core Ops, SparseCore 0:
  10.4 105.2 all-gather.1

commit v3 on v2

--- a/solution.py
+++ b/solution.py
@@ -6,7 +6,7 @@
 from jax.sharding import Mesh
 from jax.sharding import PartitionSpec as P
 
-SP = ("sp_0", "sp_1")
+SP = ("sp_0", "sp_1", "pair")
 EPSILON = 1e-06
 F32 = jnp.float32
 BF16 = jnp.bfloat16
@@ -34,10 +34,22 @@
     return mm(a_high, b_high) + (mm(a_high, b_low) + mm(a_low, b_high))
 
 
-def local_kernel(own_ref, own_rows_ref, pal_ref, pal_rows_ref, message_ref, read_ref, base_ref):
-    n = own_ref.shape[0]
+def pack_kernel(q_ref, k_ref, v_ref, strength_ref, forget_ref, spike_ref, docs_ref, out_ref):
+    n, width = q_ref.shape
+    for m, ref in enumerate((q_ref, k_ref, v_ref)):
+        out_ref[:n, m * width : (m + 1) * width] = ref[...]
+    docs = docs_ref[...].astype(F32)
+    rest = jnp.concatenate([strength_ref[...], forget_ref[...], spike_ref[...], docs, docs])
+    for m in range(3):
+        piece = rest.astype(BF16)
+        out_ref[n:, m * width : (m + 1) * width] = piece
+        rest = rest - piece.astype(F32)
+
+
+def local_kernel(own_ref, pal_ref, speed_ref, message_ref, read_ref, base_ref):
+    n = own_ref.shape[0] - 8
     width = own_ref.shape[1] // 3
-    back = lax.axis_index("sp_1") % 2
+    back = lax.axis_index("pair")
     sign = 1 - 2 * back
     forward = back == 0
     rows = lax.broadcasted_iota(jnp.int32, (n, n), 0)
@@ -55,13 +67,16 @@
     def chosen(pair):
         return jnp.where(forward, pair[0:1], pair[1:2])
 
-    def block(data_ref, rows_ref):
-        q, k, v = (data_ref[:, m * width : (m + 1) * width] for m in range(3))
-        gates = rows_ref[...]
+    def block(data_ref):
+        q, k, v = (data_ref[:n, m * width : (m + 1) * width] for m in range(3))
+        high, middle, low = (
+            data_ref[n:, m * width : (m + 1) * width].astype(F32) for m in range(3)
+        )
+        gates = (low + middle) + high
         beta_row = jax.nn.sigmoid(chosen(gates[0:2]))
         preacts = chosen(gates[2:4])
         soft = jnp.maximum(preacts, 0.0) + jnp.log1p(jnp.exp(-jnp.abs(preacts)))
-        speed = jnp.where(forward, gates[7:8, 0:1], gates[7:8, n - 1 : n])
+        speed = jnp.where(forward, speed_ref[:, 0:1], speed_ref[:, 1:2])
         decay_row = -jnp.exp(speed) * soft + chosen(gates[4:6])
         docs_row = gates[6:7]
         docs_first = jnp.where(forward, docs_row[:, 0:1], docs_row[:, n - 1 : n])
@@ -96,8 +111,8 @@
         read = qf * (q_scale * jnp.exp(running) * linked) - mm(scores, drop)
         return step, shift, read, mm(scores, update), docs_first, docs_last
 
-    step, shift, read, base, docs_first, docs_mid = block(own_ref, own_rows_ref)
-    pal_step, pal_shift, pal_read, pal_base, docs_next, docs_last = block(pal_ref, pal_rows_ref)
+    step, shift, read, base, docs_first, docs_mid = block(own_ref)
+    pal_step, pal_shift, pal_read, pal_base, docs_next, docs_last = block(pal_ref)
     link = (docs_mid == docs_next).astype(F32)
     step, shift = step * link, shift * link
     message_ref[:n, :width] = mm(pal_step, step).astype(BF16)
@@ -172,13 +187,6 @@
     widen_projection_weights,
     shrink_projection_weights,
 ):
-    up_width = widen_projection_weights.shape[1]
-    weights = lax.all_gather(
-        jnp.concatenate([widen_projection_weights, shrink_projection_weights.T], axis=1),
-        SP,
-        axis=0,
-        tiled=True,
-    )
     length, width = probe_vectors.shape
     count = lax.axis_size(SP)
 
@@ -189,20 +197,46 @@
         ways = (2 * distance, -2 * distance)
         return lax.ppermute(array, SP, [(i, (i + ways[i % 2]) % count) for i in range(count)])
 
-    data = jnp.concatenate([probe_vectors, lookup_vectors, payload_vectors], axis=1)
-    lanes = lax.broadcasted_iota(jnp.int32, (1, length), 1)
-    rows = jnp.concatenate(
-        [
-            learning_strength_preacts.reshape(2, length),
-            forget_preacts.reshape(2, length),
-            extra_forgetting_spikes.reshape(2, length),
-            sample_membership.astype(F32).reshape(1, length),
-            jnp.where(
-                lanes < length // 2,
-                forgetting_speed_exponent[0:1],
-                forgetting_speed_exponent[1:2],
-            ),
-        ]
+    data = pl.pallas_call(
+        pack_kernel,
+        out_shape=jax.ShapeDtypeStruct((length + 8, 3 * width), BF16),
+        in_specs=vmem(7),
+        out_specs=vmem(1)[0],
+        name="pack_inputs",
+    )(
+        probe_vectors,
+        lookup_vectors,
+        payload_vectors,
+        learning_strength_preacts.reshape(2, length),
+        forget_preacts.reshape(2, length),
+        extra_forgetting_spikes.reshape(2, length),
+        sample_membership.reshape(1, length),
+    )
+    pal_data = swapped(data)
+    side = lax.axis_index("pair")
+    half = widen_projection_weights.shape[1] // 2
+
+    def halves(which):
+        return jnp.concatenate(
+            [
+                lax.dynamic_slice_in_dim(array, which * half, half, 1)
+                for array in (widen_projection_weights, shrink_projection_weights.T)
+            ],
+            axis=1,
+        )
+
+    kept_half = halves(side)
+    given_half = swapped(halves(1 - side))
+    weights = lax.all_gather(
+        jnp.concatenate(
+            [
+                jnp.where(side == 0, kept_half, given_half),
+                jnp.where(side == 0, given_half, kept_half),
+            ]
+        ),
+        SP[:2],
+        axis=0,
+        tiled=True,
     )
     tall = width + 16
     message, read, base = pl.pallas_call(
@@ -212,10 +246,10 @@
             jax.ShapeDtypeStruct((2, length, width), BF16),
             jax.ShapeDtypeStruct((2, length, width), F32),
         ),
-        in_specs=vmem(4),
+        in_specs=vmem(3),
         out_specs=tuple(vmem(3)),
         name="local_maps",
-    )(data, rows, swapped(data), swapped(rows))
+    )(data, pal_data, forgetting_speed_exponent.T)
     joined, far = pl.pallas_call(
         combine_kernel,
         out_shape=(
@@ -250,19 +284,23 @@
     own_residual = lax.dynamic_slice_in_dim(skip_path_inputs, col_start, col_count, 1).astype(
         F32
     ) + jnp.sum(parts.astype(F32), axis=0)
-    residual = lax.all_gather(own_residual.astype(BF16), "tp", axis=1, tiled=True).astype(F32)
+    sent_residual = own_residual.astype(BF16)
+    both = jnp.concatenate([sent_residual, swapped(sent_residual)])
+    residual = lax.all_gather(both, "tp", axis=1, tiled=True).astype(F32)
     squares = jnp.mean(residual * residual, axis=1, keepdims=True)
     normed = (residual * lax.rsqrt(squares + EPSILON) * dense_block_scaling).astype(BF16)
-    raised = jnp.dot(normed, weights[:, :up_width], preferred_element_type=F32)
+    raised = jnp.dot(normed, weights[:, :half], preferred_element_type=F32)
     active = jnp.square(jax.nn.relu(raised)).astype(BF16)
-    lowered = lax.dot_general(active, weights[:, up_width:], NT, preferred_element_type=F32)
-    turned = jnp.moveaxis(lowered.astype(BF16).reshape(length, -1, col_count), 1, 0)
+    lowered = lax.dot_general(active, weights[:, half:], NT, preferred_element_type=F32)
+    turned = jnp.moveaxis(lowered.astype(BF16).reshape(2 * length, -1, col_count), 1, 0)
     pieces = lax.all_to_all(turned, "tp", 0, 0, tiled=True)
-    return (own_residual + jnp.sum(pieces.astype(F32), axis=0)).astype(BF16)
+    sums = jnp.sum(pieces.astype(F32), axis=0)
+    given = swapped(sums[length:].astype(BF16)).astype(F32)
+    return (own_residual + sums[:length] + given).astype(BF16)
 
 
 def solution(mesh):
-    torus = Mesh(mesh.devices.reshape(8, 8, mesh.shape["tp"]), ("sp_0", "sp_1", "tp"))
+    torus = Mesh(mesh.devices.reshape(8, 4, 2, mesh.shape["tp"]), (*SP, "tp"))
     placed = (
         P(SP, None),
         P(SP, "tp"),

time: 145 us -> 258 us (1.78)
  waiting for transfers between devices: 39.2 us -> 157 us
  starting transfers between devices: 30.8 us -> 37.1 us
  blocking collectives: 28.2 us -> 22.5 us
  local copies, waits for them, and re-layouts: 7.49 us -> 2.63 us
    all_gather x1 -> x2, waiting for transfers between devices: 7.1 us -> 119 us  [the longest x1 102 us: shards(): lax.all_gather(jnp.concatenate([jnp.where(side == 0, kept_half, given_hal...]
    all_gather x1 -> x0, blocking collectives: 13.9 us -> none  [shards(): lax.all_gather(own_residual.astype(BF16), 'tp', axis=1, tiled=True)]
    all_to_all x1, blocking collectives: 14.3 us -> 22.5 us  [shards(): pieces = lax.all_to_all(turned, 'tp', 0, 0, tiled=True)]
    ppermute x3 -> x5, starting transfers between devices: 12.5 us -> 19 us  [swapped(): return lax.ppermute(array, SP, [(i, i ^ 1) for i in range(count)])]
    ppermute x3 -> x5, waiting for transfers between devices: 4.26 us -> 10.1 us  [swapped(): return lax.ppermute(array, SP, [(i, i ^ 1) for i in range(count)])]
  transfers between devices with their start and end apart: 8 -> 11, of which waited for: 6 -> 10; matrix products, arithmetic and copies ran while one was open for 5% -> 1% of each run, Pallas kernels for 9% -> 0%
where the time goes in v3:
time: 258 us; the launch traced here: 257 us
  waiting for transfers between devices  157 us (61%)
  starting transfers between devices  37.1 us (14%)
  blocking collectives  22.5 us (9%)
  Pallas kernels  14.3 us (6%)
  between operations  13.6 us (5%)
  other arithmetic  5.44 us (2%)
  matrix products  3.91 us (2%)
  local copies, waits for them, and re-layouts  2.63 us (1%)
    all_gather x1, waiting for transfers between devices, shards(): lax.all_gather(jnp.concatenate([jnp.where(side == 0, kept_half, given_hal...  102 us
    all_to_all x1, blocking collectives, shards(): pieces = lax.all_to_all(turned, 'tp', 0, 0, tiled=True)  22.5 us
    ppermute x5, starting transfers between devices, swapped(): return lax.ppermute(array, SP, [(i, i ^ 1) for i in range(count)])  19 us
    ppermute x3, waiting for transfers between devices, passed(): lax.ppermute(array, SP, [(i, (i + ways[i % 2]) % count) for i in range(co...  19 us
    all_gather x1, waiting for transfers between devices, shards(): residual = lax.all_gather(both, 'tp', axis=1, tiled=True).astype(F32)  16.4 us
    ppermute x5, waiting for transfers between devices, swapped(): return lax.ppermute(array, SP, [(i, i ^ 1) for i in range(count)])  10.1 us
    all_to_all x1, starting transfers between devices, shards(): parts = lax.all_to_all(head_terms, 'tp', 0, 0, tiled=True)  9.7 us
    all_to_all x1, waiting for transfers between devices, shards(): parts = lax.all_to_all(head_terms, 'tp', 0, 0, tiled=True)  9.35 us
  transfers between devices with their start and end apart: 11, of which 10 were waited for; matrix products, arithmetic and copies ran while one was open for 1% of the time, Pallas kernels for 0%

profile of v3, /device:TPU:1, one launch (start us, length us, event | category | flops | bytes accessed | tf_op | source)
XLA Modules:
  0.0 256.7 jit_solution(12202805451451469435)
XLA Ops:
  6.5 1.5 pack_inputs.1.own_ref
  8.0 4.0 %collective-permute-start = (bf16[136,384]{1,0:T(8,128)(2,1)}, bf16[136,384]{1,0:T(8,128)(2,1)S(1)}, u32[]{:S(2)}, u32[]{:S(2)}) collective-permute-start(bf16[136,384]{1,0:T(8,128)(2,1)} %pack_inputs.1.own_ref), channel_id=1, source_target_pairs={{0,8},{8,0},{16,24},{24,16},{32,40},{40,32},{48,56},{56,48},{64,72... | collective-permute-start | bytes 313352 | tf_op jit(solution)/shard_map/ppermute | solution.py:194
  12.1 2.3 collective-permute-done.pal_ref
  14.3 0.0 copy-start
  14.3 0.6 copy-done
  15.0 6.9 %local_maps.1 = (bf16[144,256]{1,0:T(8,128)(2,1)}, bf16[2,128,128]{2,1,0:T(8,128)(2,1)}, f32[2,128,128]{2,1,0:T(8,128)}) custom-call(bf16[136,384]{1,0:T(8,128)(2,1)} %pack_inputs.1.own_ref, bf16[136,384]{1,0:T(8,128)(2,1)} %copy-done, f32[1,2]{1,0:T(1,128)} %bitcast.23), custom_call_target="tpu_custom_call" | custom-call | tf_op jit(solution)/shard_map/local_maps/pallas_call | solution.py:242
  21.8 0.0 copy-start.3
  21.8 0.0 copy-start.4
  21.8 4.5 %collective-permute-start.1 = (bf16[144,256]{1,0:T(8,128)(2,1)}, bf16[144,256]{1,0:T(8,128)(2,1)S(1)}, u32[]{:S(2)}, u32[]{:S(2)}) collective-permute-start(bf16[144,256]{1,0:T(8,128)(2,1)} %get-tuple-element.12.own_ref), channel_id=1, source_target_pairs={{0,16},{8,504},{16,32},{24,8},{32,48},{40,24},{48,64},{56,40},{64,... | collective-permute-start | bytes 221192 | tf_op jit(solution)/shard_map/ppermute | solution.py:198
  26.3 12.1 %collective-permute-done.1.in_ref = bf16[144,256]{1,0:T(8,128)(2,1)S(1)} collective-permute-done((bf16[144,256]{1,0:T(8,128)(2,1)}, bf16[144,256]{1,0:T(8,128)(2,1)S(1)}, u32[]{:S(2)}, u32[]{:S(2)}) %collective-permute-start.1) | collective-permute-done | bytes 73760 | tf_op jit(solution)/shard_map/ppermute | solution.py:198
  38.4 0.0 copy-start.1
  38.4 0.6 copy-done.1
  39.0 1.7 combine_maps.1
  40.8 1.9 collective-permute-start.2
  42.7 1.9 collective-permute-start.3
  44.6 6.9 %collective-permute-done.3.far_ref = bf16[144,128]{1,0:T(8,128)(2,1)S(1)} collective-permute-done((bf16[144,128]{1,0:T(8,128)(2,1)}, bf16[144,128]{1,0:T(8,128)(2,1)S(1)}, u32[]{:S(2)}, u32[]{:S(2)}) %collective-permute-start.3) | collective-permute-done | bytes 36896 | tf_op jit(solution)/shard_map/ppermute | solution.py:198
  51.6 0.0 copy-start.5
  51.6 0.0 collective-permute-done.2.near_ref
  51.6 0.0 copy-start.2
  51.6 0.6 copy-done.5
  52.2 0.0 copy-done.2
  52.2 2.0 apply_state.1
  54.1 6.1 %collective-permute-start.4 = (bf16[128,128]{1,0:T(8,128)(2,1)}, bf16[128,128]{1,0:T(8,128)(2,1)S(1)}, u32[]{:S(2)}, u32[]{:S(2)}) collective-permute-start(bf16[128,128]{1,0:T(8,128)(2,1)} %get-tuple-element.18), channel_id=1, source_target_pairs={{0,8},{8,0},{16,24},{24,16},{32,40},{40,32},{48,56},{56,48},{64,72... | collective-permute-start | bytes 98312 | tf_op jit(solution)/shard_map/ppermute | solution.py:194
  60.3 1.5 collective-permute-done.4.in_ref
  61.8 0.0 copy-start.6
  61.8 0.6 copy-done.6
  62.4 2.3 finish_mixer.1
  64.7 0.0 copy-start.7
  64.7 9.7 %all-to-all-start = ((bf16[8,128,256]{2,1,0:T(8,128)(2,1)}), bf16[8,128,256]{2,1,0:T(8,128)(2,1)S(1)}, u32[]{:S(2)}, u32[]{:S(2)}) async-start(bf16[8,128,256]{2,1,0:T(8,128)(2,1)} %finish_mixer.1), calls=%async_computation | async-start | bytes 1048576 | tf_op jit(solution)/shard_map/all_to_all | solution.py:283
  74.4 0.0 all-gather.3.cloned.1.call-start
  74.4 9.3 %all-to-all-done = bf16[8,128,256]{2,1,0:T(8,128)(2,1)S(1)} async-done(((bf16[8,128,256]{2,1,0:T(8,128)(2,1)}), bf16[8,128,256]{2,1,0:T(8,128)(2,1)S(1)}, u32[]{:S(2)}, u32[]{:S(2)}) %all-to-all-start) | async-done | bytes 524320 | tf_op jit(solution)/shard_map/all_to_all | solution.py:283
  83.7 0.1 convert_reduce_fusion.1
  83.8 0.9 fusion.26
  84.7 3.6 %collective-permute-start.5 = (bf16[128,256]{1,0:T(8,128)(2,1)S(1)}, bf16[128,256]{1,0:T(8,128)(2,1)S(1)}, u32[]{:S(2)}, u32[]{:S(2)}) collective-permute-start(bf16[128,256]{1,0:T(8,128)(2,1)S(1)} %fusion.26), channel_id=1, source_target_pairs={{0,8},{8,0},{16,24},{24,16},{32,40},{40,32},{48,56},{56,48},{64,72... | collective-permute-start | bytes 196616 | tf_op jit(solution)/shard_map/ppermute | solution.py:194
  88.3 1.6 collective-permute-done.5
  89.9 0.7 pad_maximum_fusion
  90.6 0.0 all-gather.3.cloned.1.call-update
  90.6 0.0 all-gather.5.cloned.1.call-start
  90.7 0.0 copy-done.3
  90.7 0.0 copy-done.4
  90.8 3.4 %collective-permute-start.6 = (bf16[32,1024]{1,0:T(8,128)(2,1)S(1)}, bf16[32,1024]{1,0:T(8,128)(2,1)S(1)}, u32[]{:S(2)}, u32[]{:S(2)}) collective-permute-start(bf16[32,1024]{1,0:T(8,128)(2,1)S(1)} %pad_maximum_fusion.3), channel_id=1, source_target_pairs={{0,8},{8,0},{16,24},{24,16},{32,40},{40,32},{48,56},{56,48},{64,72... | collective-permute-start | bytes 196616 | tf_op jit(solution)/shard_map/ppermute | solution.py:194
  94.1 1.6 collective-permute-done.6
  95.8 0.7 pad_maximum_fusion.1
  96.5 0.0 all-gather.5.cloned.1.call-update
  96.5 16.4 %all-gather.3.cloned.1.call-done = bf16[256,2048]{1,0:T(8,128)(2,1)} async-done(((bf16[256,256]{1,0:T(8,128)(2,1)}), bf16[256,2048]{1,0:T(8,128)(2,1)}) %all-gather.3.cloned.1.call-update) | async-done | bytes 1048592 | tf_op jit(solution)/shard_map/all_gather | solution.py:289
  112.9 1.5 fusion
  114.4 102.3 %all-gather.5.cloned.1.call-done = bf16[2048,1024]{1,0:T(8,128)(2,1)} async-done(((bf16[64,1024]{1,0:T(8,128)(2,1)}), bf16[2048,1024]{1,0:T(8,128)(2,1)}) %all-gather.5.cloned.1.call-update) | async-done | bytes 4194320 | tf_op jit(solution)/shard_map/all_gather | solution.py:230
  216.7 0.0 copy-done.7
  216.7 3.9 %convolution_convert_fusion = bf16[256,2048]{1,0:T(8,128)(2,1)S(1)} fusion(bf16[2048,1024]{1,0:T(8,128)(2,1)} %all-gather.5.cloned.1.call-done, bf16[256,2048]{1,0:T(8,128)(2,1)} %all-gather.3.cloned.1.call-done, f32[2048]{0:T(1024)S(1)} %copy-done.7, f32[256]{0:T(256)S(1)} %add_rsqrt_fusion), kind=kOutput, calls=%fused_computation.2 | convolution fusion | flops 1076756480 | bytes 6300672 | tf_op jit(solution)/shard_map/dot_general | solution.py:294
  220.6 0.1 copy.18
  220.7 22.5 %all_to_all.10 = bf16[8,256,256]{2,1,0:T(8,128)(2,1)S(1)} all-to-all(bf16[8,256,256]{2,1,0:T(8,128)(2,1)S(1)} %bitcast.17), channel_id=1, replica_groups=mesh['sp_0'=8,'sp_1'=4,'pair'=2,'tp'=8] {'tp'}, dimensions={0} | all-to-all | bytes 2097152 | tf_op jit(solution)/shard_map/all_to_all | solution.py:296
  243.2 0.1 convert_reduce_fusion
  243.4 1.9 collective-permute-start.7
  245.3 3.1 %collective-permute-done.7 = bf16[128,256]{1,0:T(8,128)(2,1)S(1)} collective-permute-done((bf16[128,256]{1,0:T(8,128)(2,1)S(1)}, bf16[128,256]{1,0:T(8,128)(2,1)S(1)}, u32[]{:S(2)}, u32[]{:S(2)}) %collective-permute-start.7) | collective-permute-done | bytes 65568 | tf_op jit(solution)/shard_map/ppermute | solution.py:194
  248.4 1.5 fusion.25
  (6 shorter events, 0.1 us)
Async XLA Ops:
  8.0 6.3 %collective-permute-start = (bf16[136,384]{1,0:T(8,128)(2,1)}, bf16[136,384]{1,0:T(8,128)(2,1)S(1)}, u32[]{:S(2)}, u32[]{:S(2)}) collective-permute-start(bf16[136,384]{1,0:T(8,128)(2,1)} %pack_inputs.1.own_ref), channel_id=1, source_target_pairs={{0,8},{8,0},{16,24},{24,16},{32,40},{40,32},{48,56},{56,48},{64,72... | collective-permute-start | bytes 313352 | tf_op jit(solution)/shard_map/ppermute | solution.py:194
  14.3 0.6 copy-start
  21.8 68.9 %copy-start.3 = (bf16[32,1024]{1,0:T(8,128)(2,1)S(1)}, bf16[32,1024]{1,0:T(8,128)(2,1)}, u32[]{:S(2)}) copy-start(bf16[32,1024]{1,0:T(8,128)(2,1)} %param.26) | copy-start | bytes 196612
  21.8 68.9 %copy-start.4 = (bf16[1024,32]{0,1:T(8,128)(2,1)S(1)}, bf16[1024,32]{0,1:T(8,128)(2,1)}, u32[]{:S(2)}) copy-start(bf16[1024,32]{0,1:T(8,128)(2,1)} %param.27) | copy-start | bytes 196612
  21.8 16.6 %collective-permute-start.1 = (bf16[144,256]{1,0:T(8,128)(2,1)}, bf16[144,256]{1,0:T(8,128)(2,1)S(1)}, u32[]{:S(2)}, u32[]{:S(2)}) collective-permute-start(bf16[144,256]{1,0:T(8,128)(2,1)} %get-tuple-element.12.own_ref), channel_id=1, source_target_pairs={{0,16},{8,504},{16,32},{24,8},{32,48},{40,24},{48,64},{56,40},{64,... | collective-permute-start | bytes 221192 | tf_op jit(solution)/shard_map/ppermute | solution.py:198
  38.4 0.6 copy-start.1
  40.8 10.8 %collective-permute-start.2 = (bf16[144,256]{1,0:T(8,128)(2,1)}, bf16[144,256]{1,0:T(8,128)(2,1)S(1)}, u32[]{:S(2)}, u32[]{:S(2)}) collective-permute-start(bf16[144,256]{1,0:T(8,128)(2,1)} %get-tuple-element.13), channel_id=1, source_target_pairs={{0,16},{8,504},{16,32},{24,8},{32,48},{40,24},{48,64},{56,40},{64,... | collective-permute-start | bytes 221192 | tf_op jit(solution)/shard_map/ppermute | solution.py:198
  42.7 8.9 %collective-permute-start.3 = (bf16[144,128]{1,0:T(8,128)(2,1)}, bf16[144,128]{1,0:T(8,128)(2,1)S(1)}, u32[]{:S(2)}, u32[]{:S(2)}) collective-permute-start(bf16[144,128]{1,0:T(8,128)(2,1)} %get-tuple-element.14), channel_id=1, source_target_pairs={{0,48},{8,472},{16,64},{24,488},{32,80},{40,504},{48,96},{56,8},{6... | collective-permute-start | bytes 110600 | tf_op jit(solution)/shard_map/ppermute | solution.py:198
  51.6 0.6 copy-start.5
  51.6 0.6 copy-start.2
  54.1 7.6 %collective-permute-start.4 = (bf16[128,128]{1,0:T(8,128)(2,1)}, bf16[128,128]{1,0:T(8,128)(2,1)S(1)}, u32[]{:S(2)}, u32[]{:S(2)}) collective-permute-start(bf16[128,128]{1,0:T(8,128)(2,1)} %get-tuple-element.18), channel_id=1, source_target_pairs={{0,8},{8,0},{16,24},{24,16},{32,40},{40,32},{48,56},{56,48},{64,72... | collective-permute-start | bytes 98312 | tf_op jit(solution)/shard_map/ppermute | solution.py:194
  61.8 0.6 copy-start.6
  64.7 152.1 %copy-start.7 = (f32[2048]{0:T(1024)S(1)}, f32[2048]{0:T(1024)}, u32[]{:S(2)}) copy-start(f32[2048]{0:T(1024)} %param.25) | copy-start | bytes 24580
  64.7 19.0 %all-to-all-start = ((bf16[8,128,256]{2,1,0:T(8,128)(2,1)}), bf16[8,128,256]{2,1,0:T(8,128)(2,1)S(1)}, u32[]{:S(2)}, u32[]{:S(2)}) async-start(bf16[8,128,256]{2,1,0:T(8,128)(2,1)} %finish_mixer.1), calls=%async_computation | async-start | bytes 1048576 | tf_op jit(solution)/shard_map/all_to_all | solution.py:283
  74.4 38.5 %all-gather.3.cloned.1.call-start = ((), (), s32[]{:S(2)}) async-start(), calls=%async_computation.2 | async-start | bytes 1179648 | tf_op jit(solution)/shard_map/all_gather | solution.py:289
  84.7 5.3 %collective-permute-start.5 = (bf16[128,256]{1,0:T(8,128)(2,1)S(1)}, bf16[128,256]{1,0:T(8,128)(2,1)S(1)}, u32[]{:S(2)}, u32[]{:S(2)}) collective-permute-start(bf16[128,256]{1,0:T(8,128)(2,1)S(1)} %fusion.26), channel_id=1, source_target_pairs={{0,8},{8,0},{16,24},{24,16},{32,40},{40,32},{48,56},{56,48},{64,72... | collective-permute-start | bytes 196616 | tf_op jit(solution)/shard_map/ppermute | solution.py:194
  90.6 126.1 %all-gather.5.cloned.1.call-start = ((), (), s32[]{:S(2)}) async-start(), calls=%async_computation.3 | async-start | bytes 4325376 | tf_op jit(solution)/shard_map/all_gather | solution.py:230
  90.8 5.0 %collective-permute-start.6 = (bf16[32,1024]{1,0:T(8,128)(2,1)S(1)}, bf16[32,1024]{1,0:T(8,128)(2,1)S(1)}, u32[]{:S(2)}, u32[]{:S(2)}) collective-permute-start(bf16[32,1024]{1,0:T(8,128)(2,1)S(1)} %pad_maximum_fusion.3), channel_id=1, source_target_pairs={{0,8},{8,0},{16,24},{24,16},{32,40},{40,32},{48,56},{56,48},{64,72... | collective-permute-start | bytes 196616 | tf_op jit(solution)/shard_map/ppermute | solution.py:194
  243.4 5.0 %collective-permute-start.7 = (bf16[128,256]{1,0:T(8,128)(2,1)S(1)}, bf16[128,256]{1,0:T(8,128)(2,1)S(1)}, u32[]{:S(2)}, u32[]{:S(2)}) collective-permute-start(bf16[128,256]{1,0:T(8,128)(2,1)S(1)} %slice.39), channel_id=1, source_target_pairs={{0,8},{8,0},{16,24},{24,16},{32,40},{40,32},{48,56},{56,48},{64,72... | collective-permute-start | bytes 196616 | tf_op jit(solution)/shard_map/ppermute | solution.py:194
Sparse Core Ops, SparseCore 0:
  90.7 22.0 all-gather.2
  116.0 100.6 all-gather.4

commit v4 on v3

--- a/solution.py
+++ b/solution.py
@@ -213,28 +213,10 @@
         sample_membership.reshape(1, length),
     )
     pal_data = swapped(data)
-    side = lax.axis_index("pair")
-    half = widen_projection_weights.shape[1] // 2
-
-    def halves(which):
-        return jnp.concatenate(
-            [
-                lax.dynamic_slice_in_dim(array, which * half, half, 1)
-                for array in (widen_projection_weights, shrink_projection_weights.T)
-            ],
-            axis=1,
-        )
-
-    kept_half = halves(side)
-    given_half = swapped(halves(1 - side))
+    up_width = widen_projection_weights.shape[1]
     weights = lax.all_gather(
-        jnp.concatenate(
-            [
-                jnp.where(side == 0, kept_half, given_half),
-                jnp.where(side == 0, given_half, kept_half),
-            ]
-        ),
-        SP[:2],
+        jnp.concatenate([widen_projection_weights, shrink_projection_weights.T], axis=1),
+        SP,
         axis=0,
         tiled=True,
     )
@@ -284,19 +266,15 @@
     own_residual = lax.dynamic_slice_in_dim(skip_path_inputs, col_start, col_count, 1).astype(
         F32
     ) + jnp.sum(parts.astype(F32), axis=0)
-    sent_residual = own_residual.astype(BF16)
-    both = jnp.concatenate([sent_residual, swapped(sent_residual)])
-    residual = lax.all_gather(both, "tp", axis=1, tiled=True).astype(F32)
+    residual = lax.all_gather(own_residual.astype(BF16), "tp", axis=1, tiled=True).astype(F32)
     squares = jnp.mean(residual * residual, axis=1, keepdims=True)
     normed = (residual * lax.rsqrt(squares + EPSILON) * dense_block_scaling).astype(BF16)
-    raised = jnp.dot(normed, weights[:, :half], preferred_element_type=F32)
+    raised = jnp.dot(normed, weights[:, :up_width], preferred_element_type=F32)
     active = jnp.square(jax.nn.relu(raised)).astype(BF16)
-    lowered = lax.dot_general(active, weights[:, half:], NT, preferred_element_type=F32)
-    turned = jnp.moveaxis(lowered.astype(BF16).reshape(2 * length, -1, col_count), 1, 0)
+    lowered = lax.dot_general(active, weights[:, up_width:], NT, preferred_element_type=F32)
+    turned = jnp.moveaxis(lowered.astype(BF16).reshape(length, -1, col_count), 1, 0)
     pieces = lax.all_to_all(turned, "tp", 0, 0, tiled=True)
-    sums = jnp.sum(pieces.astype(F32), axis=0)
-    given = swapped(sums[length:].astype(BF16)).astype(F32)
-    return (own_residual + sums[:length] + given).astype(BF16)
+    return (own_residual + jnp.sum(pieces.astype(F32), axis=0)).astype(BF16)
 
 
 def solution(mesh):

time: 258 us -> 144 us (0.56)
  waiting for transfers between devices: 157 us -> 47.7 us
  starting transfers between devices: 37.1 us -> 27.3 us
  blocking collectives: 22.5 us -> 28.2 us
    all_gather x2 -> x1, waiting for transfers between devices: 119 us -> 14.9 us  [shards(): lax.all_gather(jnp.concatenate([widen_projection_weights, shrink_projecti...]
    all_gather x0 -> x1, blocking collectives: none -> 13.9 us  [shards(): lax.all_gather(own_residual.astype(BF16), 'tp', axis=1, tiled=True)]
    ppermute x5 -> x2, starting transfers between devices: 19 us -> 9.82 us  [swapped(): return lax.ppermute(array, SP, [(i, i ^ 1) for i in range(count)])]
    all_to_all x1, blocking collectives: 22.5 us -> 14.3 us  [shards(): pieces = lax.all_to_all(turned, 'tp', 0, 0, tiled=True)]
    ppermute x5 -> x2, waiting for transfers between devices: 10.1 us -> 3.77 us  [swapped(): return lax.ppermute(array, SP, [(i, i ^ 1) for i in range(count)])]
  transfers between devices with their start and end apart: 11 -> 7, of which waited for: 10 -> 6; matrix products, arithmetic and copies ran while one was open for 1% -> 1% of each run, Pallas kernels for 0% -> 10%
where the time goes in v4:
time: 144 us
  waiting for transfers between devices  47.7 us (33%)
  blocking collectives  28.2 us (20%)
  starting transfers between devices  27.3 us (19%)
  Pallas kernels  14.4 us (10%)
  between operations  13.5 us (9%)
  matrix products  5.61 us (4%)
  other arithmetic  4.23 us (3%)
  local copies, waits for them, and re-layouts  2.54 us (2%)
    ppermute x3, waiting for transfers between devices, passed(): lax.ppermute(array, SP, [(i, (i + ways[i % 2]) % count) for i in range(co...  19.7 us
    all_gather x1, waiting for transfers between devices, shards(): lax.all_gather(jnp.concatenate([widen_projection_weights, shrink_projecti...  14.9 us
    all_to_all x1, blocking collectives, shards(): pieces = lax.all_to_all(turned, 'tp', 0, 0, tiled=True)  14.3 us
    all_gather x1, blocking collectives, shards(): lax.all_gather(own_residual.astype(BF16), 'tp', axis=1, tiled=True)  13.9 us
    ppermute x2, starting transfers between devices, swapped(): return lax.ppermute(array, SP, [(i, i ^ 1) for i in range(count)])  9.82 us
    all_to_all x1, waiting for transfers between devices, shards(): parts = lax.all_to_all(head_terms, 'tp', 0, 0, tiled=True)  9.35 us
    all_to_all x1, starting transfers between devices, shards(): parts = lax.all_to_all(head_terms, 'tp', 0, 0, tiled=True)  9.33 us
    ppermute x3, starting transfers between devices, passed(): lax.ppermute(array, SP, [(i, (i + ways[i % 2]) % count) for i in range(co...  8.19 us
  transfers between devices with their start and end apart: 7, of which 6 were waited for; matrix products, arithmetic and copies ran while one was open for 1% of the time, Pallas kernels for 10%

profile of v4, /device:TPU:1, one launch (start us, length us, event | category | flops | bytes accessed | tf_op | source)
XLA Modules:
  0.0 143.6 jit_solution(11483121077098035839)
XLA Ops:
  6.5 0.0 all-gather.2.cloned.1.call-start
  6.5 1.5 %pad_maximum_fusion = bf16[32,2048]{1,0:T(8,128)(2,1)} fusion(bf16[32,1024]{1,0:T(8,128)(2,1)} %bitcast.16, bf16[32,1024]{1,0:T(8,128)(2,1)} %param.26), kind=kLoop, calls=%fused_computation.19 | loop fusion | flops 262144 | bytes 262144 | tf_op jit(solution)/shard_map/concatenate | solution.py:218
  8.1 0.0 all-gather.2.cloned.1.call-update
  8.1 1.5 %pack_inputs.1.own_ref = bf16[136,384]{1,0:T(8,128)(2,1)} custom-call(bf16[128,128]{1,0:T(8,128)(2,1)} %q_ref.1, bf16[128,128]{1,0:T(8,128)(2,1)} %k_ref.1, bf16[128,128]{1,0:T(8,128)(2,1)} %v_ref.1, f32[2,128]{1,0:T(2,128)} %bitcast.17, f32[2,128]{1,0:T(2,128)} %bitcast.18, f32[2,128]{1,0:T(2,128)} %bitcast.19, s32[1,128]{1,0:T(1,128)} %bitcast.20), custom_call_target="tpu_custom_call" | custom-call | tf_op jit(solution)/shard_map/pack_inputs/pallas_call | solution.py:200
  9.6 4.0 %collective-permute-start = (bf16[136,384]{1,0:T(8,128)(2,1)}, bf16[136,384]{1,0:T(8,128)(2,1)S(1)}, u32[]{:S(2)}, u32[]{:S(2)}) collective-permute-start(bf16[136,384]{1,0:T(8,128)(2,1)} %pack_inputs.1.own_ref), channel_id=1, source_target_pairs={{0,8},{8,0},{16,24},{24,16},{32,40},{40,32},{48,56},{56,48},{64,72... | collective-permute-start | bytes 313352 | tf_op jit(solution)/shard_map/ppermute | solution.py:194
  13.6 2.3 %collective-permute-done.pal_ref = bf16[136,384]{1,0:T(8,128)(2,1)S(1)} collective-permute-done((bf16[136,384]{1,0:T(8,128)(2,1)}, bf16[136,384]{1,0:T(8,128)(2,1)S(1)}, u32[]{:S(2)}, u32[]{:S(2)}) %collective-permute-start) | collective-permute-done | bytes 104480 | tf_op jit(solution)/shard_map/ppermute | solution.py:194
  15.9 0.0 copy-start
  15.9 0.6 copy-done
  16.5 6.9 %local_maps.1 = (bf16[144,256]{1,0:T(8,128)(2,1)}, bf16[2,128,128]{2,1,0:T(8,128)(2,1)}, f32[2,128,128]{2,1,0:T(8,128)}) custom-call(bf16[136,384]{1,0:T(8,128)(2,1)} %pack_inputs.1.own_ref, bf16[136,384]{1,0:T(8,128)(2,1)} %copy-done, f32[1,2]{1,0:T(1,128)} %bitcast.21), custom_call_target="tpu_custom_call" | custom-call | tf_op jit(solution)/shard_map/local_maps/pallas_call | solution.py:224
  23.4 4.4 %collective-permute-start.1 = (bf16[144,256]{1,0:T(8,128)(2,1)}, bf16[144,256]{1,0:T(8,128)(2,1)S(1)}, u32[]{:S(2)}, u32[]{:S(2)}) collective-permute-start(bf16[144,256]{1,0:T(8,128)(2,1)} %get-tuple-element.12.own_ref), channel_id=1, source_target_pairs={{0,16},{8,504},{16,32},{24,8},{32,48},{40,24},{48,64},{56,40},{64,... | collective-permute-start | bytes 221192 | tf_op jit(solution)/shard_map/ppermute | solution.py:198
  27.8 12.9 %collective-permute-done.1.in_ref = bf16[144,256]{1,0:T(8,128)(2,1)S(1)} collective-permute-done((bf16[144,256]{1,0:T(8,128)(2,1)}, bf16[144,256]{1,0:T(8,128)(2,1)S(1)}, u32[]{:S(2)}, u32[]{:S(2)}) %collective-permute-start.1) | collective-permute-done | bytes 73760 | tf_op jit(solution)/shard_map/ppermute | solution.py:198
  40.6 0.0 copy-start.1
  40.7 0.6 copy-done.1
  41.3 1.7 %combine_maps.1 = (bf16[144,256]{1,0:T(8,128)(2,1)}, bf16[144,128]{1,0:T(8,128)(2,1)}) custom-call(bf16[144,256]{1,0:T(8,128)(2,1)} %get-tuple-element.12.own_ref, bf16[144,256]{1,0:T(8,128)(2,1)} %copy-done.1), custom_call_target="tpu_custom_call" | custom-call | tf_op jit(solution)/shard_map/combine_maps/pallas_call | solution.py:235
  43.0 1.9 %collective-permute-start.2 = (bf16[144,256]{1,0:T(8,128)(2,1)}, bf16[144,256]{1,0:T(8,128)(2,1)S(1)}, u32[]{:S(2)}, u32[]{:S(2)}) collective-permute-start(bf16[144,256]{1,0:T(8,128)(2,1)} %get-tuple-element.13), channel_id=1, source_target_pairs={{0,16},{8,504},{16,32},{24,8},{32,48},{40,24},{48,64},{56,40},{64,... | collective-permute-start | bytes 221192 | tf_op jit(solution)/shard_map/ppermute | solution.py:198
  44.9 1.9 %collective-permute-start.3 = (bf16[144,128]{1,0:T(8,128)(2,1)}, bf16[144,128]{1,0:T(8,128)(2,1)S(1)}, u32[]{:S(2)}, u32[]{:S(2)}) collective-permute-start(bf16[144,128]{1,0:T(8,128)(2,1)} %get-tuple-element.14), channel_id=1, source_target_pairs={{0,48},{8,472},{16,64},{24,488},{32,80},{40,504},{48,96},{56,8},{6... | collective-permute-start | bytes 110600 | tf_op jit(solution)/shard_map/ppermute | solution.py:198
  46.9 6.8 %collective-permute-done.3.far_ref = bf16[144,128]{1,0:T(8,128)(2,1)S(1)} collective-permute-done((bf16[144,128]{1,0:T(8,128)(2,1)}, bf16[144,128]{1,0:T(8,128)(2,1)S(1)}, u32[]{:S(2)}, u32[]{:S(2)}) %collective-permute-start.3) | collective-permute-done | bytes 36896 | tf_op jit(solution)/shard_map/ppermute | solution.py:198
  53.7 0.0 copy-start.3
  53.7 0.0 collective-permute-done.2.near_ref
  53.7 0.0 copy-start.2
  53.7 0.6 copy-done.3
  54.3 0.0 copy-done.2
  54.3 2.0 %apply_state.1 = (f32[128,128]{1,0:T(8,128)}, bf16[128,128]{1,0:T(8,128)(2,1)}) custom-call(bf16[144,256]{1,0:T(8,128)(2,1)} %get-tuple-element.12.own_ref, bf16[144,256]{1,0:T(8,128)(2,1)} %copy-done.2, bf16[144,128]{1,0:T(8,128)(2,1)} %copy-done.3, bf16[2,128,128]{2,1,0:T(8,128)(2,1)} %get-tuple-element.15.read_ref, f32[2,128,128]{2,1,0:T(8,128)} %get-tuple-element.16.base_ref), custom_call_target="tpu_custom_call" | custom-call | tf_op jit(solution)/shard_map/apply_state/pallas_call | solution.py:245
  56.3 5.8 %collective-permute-start.4 = (bf16[128,128]{1,0:T(8,128)(2,1)}, bf16[128,128]{1,0:T(8,128)(2,1)S(1)}, u32[]{:S(2)}, u32[]{:S(2)}) collective-permute-start(bf16[128,128]{1,0:T(8,128)(2,1)} %get-tuple-element.18), channel_id=1, source_target_pairs={{0,8},{8,0},{16,24},{24,16},{32,40},{40,32},{48,56},{56,48},{64,72... | collective-permute-start | bytes 98312 | tf_op jit(solution)/shard_map/ppermute | solution.py:194
  62.1 1.5 %collective-permute-done.4.in_ref = bf16[128,128]{1,0:T(8,128)(2,1)S(1)} collective-permute-done((bf16[128,128]{1,0:T(8,128)(2,1)}, bf16[128,128]{1,0:T(8,128)(2,1)S(1)}, u32[]{:S(2)}, u32[]{:S(2)}) %collective-permute-start.4) | collective-permute-done | bytes 32800 | tf_op jit(solution)/shard_map/ppermute | solution.py:194
  63.6 0.0 copy-start.4
  63.6 0.6 copy-done.4
  64.2 2.3 %finish_mixer.1 = bf16[8,128,256]{2,1,0:T(8,128)(2,1)} custom-call(f32[128,128]{1,0:T(8,128)} %get-tuple-element.17.mine_ref, bf16[128,128]{1,0:T(8,128)(2,1)} %copy-done.4, f32[1,128]{1,0:T(1,128)} %bitcast.22, bf16[128,2048]{1,0:T(8,128)(2,1)} %exit_ref.1), custom_call_target="tpu_custom_call" | custom-call | tf_op jit(solution)/shard_map/finish_mixer/pallas_call | solution.py:255
  66.6 9.3 %all-to-all-start = ((bf16[8,128,256]{2,1,0:T(8,128)(2,1)}), bf16[8,128,256]{2,1,0:T(8,128)(2,1)S(1)}, u32[]{:S(2)}, u32[]{:S(2)}) async-start(bf16[8,128,256]{2,1,0:T(8,128)(2,1)} %finish_mixer.1), calls=%async_computation | async-start | bytes 1048576 | tf_op jit(solution)/shard_map/all_to_all | solution.py:265
  75.9 9.3 %all-to-all-done = bf16[8,128,256]{2,1,0:T(8,128)(2,1)S(1)} async-done(((bf16[8,128,256]{2,1,0:T(8,128)(2,1)}), bf16[8,128,256]{2,1,0:T(8,128)(2,1)S(1)}, u32[]{:S(2)}, u32[]{:S(2)}) %all-to-all-start) | async-done | bytes 524320 | tf_op jit(solution)/shard_map/all_to_all | solution.py:265
  85.2 0.1 convert_reduce_fusion.1
  85.3 0.9 fusion.28
  86.2 13.9 %all_gather.6 = bf16[128,2048]{1,0:T(8,128)(2,1)S(1)} all-gather(bf16[128,256]{1,0:T(8,128)(2,1)S(1)} %fusion.28), channel_id=1, replica_groups=mesh['sp_0'=8,'sp_1'=4,'pair'=2,'tp'=8] {'tp'}, dimensions={1}, use_global_device_ids=true | all-gather | bytes 589824 | tf_op jit(solution)/shard_map/all_gather | solution.py:269
  100.1 0.2 fusion.18
  100.3 14.9 %all-gather.2.cloned.1.call-done = bf16[2048,2048]{1,0:T(8,128)(2,1)} async-done(((bf16[32,2048]{1,0:T(8,128)(2,1)}), bf16[2048,2048]{1,0:T(8,128)(2,1)}) %all-gather.2.cloned.1.call-update) | async-done | bytes 8388624 | tf_op jit(solution)/shard_map/all_gather | solution.py:217
  115.2 5.6 %fusion.4 = bf16[128,2048]{1,0:T(8,128)(2,1)S(1)} fusion(bf16[2048,2048]{1,0:T(8,128)(2,1)} %all-gather.2.cloned.1.call-done, bf16[128,2048]{1,0:T(8,128)(2,1)S(1)} %all_gather.6, f32[2048]{0:T(1024)} %param.25, f32[128]{0:T(128)S(1)} %add_rsqrt_fusion), kind=kOutput, calls=%fused_computation.4 | convolution fusion | flops 1075445760 | bytes 9445888 | tf_op jit(solution)/shard_map/dot_general | solution.py:274
  120.8 14.3 %all_to_all.10 = bf16[8,128,256]{2,1,0:T(8,128)(2,1)S(1)} all-to-all(bf16[8,128,256]{2,1,0:T(8,128)(2,1)S(1)} %bitcast.14), channel_id=1, replica_groups=mesh['sp_0'=8,'sp_1'=4,'pair'=2,'tp'=8] {'tp'}, dimensions={0} | all-to-all | bytes 1048576 | tf_op jit(solution)/shard_map/all_to_all | solution.py:276
  135.1 0.1 convert_reduce_fusion
  135.2 1.5 %add_convert_fusion = bf16[128,256]{1,0:T(8,128)(2,1)} fusion(f32[128,256]{1,0:T(8,128)S(1)} %convert_reduce_fusion, f32[128,256]{1,0:T(8,128)S(1)} %convert_reduce_fusion.1, bf16[128,2048]{1,0:T(8,128)(2,1)} %param.14, s32[]{:T(128)S(6)} %select_n.3), kind=kLoop, calls=%fused_computation.20 | loop fusion | flops 131072 | bytes 393220 | tf_op jit(solution)/shard_map/convert_element_type | solution.py:277
  (2 shorter events, 0.0 us)
Async XLA Ops:
  6.5 108.6 %all-gather.2.cloned.1.call-start = ((), (), s32[]{:S(2)}) async-start(), calls=%async_computation.2 | async-start | bytes 8519680 | tf_op jit(solution)/shard_map/all_gather | solution.py:217
  9.6 6.3 %collective-permute-start = (bf16[136,384]{1,0:T(8,128)(2,1)}, bf16[136,384]{1,0:T(8,128)(2,1)S(1)}, u32[]{:S(2)}, u32[]{:S(2)}) collective-permute-start(bf16[136,384]{1,0:T(8,128)(2,1)} %pack_inputs.1.own_ref), channel_id=1, source_target_pairs={{0,8},{8,0},{16,24},{24,16},{32,40},{40,32},{48,56},{56,48},{64,72... | collective-permute-start | bytes 313352 | tf_op jit(solution)/shard_map/ppermute | solution.py:194
  15.9 0.6 copy-start
  23.4 17.3 %collective-permute-start.1 = (bf16[144,256]{1,0:T(8,128)(2,1)}, bf16[144,256]{1,0:T(8,128)(2,1)S(1)}, u32[]{:S(2)}, u32[]{:S(2)}) collective-permute-start(bf16[144,256]{1,0:T(8,128)(2,1)} %get-tuple-element.12.own_ref), channel_id=1, source_target_pairs={{0,16},{8,504},{16,32},{24,8},{32,48},{40,24},{48,64},{56,40},{64,... | collective-permute-start | bytes 221192 | tf_op jit(solution)/shard_map/ppermute | solution.py:198
  40.6 0.6 copy-start.1
  43.0 10.7 %collective-permute-start.2 = (bf16[144,256]{1,0:T(8,128)(2,1)}, bf16[144,256]{1,0:T(8,128)(2,1)S(1)}, u32[]{:S(2)}, u32[]{:S(2)}) collective-permute-start(bf16[144,256]{1,0:T(8,128)(2,1)} %get-tuple-element.13), channel_id=1, source_target_pairs={{0,16},{8,504},{16,32},{24,8},{32,48},{40,24},{48,64},{56,40},{64,... | collective-permute-start | bytes 221192 | tf_op jit(solution)/shard_map/ppermute | solution.py:198
  44.9 8.8 %collective-permute-start.3 = (bf16[144,128]{1,0:T(8,128)(2,1)}, bf16[144,128]{1,0:T(8,128)(2,1)S(1)}, u32[]{:S(2)}, u32[]{:S(2)}) collective-permute-start(bf16[144,128]{1,0:T(8,128)(2,1)} %get-tuple-element.14), channel_id=1, source_target_pairs={{0,48},{8,472},{16,64},{24,488},{32,80},{40,504},{48,96},{56,8},{6... | collective-permute-start | bytes 110600 | tf_op jit(solution)/shard_map/ppermute | solution.py:198
  53.7 0.6 copy-start.3
  53.7 0.6 copy-start.2
  56.3 7.3 %collective-permute-start.4 = (bf16[128,128]{1,0:T(8,128)(2,1)}, bf16[128,128]{1,0:T(8,128)(2,1)S(1)}, u32[]{:S(2)}, u32[]{:S(2)}) collective-permute-start(bf16[128,128]{1,0:T(8,128)(2,1)} %get-tuple-element.18), channel_id=1, source_target_pairs={{0,8},{8,0},{16,24},{24,16},{32,40},{40,32},{48,56},{56,48},{64,72... | collective-permute-start | bytes 98312 | tf_op jit(solution)/shard_map/ppermute | solution.py:194
  63.6 0.6 copy-start.4
  66.6 18.7 %all-to-all-start = ((bf16[8,128,256]{2,1,0:T(8,128)(2,1)}), bf16[8,128,256]{2,1,0:T(8,128)(2,1)S(1)}, u32[]{:S(2)}, u32[]{:S(2)}) async-start(bf16[8,128,256]{2,1,0:T(8,128)(2,1)} %finish_mixer.1), calls=%async_computation | async-start | bytes 1048576 | tf_op jit(solution)/shard_map/all_to_all | solution.py:265
Sparse Core Ops, SparseCore 0:
  10.4 104.7 all-gather.1

commit v5 on v4

--- a/solution.py
+++ b/solution.py
@@ -105,11 +105,11 @@
         tail = jnp.exp(jnp.minimum(total - running_row, 0.0))
         faded = jnp.transpose(kf) * (k_scale_row * tail * ending_row)
         kept = jnp.exp(total) * (docs_first == docs_last).astype(F32)
-        step = jnp.where(eye, kept, 0.0) - mm(faded, drop)
-        shift = mm(faded, update)
+        step = jnp.where(eye, kept, 0.0) - mm3(faded, drop)
+        shift = mm3(faded, update)
         scores = scored * spread
-        read = qf * (q_scale * jnp.exp(running) * linked) - mm(scores, drop)
-        return step, shift, read, mm(scores, update), docs_first, docs_last
+        read = qf * (q_scale * jnp.exp(running) * linked) - mm3(scores, drop)
+        return step, shift, read, mm3(scores, update), docs_first, docs_last
 
     step, shift, read, base, docs_first, docs_mid = block(own_ref)
     pal_step, pal_shift, pal_read, pal_base, docs_next, docs_last = block(pal_ref)

time: 144 us -> 144 us (level)
  no operation moved by 1% of the time
where the time goes in v5:
time: 144 us
  waiting for transfers between devices  47.8 us (33%)
  blocking collectives  28.2 us (20%)
  starting transfers between devices  27.3 us (19%)
  Pallas kernels  14.6 us (10%)
  between operations  13.5 us (9%)
  matrix products  5.62 us (4%)
  other arithmetic  4.23 us (3%)
  local copies, waits for them, and re-layouts  2.54 us (2%)
    ppermute x3, waiting for transfers between devices, passed(): lax.ppermute(array, SP, [(i, (i + ways[i % 2]) % count) for i in range(co...  19.7 us
    all_gather x1, waiting for transfers between devices, shards(): lax.all_gather(jnp.concatenate([widen_projection_weights, shrink_projecti...  15 us
    all_to_all x1, blocking collectives, shards(): pieces = lax.all_to_all(turned, 'tp', 0, 0, tiled=True)  14.3 us
    all_gather x1, blocking collectives, shards(): lax.all_gather(own_residual.astype(BF16), 'tp', axis=1, tiled=True)  13.9 us
    ppermute x2, starting transfers between devices, swapped(): return lax.ppermute(array, SP, [(i, i ^ 1) for i in range(count)])  9.91 us
    all_to_all x1, waiting for transfers between devices, shards(): parts = lax.all_to_all(head_terms, 'tp', 0, 0, tiled=True)  9.35 us
    all_to_all x1, starting transfers between devices, shards(): parts = lax.all_to_all(head_terms, 'tp', 0, 0, tiled=True)  9.19 us
    ppermute x3, starting transfers between devices, passed(): lax.ppermute(array, SP, [(i, (i + ways[i % 2]) % count) for i in range(co...  8.2 us
  transfers between devices with their start and end apart: 7, of which 6 were waited for; matrix products, arithmetic and copies ran while one was open for 1% of the time, Pallas kernels for 10%

profile of v5, /device:TPU:1, one launch (start us, length us, event | category | flops | bytes accessed | tf_op | source)
XLA Modules:
  0.0 143.8 jit_solution(14822057650201219886)
XLA Ops:
  6.5 0.0 all-gather.2.cloned.1.call-start
  6.5 1.5 %pad_maximum_fusion = bf16[32,2048]{1,0:T(8,128)(2,1)} fusion(bf16[32,1024]{1,0:T(8,128)(2,1)} %bitcast.16, bf16[32,1024]{1,0:T(8,128)(2,1)} %param.26), kind=kLoop, calls=%fused_computation.19 | loop fusion | flops 262144 | bytes 262144 | tf_op jit(solution)/shard_map/concatenate | solution.py:218
  8.1 0.0 all-gather.2.cloned.1.call-update
  8.1 1.5 %pack_inputs.1.own_ref = bf16[136,384]{1,0:T(8,128)(2,1)} custom-call(bf16[128,128]{1,0:T(8,128)(2,1)} %q_ref.1, bf16[128,128]{1,0:T(8,128)(2,1)} %k_ref.1, bf16[128,128]{1,0:T(8,128)(2,1)} %v_ref.1, f32[2,128]{1,0:T(2,128)} %bitcast.17, f32[2,128]{1,0:T(2,128)} %bitcast.18, f32[2,128]{1,0:T(2,128)} %bitcast.19, s32[1,128]{1,0:T(1,128)} %bitcast.20), custom_call_target="tpu_custom_call" | custom-call | tf_op jit(solution)/shard_map/pack_inputs/pallas_call | solution.py:200
  9.6 4.0 %collective-permute-start = (bf16[136,384]{1,0:T(8,128)(2,1)}, bf16[136,384]{1,0:T(8,128)(2,1)S(1)}, u32[]{:S(2)}, u32[]{:S(2)}) collective-permute-start(bf16[136,384]{1,0:T(8,128)(2,1)} %pack_inputs.1.own_ref), channel_id=1, source_target_pairs={{0,8},{8,0},{16,24},{24,16},{32,40},{40,32},{48,56},{56,48},{64,72... | collective-permute-start | bytes 313352 | tf_op jit(solution)/shard_map/ppermute | solution.py:194
  13.6 2.3 %collective-permute-done.pal_ref = bf16[136,384]{1,0:T(8,128)(2,1)S(1)} collective-permute-done((bf16[136,384]{1,0:T(8,128)(2,1)}, bf16[136,384]{1,0:T(8,128)(2,1)S(1)}, u32[]{:S(2)}, u32[]{:S(2)}) %collective-permute-start) | collective-permute-done | bytes 104480 | tf_op jit(solution)/shard_map/ppermute | solution.py:194
  15.9 0.0 copy-start
  15.9 0.6 copy-done
  16.5 7.0 %local_maps.1 = (bf16[144,256]{1,0:T(8,128)(2,1)}, bf16[2,128,128]{2,1,0:T(8,128)(2,1)}, f32[2,128,128]{2,1,0:T(8,128)}) custom-call(bf16[136,384]{1,0:T(8,128)(2,1)} %pack_inputs.1.own_ref, bf16[136,384]{1,0:T(8,128)(2,1)} %copy-done, f32[1,2]{1,0:T(1,128)} %bitcast.21), custom_call_target="tpu_custom_call" | custom-call | tf_op jit(solution)/shard_map/local_maps/pallas_call | solution.py:224
  23.5 4.4 %collective-permute-start.1 = (bf16[144,256]{1,0:T(8,128)(2,1)}, bf16[144,256]{1,0:T(8,128)(2,1)S(1)}, u32[]{:S(2)}, u32[]{:S(2)}) collective-permute-start(bf16[144,256]{1,0:T(8,128)(2,1)} %get-tuple-element.12.own_ref), channel_id=1, source_target_pairs={{0,16},{8,504},{16,32},{24,8},{32,48},{40,24},{48,64},{56,40},{64,... | collective-permute-start | bytes 221192 | tf_op jit(solution)/shard_map/ppermute | solution.py:198
  27.9 12.9 %collective-permute-done.1.in_ref = bf16[144,256]{1,0:T(8,128)(2,1)S(1)} collective-permute-done((bf16[144,256]{1,0:T(8,128)(2,1)}, bf16[144,256]{1,0:T(8,128)(2,1)S(1)}, u32[]{:S(2)}, u32[]{:S(2)}) %collective-permute-start.1) | collective-permute-done | bytes 73760 | tf_op jit(solution)/shard_map/ppermute | solution.py:198
  40.8 0.0 copy-start.1
  40.8 0.6 copy-done.1
  41.4 1.7 %combine_maps.1 = (bf16[144,256]{1,0:T(8,128)(2,1)}, bf16[144,128]{1,0:T(8,128)(2,1)}) custom-call(bf16[144,256]{1,0:T(8,128)(2,1)} %get-tuple-element.12.own_ref, bf16[144,256]{1,0:T(8,128)(2,1)} %copy-done.1), custom_call_target="tpu_custom_call" | custom-call | tf_op jit(solution)/shard_map/combine_maps/pallas_call | solution.py:235
  43.2 1.9 %collective-permute-start.2 = (bf16[144,256]{1,0:T(8,128)(2,1)}, bf16[144,256]{1,0:T(8,128)(2,1)S(1)}, u32[]{:S(2)}, u32[]{:S(2)}) collective-permute-start(bf16[144,256]{1,0:T(8,128)(2,1)} %get-tuple-element.13), channel_id=1, source_target_pairs={{0,16},{8,504},{16,32},{24,8},{32,48},{40,24},{48,64},{56,40},{64,... | collective-permute-start | bytes 221192 | tf_op jit(solution)/shard_map/ppermute | solution.py:198
  45.1 1.9 %collective-permute-start.3 = (bf16[144,128]{1,0:T(8,128)(2,1)}, bf16[144,128]{1,0:T(8,128)(2,1)S(1)}, u32[]{:S(2)}, u32[]{:S(2)}) collective-permute-start(bf16[144,128]{1,0:T(8,128)(2,1)} %get-tuple-element.14), channel_id=1, source_target_pairs={{0,48},{8,472},{16,64},{24,488},{32,80},{40,504},{48,96},{56,8},{6... | collective-permute-start | bytes 110600 | tf_op jit(solution)/shard_map/ppermute | solution.py:198
  47.0 6.8 %collective-permute-done.3.far_ref = bf16[144,128]{1,0:T(8,128)(2,1)S(1)} collective-permute-done((bf16[144,128]{1,0:T(8,128)(2,1)}, bf16[144,128]{1,0:T(8,128)(2,1)S(1)}, u32[]{:S(2)}, u32[]{:S(2)}) %collective-permute-start.3) | collective-permute-done | bytes 36896 | tf_op jit(solution)/shard_map/ppermute | solution.py:198
  53.8 0.0 copy-start.3
  53.8 0.0 collective-permute-done.2.near_ref
  53.8 0.0 copy-start.2
  53.8 0.6 copy-done.3
  54.4 0.0 copy-done.2
  54.4 2.0 %apply_state.1 = (f32[128,128]{1,0:T(8,128)}, bf16[128,128]{1,0:T(8,128)(2,1)}) custom-call(bf16[144,256]{1,0:T(8,128)(2,1)} %get-tuple-element.12.own_ref, bf16[144,256]{1,0:T(8,128)(2,1)} %copy-done.2, bf16[144,128]{1,0:T(8,128)(2,1)} %copy-done.3, bf16[2,128,128]{2,1,0:T(8,128)(2,1)} %get-tuple-element.15.read_ref, f32[2,128,128]{2,1,0:T(8,128)} %get-tuple-element.16.base_ref), custom_call_target="tpu_custom_call" | custom-call | tf_op jit(solution)/shard_map/apply_state/pallas_call | solution.py:245
  56.4 5.9 %collective-permute-start.4 = (bf16[128,128]{1,0:T(8,128)(2,1)}, bf16[128,128]{1,0:T(8,128)(2,1)S(1)}, u32[]{:S(2)}, u32[]{:S(2)}) collective-permute-start(bf16[128,128]{1,0:T(8,128)(2,1)} %get-tuple-element.18), channel_id=1, source_target_pairs={{0,8},{8,0},{16,24},{24,16},{32,40},{40,32},{48,56},{56,48},{64,72... | collective-permute-start | bytes 98312 | tf_op jit(solution)/shard_map/ppermute | solution.py:194
  62.3 1.5 %collective-permute-done.4.in_ref = bf16[128,128]{1,0:T(8,128)(2,1)S(1)} collective-permute-done((bf16[128,128]{1,0:T(8,128)(2,1)}, bf16[128,128]{1,0:T(8,128)(2,1)S(1)}, u32[]{:S(2)}, u32[]{:S(2)}) %collective-permute-start.4) | collective-permute-done | bytes 32800 | tf_op jit(solution)/shard_map/ppermute | solution.py:194
  63.8 0.0 copy-start.4
  63.8 0.6 copy-done.4
  64.4 2.3 %finish_mixer.1 = bf16[8,128,256]{2,1,0:T(8,128)(2,1)} custom-call(f32[128,128]{1,0:T(8,128)} %get-tuple-element.17.mine_ref, bf16[128,128]{1,0:T(8,128)(2,1)} %copy-done.4, f32[1,128]{1,0:T(1,128)} %bitcast.22, bf16[128,2048]{1,0:T(8,128)(2,1)} %exit_ref.1), custom_call_target="tpu_custom_call" | custom-call | tf_op jit(solution)/shard_map/finish_mixer/pallas_call | solution.py:255
  66.8 9.2 %all-to-all-start = ((bf16[8,128,256]{2,1,0:T(8,128)(2,1)}), bf16[8,128,256]{2,1,0:T(8,128)(2,1)S(1)}, u32[]{:S(2)}, u32[]{:S(2)}) async-start(bf16[8,128,256]{2,1,0:T(8,128)(2,1)} %finish_mixer.1), calls=%async_computation | async-start | bytes 1048576 | tf_op jit(solution)/shard_map/all_to_all | solution.py:265
  76.0 9.3 %all-to-all-done = bf16[8,128,256]{2,1,0:T(8,128)(2,1)S(1)} async-done(((bf16[8,128,256]{2,1,0:T(8,128)(2,1)}), bf16[8,128,256]{2,1,0:T(8,128)(2,1)S(1)}, u32[]{:S(2)}, u32[]{:S(2)}) %all-to-all-start) | async-done | bytes 524320 | tf_op jit(solution)/shard_map/all_to_all | solution.py:265
  85.3 0.1 convert_reduce_fusion.1
  85.4 0.9 fusion.28
  86.2 13.9 %all_gather.6 = bf16[128,2048]{1,0:T(8,128)(2,1)S(1)} all-gather(bf16[128,256]{1,0:T(8,128)(2,1)S(1)} %fusion.28), channel_id=1, replica_groups=mesh['sp_0'=8,'sp_1'=4,'pair'=2,'tp'=8] {'tp'}, dimensions={1}, use_global_device_ids=true | all-gather | bytes 589824 | tf_op jit(solution)/shard_map/all_gather | solution.py:269
  100.2 0.2 fusion.18
  100.4 15.0 %all-gather.2.cloned.1.call-done = bf16[2048,2048]{1,0:T(8,128)(2,1)} async-done(((bf16[32,2048]{1,0:T(8,128)(2,1)}), bf16[2048,2048]{1,0:T(8,128)(2,1)}) %all-gather.2.cloned.1.call-update) | async-done | bytes 8388624 | tf_op jit(solution)/shard_map/all_gather | solution.py:217
  115.4 5.6 %fusion.4 = bf16[128,2048]{1,0:T(8,128)(2,1)S(1)} fusion(bf16[2048,2048]{1,0:T(8,128)(2,1)} %all-gather.2.cloned.1.call-done, bf16[128,2048]{1,0:T(8,128)(2,1)S(1)} %all_gather.6, f32[2048]{0:T(1024)} %param.25, f32[128]{0:T(128)S(1)} %add_rsqrt_fusion), kind=kOutput, calls=%fused_computation.4 | convolution fusion | flops 1075445760 | bytes 9445888 | tf_op jit(solution)/shard_map/dot_general | solution.py:274
  121.0 14.3 %all_to_all.10 = bf16[8,128,256]{2,1,0:T(8,128)(2,1)S(1)} all-to-all(bf16[8,128,256]{2,1,0:T(8,128)(2,1)S(1)} %bitcast.14), channel_id=1, replica_groups=mesh['sp_0'=8,'sp_1'=4,'pair'=2,'tp'=8] {'tp'}, dimensions={0} | all-to-all | bytes 1048576 | tf_op jit(solution)/shard_map/all_to_all | solution.py:276
  135.3 0.1 convert_reduce_fusion
  135.4 1.5 %add_convert_fusion = bf16[128,256]{1,0:T(8,128)(2,1)} fusion(f32[128,256]{1,0:T(8,128)S(1)} %convert_reduce_fusion, f32[128,256]{1,0:T(8,128)S(1)} %convert_reduce_fusion.1, bf16[128,2048]{1,0:T(8,128)(2,1)} %param.14, s32[]{:T(128)S(6)} %select_n.3), kind=kLoop, calls=%fused_computation.20 | loop fusion | flops 131072 | bytes 393220 | tf_op jit(solution)/shard_map/convert_element_type | solution.py:277
  (2 shorter events, 0.0 us)
Async XLA Ops:
  6.5 108.8 %all-gather.2.cloned.1.call-start = ((), (), s32[]{:S(2)}) async-start(), calls=%async_computation.2 | async-start | bytes 8519680 | tf_op jit(solution)/shard_map/all_gather | solution.py:217
  9.6 6.3 %collective-permute-start = (bf16[136,384]{1,0:T(8,128)(2,1)}, bf16[136,384]{1,0:T(8,128)(2,1)S(1)}, u32[]{:S(2)}, u32[]{:S(2)}) collective-permute-start(bf16[136,384]{1,0:T(8,128)(2,1)} %pack_inputs.1.own_ref), channel_id=1, source_target_pairs={{0,8},{8,0},{16,24},{24,16},{32,40},{40,32},{48,56},{56,48},{64,72... | collective-permute-start | bytes 313352 | tf_op jit(solution)/shard_map/ppermute | solution.py:194
  15.9 0.6 copy-start
  23.5 17.3 %collective-permute-start.1 = (bf16[144,256]{1,0:T(8,128)(2,1)}, bf16[144,256]{1,0:T(8,128)(2,1)S(1)}, u32[]{:S(2)}, u32[]{:S(2)}) collective-permute-start(bf16[144,256]{1,0:T(8,128)(2,1)} %get-tuple-element.12.own_ref), channel_id=1, source_target_pairs={{0,16},{8,504},{16,32},{24,8},{32,48},{40,24},{48,64},{56,40},{64,... | collective-permute-start | bytes 221192 | tf_op jit(solution)/shard_map/ppermute | solution.py:198
  40.8 0.6 copy-start.1
  43.2 10.6 %collective-permute-start.2 = (bf16[144,256]{1,0:T(8,128)(2,1)}, bf16[144,256]{1,0:T(8,128)(2,1)S(1)}, u32[]{:S(2)}, u32[]{:S(2)}) collective-permute-start(bf16[144,256]{1,0:T(8,128)(2,1)} %get-tuple-element.13), channel_id=1, source_target_pairs={{0,16},{8,504},{16,32},{24,8},{32,48},{40,24},{48,64},{56,40},{64,... | collective-permute-start | bytes 221192 | tf_op jit(solution)/shard_map/ppermute | solution.py:198
  45.1 8.7 %collective-permute-start.3 = (bf16[144,128]{1,0:T(8,128)(2,1)}, bf16[144,128]{1,0:T(8,128)(2,1)S(1)}, u32[]{:S(2)}, u32[]{:S(2)}) collective-permute-start(bf16[144,128]{1,0:T(8,128)(2,1)} %get-tuple-element.14), channel_id=1, source_target_pairs={{0,48},{8,472},{16,64},{24,488},{32,80},{40,504},{48,96},{56,8},{6... | collective-permute-start | bytes 110600 | tf_op jit(solution)/shard_map/ppermute | solution.py:198
  53.8 0.6 copy-start.3
  53.8 0.6 copy-start.2
  56.4 7.4 %collective-permute-start.4 = (bf16[128,128]{1,0:T(8,128)(2,1)}, bf16[128,128]{1,0:T(8,128)(2,1)S(1)}, u32[]{:S(2)}, u32[]{:S(2)}) collective-permute-start(bf16[128,128]{1,0:T(8,128)(2,1)} %get-tuple-element.18), channel_id=1, source_target_pairs={{0,8},{8,0},{16,24},{24,16},{32,40},{40,32},{48,56},{56,48},{64,72... | collective-permute-start | bytes 98312 | tf_op jit(solution)/shard_map/ppermute | solution.py:194
  63.8 0.6 copy-start.4
  66.8 18.5 %all-to-all-start = ((bf16[8,128,256]{2,1,0:T(8,128)(2,1)}), bf16[8,128,256]{2,1,0:T(8,128)(2,1)S(1)}, u32[]{:S(2)}, u32[]{:S(2)}) async-start(bf16[8,128,256]{2,1,0:T(8,128)(2,1)} %finish_mixer.1), calls=%async_computation | async-start | bytes 1048576 | tf_op jit(solution)/shard_map/all_to_all | solution.py:265
Sparse Core Ops, SparseCore 0:
  10.4 104.9 all-gather.1

commit v6 on v5

--- a/solution.py
+++ b/solution.py
@@ -8,6 +8,7 @@
 
 SP = ("sp_0", "sp_1", "pair")
 EPSILON = 1e-06
+SIDE = 128
 F32 = jnp.float32
 BF16 = jnp.bfloat16
 NT = (((1,), (1,)), ((), ()))
@@ -213,13 +214,19 @@
         sample_membership.reshape(1, length),
     )
     pal_data = swapped(data)
-    up_width = widen_projection_weights.shape[1]
+    up_width = widen_projection_weights.shape[1] - SIDE
+    turned_down = shrink_projection_weights.T
     weights = lax.all_gather(
-        jnp.concatenate([widen_projection_weights, shrink_projection_weights.T], axis=1),
+        jnp.concatenate([widen_projection_weights[:, :up_width], turned_down[:, :up_width]], axis=1),
         SP,
         axis=0,
         tiled=True,
     )
+    few = jnp.concatenate([widen_projection_weights[:, up_width:], turned_down[:, up_width:]], axis=1)
+    for axes in (SP[1:], SP[:1]):
+        size = lax.axis_size(axes)
+        copies = jnp.broadcast_to(few[None], (size, *few.shape))
+        few = lax.all_to_all(copies, axes, 0, 0, tiled=True).reshape(-1, few.shape[1])
     tall = width + 16
     message, read, base = pl.pallas_call(
         local_kernel,
@@ -232,6 +239,7 @@
         out_specs=tuple(vmem(3)),
         name="local_maps",
     )(data, pal_data, forgetting_speed_exponent.T)
+    before = passed(message, 1)
     joined, far = pl.pallas_call(
         combine_kernel,
         out_shape=(
@@ -241,7 +249,7 @@
         in_specs=vmem(2),
         out_specs=tuple(vmem(2)),
         name="combine_maps",
-    )(message, passed(message, 1))
+    )(message, before)
     mine, other = pl.pallas_call(
         apply_kernel,
         out_shape=(
@@ -259,6 +267,7 @@
         out_specs=vmem(1)[0],
         name="finish_mixer",
     )(mine, swapped(other), channel_group_scaling.reshape(1, width), blend_exit_weights)
+    few, head_terms = lax.optimization_barrier((few, head_terms))
     model_width = skip_path_inputs.shape[1]
     col_count = model_width // lax.axis_size("tp")
     col_start = lax.axis_index("tp") * col_count
@@ -269,9 +278,13 @@
     residual = lax.all_gather(own_residual.astype(BF16), "tp", axis=1, tiled=True).astype(F32)
     squares = jnp.mean(residual * residual, axis=1, keepdims=True)
     normed = (residual * lax.rsqrt(squares + EPSILON) * dense_block_scaling).astype(BF16)
-    raised = jnp.dot(normed, weights[:, :up_width], preferred_element_type=F32)
-    active = jnp.square(jax.nn.relu(raised)).astype(BF16)
-    lowered = lax.dot_general(active, weights[:, up_width:], NT, preferred_element_type=F32)
+
+    def fed(matrix, middle):
+        raised = jnp.dot(normed, matrix[:, :middle], preferred_element_type=F32)
+        active = jnp.square(jax.nn.relu(raised)).astype(BF16)
+        return lax.dot_general(active, matrix[:, middle:], NT, preferred_element_type=F32)
+
+    lowered = fed(few, SIDE) + fed(weights, up_width)
     turned = jnp.moveaxis(lowered.astype(BF16).reshape(length, -1, col_count), 1, 0)
     pieces = lax.all_to_all(turned, "tp", 0, 0, tiled=True)
     return (own_residual + jnp.sum(pieces.astype(F32), axis=0)).astype(BF16)
@@ -295,6 +308,7 @@
         P(SP, "tp"),
         P("tp", SP),
     )
+
     return jax.shard_map(
         shards, mesh=torus, in_specs=placed, out_specs=P(SP, "tp"), check_vma=False
     )

time: 144 us -> 149 us (1.035)
  waiting for transfers between devices: 47.8 us -> 27.2 us
  blocking collectives: 28.2 us -> 41.3 us
  starting transfers between devices: 27.3 us -> 35.9 us
  local copies, waits for them, and re-layouts: 2.54 us -> 6.72 us
    all_to_all x0 -> x1, blocking collectives: none -> 15.4 us  [shards(): lax.all_to_all(copies, axes, 0, 0, tiled=True).reshape(-1, few.shape[1])]
    all_gather x1, waiting for transfers between devices: 15 us -> 0.02 us  [shards(): lax.all_gather(jnp.concatenate([widen_projection_weights[:, :up_width], t...]
    all_to_all x0 -> x1, starting transfers between devices: none -> 9.86 us  [shards(): lax.all_to_all(copies, axes, 0, 0, tiled=True).reshape(-1, few.shape[1])]
    ppermute x3, waiting for transfers between devices: 19.7 us -> 11.1 us  [passed(): lax.ppermute(array, SP, [(i, (i + ways[i % 2]) % count) for i in range(co...]
    ppermute x2, starting transfers between devices: 9.91 us -> 6.19 us  [swapped(): return lax.ppermute(array, SP, [(i, i ^ 1) for i in range(count)])]
    slice x0 -> x4, local copies, waits for them, and re-layouts: none -> 3.06 us  [the longest x1 0.83 us: shards(): turned_down[:, :up_width]]
    ppermute x2, waiting for transfers between devices: 3.77 us -> 6.7 us  [swapped(): return lax.ppermute(array, SP, [(i, i ^ 1) for i in range(count)])]
    all_to_all x1, blocking collectives: 14.3 us -> 12 us  [shards(): pieces = lax.all_to_all(turned, 'tp', 0, 0, tiled=True)]
  transfers between devices with their start and end apart: 7 -> 8, of which waited for: 6 -> 5; matrix products, arithmetic and copies ran while one was open for 1% -> 3% of each run, Pallas kernels for 10% -> 10%
where the time goes in v6:
time: 149 us; the launch traced here: 148 us
  blocking collectives  41.3 us (28%)
  starting transfers between devices  35.9 us (24%)
  waiting for transfers between devices  27.2 us (18%)
  Pallas kernels  14.5 us (10%)
  between operations  13.5 us (9%)
  local copies, waits for them, and re-layouts  6.72 us (5%)
  matrix products  5.7 us (4%)
  other arithmetic  3.37 us (2%)
    all_to_all x1, blocking collectives, shards(): lax.all_to_all(copies, axes, 0, 0, tiled=True).reshape(-1, few.shape[1])  15.4 us
    all_gather x1, blocking collectives, shards(): lax.all_gather(own_residual.astype(BF16), 'tp', axis=1, tiled=True)  13.9 us
    all_to_all x1, blocking collectives, shards(): pieces = lax.all_to_all(turned, 'tp', 0, 0, tiled=True)  12 us
    ppermute x3, waiting for transfers between devices, passed(): lax.ppermute(array, SP, [(i, (i + ways[i % 2]) % count) for i in range(co...  11.1 us
    all_to_all x1, starting transfers between devices, shards(): parts = lax.all_to_all(head_terms, 'tp', 0, 0, tiled=True)  10.8 us
    all_to_all x1, starting transfers between devices, shards(): lax.all_to_all(copies, axes, 0, 0, tiled=True).reshape(-1, few.shape[1])  9.86 us
    all_to_all x1, waiting for transfers between devices, shards(): parts = lax.all_to_all(head_terms, 'tp', 0, 0, tiled=True)  9.35 us
    ppermute x3, starting transfers between devices, passed(): lax.ppermute(array, SP, [(i, (i + ways[i % 2]) % count) for i in range(co...  9.08 us
  transfers between devices with their start and end apart: 8, of which 5 were waited for; matrix products, arithmetic and copies ran while one was open for 3% of the time, Pallas kernels for 10%

profile of v6, /device:TPU:1, one launch (start us, length us, event | category | flops | bytes accessed | tf_op | source)
XLA Modules:
  0.0 148.2 jit_solution(15987425278715594067)
XLA Ops:
  6.5 0.0 copy-start.5
  6.5 0.0 all-gather.2.cloned.1.call-start
  6.5 0.8 slice.33
  7.4 0.8 slice.28
  8.2 0.7 pad_maximum_fusion
  8.9 0.0 all-gather.2.cloned.1.call-update
  8.9 0.7 slice.32
  9.6 0.7 slice.24
  10.3 15.4 %all_to_all.20 = bf16[8,32,256]{2,1,0:T(8,128)(2,1)S(1)} all-to-all(bf16[8,32,256]{2,1,0:T(8,128)(2,1)S(1)} %broadcast_in_dim.6), channel_id=1, replica_groups=mesh['sp_0'=8,'sp_1'=4,'pair'=2,'tp'=8] {'sp_1','pair'}, dimensions={0} | all-to-all | bytes 262144 | tf_op jit(solution)/shard_map/all_to_all | solution.py:229
  25.7 1.1 broadcast_in_dim.8
  26.7 9.9 %all-to-all-start.1 = ((bf16[8,256,256]{2,1,0:T(8,128)(2,1)}), bf16[8,256,256]{2,1,0:T(8,128)(2,1)S(1)}, u32[]{:S(2)}, u32[]{:S(2)}) async-start(bf16[8,256,256]{2,1,0:T(8,128)(2,1)} %broadcast_in_dim.8), calls=%async_computation.1 | async-start | bytes 2097152 | tf_op jit(solution)/shard_map/all_to_all | solution.py:229
  36.6 1.5 %pack_inputs.1.own_ref = bf16[136,384]{1,0:T(8,128)(2,1)} custom-call(bf16[128,128]{1,0:T(8,128)(2,1)} %q_ref.1, bf16[128,128]{1,0:T(8,128)(2,1)} %k_ref.1, bf16[128,128]{1,0:T(8,128)(2,1)} %v_ref.1, f32[2,128]{1,0:T(2,128)} %bitcast.22, f32[2,128]{1,0:T(2,128)} %bitcast.23, f32[2,128]{1,0:T(2,128)} %bitcast.24, s32[1,128]{1,0:T(1,128)} %bitcast.25), custom_call_target="tpu_custom_call" | custom-call | tf_op jit(solution)/shard_map/pack_inputs/pallas_call | solution.py:201
  38.1 2.3 %collective-permute-start = (bf16[136,384]{1,0:T(8,128)(2,1)}, bf16[136,384]{1,0:T(8,128)(2,1)S(1)}, u32[]{:S(2)}, u32[]{:S(2)}) collective-permute-start(bf16[136,384]{1,0:T(8,128)(2,1)} %pack_inputs.1.own_ref), channel_id=1, source_target_pairs={{0,8},{8,0},{16,24},{24,16},{32,40},{40,32},{48,56},{56,48},{64,72... | collective-permute-start | bytes 313352 | tf_op jit(solution)/shard_map/ppermute | solution.py:195
  40.5 4.0 %collective-permute-done.pal_ref = bf16[136,384]{1,0:T(8,128)(2,1)S(1)} collective-permute-done((bf16[136,384]{1,0:T(8,128)(2,1)}, bf16[136,384]{1,0:T(8,128)(2,1)S(1)}, u32[]{:S(2)}, u32[]{:S(2)}) %collective-permute-start) | collective-permute-done | bytes 104480 | tf_op jit(solution)/shard_map/ppermute | solution.py:195
  44.4 0.0 copy-start
  44.4 0.6 copy-done
  45.1 7.0 %local_maps.1 = (bf16[144,256]{1,0:T(8,128)(2,1)}, bf16[2,128,128]{2,1,0:T(8,128)(2,1)}, f32[2,128,128]{2,1,0:T(8,128)}) custom-call(bf16[136,384]{1,0:T(8,128)(2,1)} %pack_inputs.1.own_ref, bf16[136,384]{1,0:T(8,128)(2,1)} %copy-done, f32[1,2]{1,0:T(1,128)} %bitcast.26), custom_call_target="tpu_custom_call" | custom-call | tf_op jit(solution)/shard_map/local_maps/pallas_call | solution.py:231
  52.1 1.9 %collective-permute-start.1 = (bf16[144,256]{1,0:T(8,128)(2,1)}, bf16[144,256]{1,0:T(8,128)(2,1)S(1)}, u32[]{:S(2)}, u32[]{:S(2)}) collective-permute-start(bf16[144,256]{1,0:T(8,128)(2,1)} %get-tuple-element.14.own_ref), channel_id=1, source_target_pairs={{0,16},{8,504},{16,32},{24,8},{32,48},{40,24},{48,64},{56,40},{64,... | collective-permute-start | bytes 221192 | tf_op jit(solution)/shard_map/ppermute | solution.py:199
  54.0 8.0 %collective-permute-done.1.in_ref = bf16[144,256]{1,0:T(8,128)(2,1)S(1)} collective-permute-done((bf16[144,256]{1,0:T(8,128)(2,1)}, bf16[144,256]{1,0:T(8,128)(2,1)S(1)}, u32[]{:S(2)}, u32[]{:S(2)}) %collective-permute-start.1) | collective-permute-done | bytes 73760 | tf_op jit(solution)/shard_map/ppermute | solution.py:199
  62.0 0.0 copy-start.1
  62.0 0.6 copy-done.1
  62.6 1.7 %combine_maps.1 = (bf16[144,256]{1,0:T(8,128)(2,1)}, bf16[144,128]{1,0:T(8,128)(2,1)}) custom-call(bf16[144,256]{1,0:T(8,128)(2,1)} %get-tuple-element.14.own_ref, bf16[144,256]{1,0:T(8,128)(2,1)} %copy-done.1), custom_call_target="tpu_custom_call" | custom-call | tf_op jit(solution)/shard_map/combine_maps/pallas_call | solution.py:243
  64.4 1.9 %collective-permute-start.2 = (bf16[144,256]{1,0:T(8,128)(2,1)}, bf16[144,256]{1,0:T(8,128)(2,1)S(1)}, u32[]{:S(2)}, u32[]{:S(2)}) collective-permute-start(bf16[144,256]{1,0:T(8,128)(2,1)} %get-tuple-element.15), channel_id=1, source_target_pairs={{0,16},{8,504},{16,32},{24,8},{32,48},{40,24},{48,64},{56,40},{64,... | collective-permute-start | bytes 221192 | tf_op jit(solution)/shard_map/ppermute | solution.py:199
  66.3 5.3 %collective-permute-start.3 = (bf16[144,128]{1,0:T(8,128)(2,1)}, bf16[144,128]{1,0:T(8,128)(2,1)S(1)}, u32[]{:S(2)}, u32[]{:S(2)}) collective-permute-start(bf16[144,128]{1,0:T(8,128)(2,1)} %get-tuple-element.16), channel_id=1, source_target_pairs={{0,48},{8,472},{16,64},{24,488},{32,80},{40,504},{48,96},{56,8},{6... | collective-permute-start | bytes 110600 | tf_op jit(solution)/shard_map/ppermute | solution.py:199
  71.6 3.1 %collective-permute-done.3.far_ref = bf16[144,128]{1,0:T(8,128)(2,1)S(1)} collective-permute-done((bf16[144,128]{1,0:T(8,128)(2,1)}, bf16[144,128]{1,0:T(8,128)(2,1)S(1)}, u32[]{:S(2)}, u32[]{:S(2)}) %collective-permute-start.3) | collective-permute-done | bytes 36896 | tf_op jit(solution)/shard_map/ppermute | solution.py:199
  74.7 0.0 copy-start.3
  74.7 0.0 collective-permute-done.2.near_ref
  74.7 0.0 copy-start.2
  74.7 0.6 copy-done.3
  75.3 0.0 copy-done.2
  75.3 2.0 %apply_state.1 = (f32[128,128]{1,0:T(8,128)}, bf16[128,128]{1,0:T(8,128)(2,1)}) custom-call(bf16[144,256]{1,0:T(8,128)(2,1)} %get-tuple-element.14.own_ref, bf16[144,256]{1,0:T(8,128)(2,1)} %copy-done.2, bf16[144,128]{1,0:T(8,128)(2,1)} %copy-done.3, bf16[2,128,128]{2,1,0:T(8,128)(2,1)} %get-tuple-element.17.read_ref, f32[2,128,128]{2,1,0:T(8,128)} %get-tuple-element.18.base_ref), custom_call_target="tpu_custom_call" | custom-call | tf_op jit(solution)/shard_map/apply_state/pallas_call | solution.py:253
  77.3 3.8 %collective-permute-start.4 = (bf16[128,128]{1,0:T(8,128)(2,1)}, bf16[128,128]{1,0:T(8,128)(2,1)S(1)}, u32[]{:S(2)}, u32[]{:S(2)}) collective-permute-start(bf16[128,128]{1,0:T(8,128)(2,1)} %get-tuple-element.20), channel_id=1, source_target_pairs={{0,8},{8,0},{16,24},{24,16},{32,40},{40,32},{48,56},{56,48},{64,72... | collective-permute-start | bytes 98312 | tf_op jit(solution)/shard_map/ppermute | solution.py:195
  81.1 2.7 %collective-permute-done.4.in_ref = bf16[128,128]{1,0:T(8,128)(2,1)S(1)} collective-permute-done((bf16[128,128]{1,0:T(8,128)(2,1)}, bf16[128,128]{1,0:T(8,128)(2,1)S(1)}, u32[]{:S(2)}, u32[]{:S(2)}) %collective-permute-start.4) | collective-permute-done | bytes 32800 | tf_op jit(solution)/shard_map/ppermute | solution.py:195
  83.9 0.0 copy-start.4
  83.9 0.6 copy-done.4
  84.5 2.3 %finish_mixer.1 = bf16[8,128,256]{2,1,0:T(8,128)(2,1)} custom-call(f32[128,128]{1,0:T(8,128)} %get-tuple-element.19.mine_ref, bf16[128,128]{1,0:T(8,128)(2,1)} %copy-done.4, f32[1,128]{1,0:T(1,128)} %bitcast.27, bf16[128,2048]{1,0:T(8,128)(2,1)} %exit_ref.1), custom_call_target="tpu_custom_call" | custom-call | tf_op jit(solution)/shard_map/finish_mixer/pallas_call | solution.py:263
  86.8 0.0 all-to-all-done.1
  86.8 10.8 %all-to-all-start.2 = ((bf16[8,128,256]{2,1,0:T(8,128)(2,1)}), bf16[8,128,256]{2,1,0:T(8,128)(2,1)S(1)}, u32[]{:S(2)}, u32[]{:S(2)}) async-start(bf16[8,128,256]{2,1,0:T(8,128)(2,1)} %finish_mixer.1), calls=%async_computation.2 | async-start | bytes 1048576 | tf_op jit(solution)/shard_map/all_to_all | solution.py:274
  97.6 9.3 %all-to-all-done.2 = bf16[8,128,256]{2,1,0:T(8,128)(2,1)S(1)} async-done(((bf16[8,128,256]{2,1,0:T(8,128)(2,1)}), bf16[8,128,256]{2,1,0:T(8,128)(2,1)S(1)}, u32[]{:S(2)}, u32[]{:S(2)}) %all-to-all-start.2) | async-done | bytes 524320 | tf_op jit(solution)/shard_map/all_to_all | solution.py:274
  106.9 0.1 convert_reduce_fusion.1
  107.0 0.9 fusion.35
  107.8 13.9 %all_gather.6 = bf16[128,2048]{1,0:T(8,128)(2,1)S(1)} all-gather(bf16[128,256]{1,0:T(8,128)(2,1)S(1)} %fusion.35), channel_id=1, replica_groups=mesh['sp_0'=8,'sp_1'=4,'pair'=2,'tp'=8] {'tp'}, dimensions={1}, use_global_device_ids=true | all-gather | bytes 589824 | tf_op jit(solution)/shard_map/all_gather | solution.py:278
  121.8 0.2 fusion.24
  122.0 0.0 copy-done.5
  122.0 0.6 fusion.23
  122.6 0.0 all-gather.2.cloned.1.call-done
  122.6 5.1 %fusion.7 = bf16[128,2048]{1,0:T(8,128)(2,1)S(1)} fusion(f32[128,2048]{1,0:T(8,128)S(1)} %fusion.23, bf16[2048,1792]{1,0:T(8,128)(2,1)} %all-gather.2.cloned.1.call-done, bf16[128,2048]{1,0:T(8,128)(2,1)S(1)} %all_gather.6, f32[2048]{0:T(1024)S(1)} %copy-done.5, f32[128]{0:T(128)S(1)} %add_rsqrt_fusion), kind=kOutput, calls=%fused_computation.5 | convolution fusion | flops 941441024 | bytes 9445888 | tf_op jit(solution)/shard_map/dot_general | solution.py:285
  127.7 12.0 %all_to_all.21 = bf16[8,128,256]{2,1,0:T(8,128)(2,1)S(1)} all-to-all(bf16[8,128,256]{2,1,0:T(8,128)(2,1)S(1)} %bitcast.17), channel_id=1, replica_groups=mesh['sp_0'=8,'sp_1'=4,'pair'=2,'tp'=8] {'tp'}, dimensions={0} | all-to-all | bytes 1048576 | tf_op jit(solution)/shard_map/all_to_all | solution.py:289
  139.8 0.1 convert_reduce_fusion
  139.8 1.5 %add_convert_fusion = bf16[128,256]{1,0:T(8,128)(2,1)} fusion(f32[128,256]{1,0:T(8,128)S(1)} %convert_reduce_fusion, f32[128,256]{1,0:T(8,128)S(1)} %convert_reduce_fusion.1, bf16[128,2048]{1,0:T(8,128)(2,1)} %param.14, s32[]{:T(128)S(6)} %select_n.3), kind=kLoop, calls=%fused_computation.24 | loop fusion | flops 131072 | bytes 393220 | tf_op jit(solution)/shard_map/convert_element_type | solution.py:290
  (4 shorter events, 0.1 us)
Async XLA Ops:
  6.5 115.4 %copy-start.5 = (f32[2048]{0:T(1024)S(1)}, f32[2048]{0:T(1024)}, u32[]{:S(2)}) copy-start(f32[2048]{0:T(1024)} %param.25) | copy-start | bytes 24580
  6.5 116.0 %all-gather.2.cloned.1.call-start = ((), (), s32[]{:S(2)}) async-start(), calls=%async_computation.4 | async-start | bytes 7454720 | tf_op jit(solution)/shard_map/all_gather | solution.py:219
  26.7 60.0 %all-to-all-start.1 = ((bf16[8,256,256]{2,1,0:T(8,128)(2,1)}), bf16[8,256,256]{2,1,0:T(8,128)(2,1)S(1)}, u32[]{:S(2)}, u32[]{:S(2)}) async-start(bf16[8,256,256]{2,1,0:T(8,128)(2,1)} %broadcast_in_dim.8), calls=%async_computation.1 | async-start | bytes 2097152 | tf_op jit(solution)/shard_map/all_to_all | solution.py:229
  38.1 6.3 %collective-permute-start = (bf16[136,384]{1,0:T(8,128)(2,1)}, bf16[136,384]{1,0:T(8,128)(2,1)S(1)}, u32[]{:S(2)}, u32[]{:S(2)}) collective-permute-start(bf16[136,384]{1,0:T(8,128)(2,1)} %pack_inputs.1.own_ref), channel_id=1, source_target_pairs={{0,8},{8,0},{16,24},{24,16},{32,40},{40,32},{48,56},{56,48},{64,72... | collective-permute-start | bytes 313352 | tf_op jit(solution)/shard_map/ppermute | solution.py:195
  44.4 0.7 copy-start
  52.1 9.9 %collective-permute-start.1 = (bf16[144,256]{1,0:T(8,128)(2,1)}, bf16[144,256]{1,0:T(8,128)(2,1)S(1)}, u32[]{:S(2)}, u32[]{:S(2)}) collective-permute-start(bf16[144,256]{1,0:T(8,128)(2,1)} %get-tuple-element.14.own_ref), channel_id=1, source_target_pairs={{0,16},{8,504},{16,32},{24,8},{32,48},{40,24},{48,64},{56,40},{64,... | collective-permute-start | bytes 221192 | tf_op jit(solution)/shard_map/ppermute | solution.py:199
  62.0 0.6 copy-start.1
  64.4 10.3 %collective-permute-start.2 = (bf16[144,256]{1,0:T(8,128)(2,1)}, bf16[144,256]{1,0:T(8,128)(2,1)S(1)}, u32[]{:S(2)}, u32[]{:S(2)}) collective-permute-start(bf16[144,256]{1,0:T(8,128)(2,1)} %get-tuple-element.15), channel_id=1, source_target_pairs={{0,16},{8,504},{16,32},{24,8},{32,48},{40,24},{48,64},{56,40},{64,... | collective-permute-start | bytes 221192 | tf_op jit(solution)/shard_map/ppermute | solution.py:199
  66.3 8.4 %collective-permute-start.3 = (bf16[144,128]{1,0:T(8,128)(2,1)}, bf16[144,128]{1,0:T(8,128)(2,1)S(1)}, u32[]{:S(2)}, u32[]{:S(2)}) collective-permute-start(bf16[144,128]{1,0:T(8,128)(2,1)} %get-tuple-element.16), channel_id=1, source_target_pairs={{0,48},{8,472},{16,64},{24,488},{32,80},{40,504},{48,96},{56,8},{6... | collective-permute-start | bytes 110600 | tf_op jit(solution)/shard_map/ppermute | solution.py:199
  74.7 0.6 copy-start.3
  74.7 0.6 copy-start.2
  77.3 6.6 %collective-permute-start.4 = (bf16[128,128]{1,0:T(8,128)(2,1)}, bf16[128,128]{1,0:T(8,128)(2,1)S(1)}, u32[]{:S(2)}, u32[]{:S(2)}) collective-permute-start(bf16[128,128]{1,0:T(8,128)(2,1)} %get-tuple-element.20), channel_id=1, source_target_pairs={{0,8},{8,0},{16,24},{24,16},{32,40},{40,32},{48,56},{56,48},{64,72... | collective-permute-start | bytes 98312 | tf_op jit(solution)/shard_map/ppermute | solution.py:195
  83.9 0.6 copy-start.4
  86.8 20.1 %all-to-all-start.2 = ((bf16[8,128,256]{2,1,0:T(8,128)(2,1)}), bf16[8,128,256]{2,1,0:T(8,128)(2,1)S(1)}, u32[]{:S(2)}, u32[]{:S(2)}) async-start(bf16[8,128,256]{2,1,0:T(8,128)(2,1)} %finish_mixer.1), calls=%async_computation.2 | async-start | bytes 1048576 | tf_op jit(solution)/shard_map/all_to_all | solution.py:274
Sparse Core Ops, SparseCore 0:
  10.3 107.5 all-gather.1
